TPU v7x, 32 devices: a whole 2x2x4 slice. The times are simulated.
32 devices in a mesh: sp: 4 (over z), fs: 4 (over y, x), tp: 2 (over core).
Axes of the slice: x: 2, y: 2, z: 4, core: 2. Of those that a mesh axis runs over, the one named last changes fastest.
Arguments:
- tokens: bfloat16 [1024, 2048], P(('sp', 'fs', 'tp')), may hold values from -6 to 6
- norm_gain: float32 [2048], replicated, may hold values from 0.1 to 1.9
- w_query: bfloat16 [2048, 2048], P(None, ('fs', 'tp')), may hold values from -0.9722718 to 0.9722718
- w_key: bfloat16 [2048, 512], P(None, 'fs'), may hold values from -0.77339804 to 0.77339804
- w_value: bfloat16 [2048, 512], P(None, 'fs'), may hold values from -0.125 to 0.125
- w_conv_value: bfloat16 [2048, 1024], P(None, ('fs', 'tp')), may hold values from -0.125 to 0.125
- w_conv_pre: bfloat16 [2048, 1024], P(None, ('fs', 'tp')), may hold values from -0.125 to 0.125
- w_conv_post: bfloat16 [2048, 1024], P(None, ('fs', 'tp')), may hold values from -0.125 to 0.125
- conv_taps: bfloat16 [3, 1024], replicated, may hold values from -3.5 to 3.5
- log_gate_cache: float32 [16, 1024], replicated, may hold values from -65 to 0, as said below
- w_out_conv: bfloat16 [1024, 2048], P(('fs', 'tp')), may hold values from -0.125 to 0.125
- w_out_attn: bfloat16 [2048, 2048], P(('fs', 'tp')), may hold values from -0.375 to 0.375
Outputs:
- mixed: bfloat16 [1024, 2048], P(('sp', 'fs', 'tp'))
Inputs may be any that keep to these rules, and one draw needn't show every extreme that they name: `log_gate_cache`: each row is a cumulative sum over positions of log forget gates, none of them positive.
All inputs are finite; a program needn't handle non-finite values.
Results may differ from a plain program's by a relative error of at most 0.014.
The roundings to bfloat16 on the way count: a program that leaves them out, or rounds other values in their place, can miss the bound.
Values may be sent and summed in bfloat16 or wider, within the bound.
No kernel may reach another device: no remote copies, remote signals or barrier semaphores. Data moves between devices by JAX's collectives and lax.ppermute only.
A program may use at most 64 MiB of HBM per device.

v0:
```python
import jax
import jax.numpy as jnp
from jax import lax
from jax.sharding import PartitionSpec as P

epsilon = 1e-06
masked_score = -1e30


def passed_along(block, axis, distance):
    devices = range(lax.axis_size(axis))
    route = [(i - distance, i) for i in devices if i - distance in devices]
    return lax.ppermute(block, axis, route)


def shards(
    tokens,
    norm_gain,
    w_query,
    w_key,
    w_value,
    w_conv_value,
    w_conv_pre,
    w_conv_post,
    conv_taps,
    log_gate_cache,
    w_out_conv,
    w_out_attn,
):
    float_rows = tokens.astype(jnp.float32)
    scaled = float_rows * lax.rsqrt(
        jnp.mean(float_rows * float_rows, axis=1, keepdims=True) + epsilon
    )
    normed_own = (scaled * norm_gain).astype(jnp.bfloat16)
    normed = lax.all_gather(normed_own, ("fs", "tp"), axis=0, tiled=True)
    block_rows = normed.shape[0]
    channels = w_conv_post.shape[1]
    head_dim = w_key.shape[1]
    local_heads = w_query.shape[1] // head_dim
    group = lax.axis_index(("fs", "tp"))
    local_weight = jnp.concatenate([w_conv_post, w_conv_pre, w_conv_value, w_query], axis=1)
    projected = jnp.dot(normed, local_weight, preferred_element_type=jnp.float32).astype(
        jnp.bfloat16
    )
    post_gate = projected[:, :channels]
    pre_gate = projected[:, channels : 2 * channels]
    conv_value = projected[:, 2 * channels : 3 * channels]
    queries = projected[:, 3 * channels :].reshape(block_rows, local_heads, head_dim)
    mixed_in = (pre_gate.astype(jnp.float32) * conv_value.astype(jnp.float32)).astype(jnp.bfloat16)
    kernel = conv_taps.shape[0]
    carried = passed_along(mixed_in[block_rows - (kernel - 1) :], "sp", 1)
    extended = jnp.concatenate([carried, mixed_in], axis=0).astype(jnp.float32)
    tap_weights = lax.dynamic_slice_in_dim(conv_taps, group * channels, channels, 1).astype(
        jnp.float32
    )
    conv_sum = tap_weights[0] * extended[0:block_rows]
    for offset in range(1, kernel):
        conv_sum = conv_sum + tap_weights[offset] * extended[offset : offset + block_rows]
    conv_out = (post_gate.astype(jnp.float32) * conv_sum).astype(jnp.bfloat16)
    core_index = lax.axis_index("tp")
    half_rows = block_rows // 2
    own_rows = lax.dynamic_slice_in_dim(normed, core_index * half_rows, half_rows, 0)
    pair_weight = jnp.concatenate([w_key, w_value], axis=1)
    pair_rows = jnp.dot(own_rows, pair_weight, preferred_element_type=jnp.float32).astype(
        jnp.bfloat16
    )
    key_half = pair_rows[:, :head_dim]
    value_half = pair_rows[:, head_dim:]
    head_gates = lax.dynamic_slice_in_dim(log_gate_cache, group * local_heads, local_heads, 0)
    anchor = lax.axis_index("sp") * block_rows
    gate_query = lax.dynamic_slice_in_dim(head_gates, anchor, block_rows, 1).T
    sequence_places = anchor + lax.iota(jnp.int32, block_rows)
    score_scale = head_dim ** (-0.5)

    def absorb(carried_state, key_block, value_block, sub_start):
        running_max, running_sum, weighted = carried_state
        sub_width = key_block.shape[0]
        scores = (
            jnp.einsum("qhd,kd->qhk", queries, key_block, preferred_element_type=jnp.float32)
            * score_scale
        )
        gate_keys = lax.dynamic_slice_in_dim(head_gates, sub_start, sub_width, 1)
        scores = scores + gate_query[:, :, None] - gate_keys[None, :, :]
        key_positions = sub_start + lax.iota(jnp.int32, sub_width)
        scores = jnp.where(
            sequence_places[:, None, None] >= key_positions[None, None, :], scores, masked_score
        )
        new_max = jnp.maximum(running_max, jnp.max(scores, axis=2))
        rescale = jnp.exp(running_max - new_max)
        weights = jnp.exp(scores - new_max[:, :, None])
        running_sum = running_sum * rescale + jnp.sum(weights, axis=2)
        weighted = weighted * rescale[:, :, None] + jnp.einsum(
            "qhk,kd->qhd",
            weights.astype(jnp.bfloat16),
            value_block,
            preferred_element_type=jnp.float32,
        )
        return (new_max, running_sum, weighted)

    initial = (
        jnp.full((block_rows, local_heads), masked_score, jnp.float32),
        jnp.zeros((block_rows, local_heads), jnp.float32),
        jnp.zeros((block_rows, local_heads, head_dim), jnp.float32),
    )
    key_piece = lax.all_gather(key_half, ("sp", "tp"), axis=0, tiled=True)
    value_piece = lax.all_gather(value_half, ("sp", "tp"), axis=0, tiled=True)
    key_count = key_piece.shape[0]
    sub_width = 512

    def sweep_keys(current):

        def absorb_step(running, step_index):
            sub_start = step_index * sub_width
            key_block = lax.dynamic_slice_in_dim(key_piece, sub_start, sub_width, 0)
            value_block = lax.dynamic_slice_in_dim(value_piece, sub_start, sub_width, 0)
            return (absorb(running, key_block, value_block, sub_start), None)

        result, unused = lax.scan(
            absorb_step, current, jnp.arange(key_count // sub_width, dtype=jnp.int32)
        )
        return result

    def keep_state(current):
        return current

    running_max, running_sum, weighted = lax.cond(
        jnp.int32(0) <= anchor + block_rows - 1, sweep_keys, keep_state, initial
    )
    attn_out = (
        (weighted / running_sum[:, :, None])
        .astype(jnp.bfloat16)
        .reshape(block_rows, local_heads * head_dim)
    )
    return lax.psum_scatter(
        (
            jnp.dot(conv_out, w_out_conv, preferred_element_type=jnp.float32)
            + jnp.dot(attn_out, w_out_attn, preferred_element_type=jnp.float32)
        ).astype(jnp.bfloat16),
        ("fs", "tp"),
        scatter_dimension=0,
        tiled=True,
    )


def solution(mesh):
    placed = (
        P(("sp", "fs", "tp"), None),
        P(),
        P(None, ("fs", "tp")),
        P(None, "fs"),
        P(None, "fs"),
        P(None, ("fs", "tp")),
        P(None, ("fs", "tp")),
        P(None, ("fs", "tp")),
        P(),
        P(),
        P(("fs", "tp"), None),
        P(("fs", "tp"), None),
    )
    return jax.shard_map(
        shards, mesh=mesh, in_specs=placed, out_specs=P(("sp", "fs", "tp"), None), check_vma=False
    )
```

profile of v0, /device:TPU:0, one launch (start us, length us, event | category | flops | bytes accessed | tf_op | source)
XLA Modules:
  0.0 123.4 jit_solution(4051089183334472649)
XLA Ops:
  6.5 1.2 fusion.32
  7.7 1.7 %fusion.34 = bf16[32,2048]{1,0:T(8,128)(2,1)} fusion(bf16[32,2048]{1,0:T(8,128)(2,1)} %param.16, f32[2048]{0:T(1024)} %param.17, f32[32]{0:T(128)S(1)} %add_rsqrt_fusion), kind=kLoop, calls=%fused_computation.47 | loop fusion | flops 262144 | bytes 270464 | tf_op jit(solution)/shard_map/convert_element_type | solution.py:34
  9.5 0.7 dynamic-slice_convert_fusion
  10.2 0.8 dynamic-slice_bitcast_fusion
  11.0 24.7 %all-gather.2.cloned.1.call-done = bf16[256,2048]{1,0:T(8,128)(2,1)} async-done(((bf16[32,2048]{1,0:T(8,128)(2,1)}), bf16[256,2048]{1,0:T(8,128)(2,1)}) %all-gather.2.cloned.1.call-update) | async-done | bytes 1048592 | tf_op jit(solution)/shard_map/all_gather | solution.py:35
  35.7 1.8 %convolution_convert_fusion = bf16[128,256]{1,0:T(8,128)(2,1)S(1)} fusion(bf16[2048,128]{1,0:T(8,128)(2,1)} %param.20, bf16[2048,128]{1,0:T(8,128)(2,1)} %param.19, bf16[256,2048]{1,0:T(8,128)(2,1)} %all-gather.2.cloned.1.call-done, s32[]{:T(128)S(6)} %select_n.27), kind=kOutput, calls=%fused_computation.38 | convolution fusion | flops 136347648 | bytes 1638404 | tf_op jit(solution)/shard_map/dot_general | solution.py:64
  37.5 2.2 %fusion.25 = bf16[256,640]{1,0:T(8,128)(2,1)S(1)} fusion(bf16[256,2048]{1,0:T(8,128)(2,1)S(1)} %copy-done.3, bf16[2048,256]{1,0:T(8,128)(2,1)S(1)} %copy-done.2, bf16[2048,128]{1,0:T(8,128)(2,1)S(1)} %copy-done.4, bf16[2048,128]{1,0:T(8,128)(2,1)} %param.22, bf16[2048,128]{1,0:T(8,128)(2,1)} %param.23), kind=kOutput, calls=%fused_computation.37 | convolution fusion | flops 681738240 | bytes 3997696 | tf_op jit(solution)/shard_map/dot_general | solution.py:42
  39.8 3.4 %collective-permute-start = (bf16[2,128]{1,0:T(2,128)(2,1)S(1)}, bf16[2,128]{1,0:T(2,128)(2,1)S(1)}, u32[]{:S(2)}, u32[]{:S(2)}) collective-permute-start(bf16[2,128]{1,0:T(2,128)(2,1)S(1)} %slice.57), channel_id=1, source_target_pairs={{0,8},{8,16},{16,24},{1,9},{9,17},{17,25},{2,10},{10,18},{18,26},{... | collective-permute-start | bytes 1544 | tf_op jit(solution)/shard_map/ppermute | solution.py:13
  43.2 14.2 %all_gather.11 = bf16[1024,128]{1,0:T(8,128)(2,1)S(1)} all-gather(bf16[128,128]{1,0:T(8,128)(2,1)S(1)} %get-tuple-element.195), channel_id=1, replica_groups=mesh['sp'=4,'fs'=4,'tp'=2] {'sp','tp'}, dimensions={0}, use_global_device_ids=true | all-gather | bytes 294912 | tf_op jit(solution)/shard_map/all_gather | solution.py:106
  57.4 14.2 %all_gather.10 = bf16[1024,128]{1,0:T(8,128)(2,1)S(1)} all-gather(bf16[128,128]{1,0:T(8,128)(2,1)S(1)} %get-tuple-element.196), channel_id=1, replica_groups=mesh['sp'=4,'fs'=4,'tp'=2] {'sp','tp'}, dimensions={0}, use_global_device_ids=true | all-gather | bytes 294912 | tf_op jit(solution)/shard_map/all_gather | solution.py:105
  71.6 7.9 %conditional.1 = (f32[256,2]{0,1:T(2,128)}, f32[256,2,128]{0,2,1:T(8,128)S(1)}) conditional(s32[]{:T(128)} %convert_element_type.55, () %tuple.19, (bf16[256,640]{1,0:T(8,128)(2,1)S(1)}, f32[16,1024]{1,0:T(8,128)}, s32[]{:T(128)}, s32[]{:T(128)}, s32[256]{0:T(256)S(1)}, /*index=5*/bf16[1024,128]{1,0:T(8,128)(2,1)S(1)}, f32[256,2]{0,1:T(2,128)S(1)}, ...), branch_computations={%region_1.0_spmd, %region_2.7_spmd} | conditional | flops 136908032 | bytes 6100363 | solution.py:126
  71.6 0.9 constant_dynamic-slice_fusion.1
  72.5 0.2 copy.16
  72.7 0.1 copy.15
  72.9 6.5 %while.18 = (s32[]{:T(128)}, f32[256,2]{0,1:T(2,128)S(1)}, f32[256,2]{0,1:T(2,128)}, f32[256,2,128]{2,0,1:T(8,128)S(1)}, s32[256]{0:T(256)S(1)}, /*index=5*/s32[...) while((s32[]{:T(128)}, f32[256,2]{0,1:T(2,128)S(1)}, ...), condition=%wide.region_6.6_spmd.clone, body=%wide.region_3.5_spmd.clone.sunk | while | flops 136907776 | bytes 4377835 | solution.py:118
  72.9 0.6 dynamic_slice.58
  74.1 0.1 broadcast_compare_fusion.2
  74.2 0.4 fusion.65
  74.6 0.2 fusion.67
  74.8 0.6 fusion.68
  75.4 0.4 convolution_add_fusion.3
  75.8 0.6 dynamic_slice.58
  77.0 0.1 broadcast_compare_fusion.2
  77.1 0.4 fusion.65
  77.5 0.2 fusion.67
  77.7 1.3 %fusion.68 = (f32[256,2]{0,1:T(2,128)}, f32[256,2]{0,1:T(2,128)S(1)}) fusion(f32[256,2]{0,1:T(2,128)S(1)} %fusion.67, f32[256,2]{0,1:T(2,128)} %get-tuple-element.292, pred[]{:T(512)S(6)} %compare.3, f32[256,2]{0,1:T(2,128)S(1)} %fusion.66, f32[256,2]{0,1:T(2,128)S(1)} %get-tuple-element.291), kind=kLoop, calls=%fused_computation.17.clone.1 | loop fusion | flops 2560 | bytes 12289 | tf_op jit(solution)/shard_map/cond/branch_1_fun/while/body/eval_jaxpr/add | solution.py:91
  79.0 0.4 convolution_add_fusion.3
  79.4 0.1 copy.20
  79.5 0.7 divide_convert_fusion
  80.3 0.4 fusion.39
  80.7 1.4 %fusion.24 = bf16[256,2048]{1,0:T(8,128)(2,1)} fusion(f32[256,2048]{1,0:T(8,128)S(1)} %fusion.39, bf16[256,256]{0,1:T(8,128)(2,1)S(1)} %bitcast.38, bf16[256,2048]{1,0:T(8,128)(2,1)S(1)} %copy-done), kind=kOutput, calls=%fused_computation.36 | convolution fusion | flops 269484032 | bytes 4325376 | tf_op jit(solution)/shard_map/dot_general | solution.py:137
  82.2 34.4 %reduce-scatter.2.cloned.1.call-done = bf16[32,2048]{1,0:T(8,128)(2,1)} async-done(((bf16[256,2048]{1,0:T(8,128)(2,1)}), bf16[32,2048]{1,0:T(8,128)(2,1)}) %reduce-scatter.2.cloned.1.call-update) | async-done | bytes 131088 | tf_op jit(solution)/shard_map/reduce_scatter | solution.py:134
  (36 shorter events, 0.2 us)
Async XLA Ops:
  6.5 74.2 %copy-start = (bf16[256,2048]{1,0:T(8,128)(2,1)S(1)}, bf16[256,2048]{1,0:T(8,128)(2,1)}, u32[]{:S(2)}) copy-start(bf16[256,2048]{1,0:T(8,128)(2,1)} %param.27) | copy-start | bytes 3145732
  6.5 31.0 %copy-start.2 = (bf16[2048,256]{1,0:T(8,128)(2,1)S(1)}, bf16[2048,256]{1,0:T(8,128)(2,1)}, u32[]{:S(2)}) copy-start(bf16[2048,256]{1,0:T(8,128)(2,1)} %param.18) | copy-start | bytes 3145732
  6.5 29.1 %all-gather.2.cloned.1.call-start = ((), (), s32[]{:S(2)}) async-start(), calls=%async_computation.1 | async-start | bytes 1179648 | tf_op jit(solution)/shard_map/all_gather | solution.py:35
  9.4 107.1 %reduce-scatter.2.cloned.1.call-start = ((), (), s32[]{:S(2)}) async-start(), calls=%async_computation.2 | async-start | bytes 1179648 | tf_op jit(solution)/shard_map/reduce_scatter | solution.py:134
  35.7 1.8 %copy-start.3 = (bf16[256,2048]{1,0:T(8,128)(2,1)S(1)}, bf16[256,2048]{1,0:T(8,128)(2,1)}, u32[]{:S(2)}) copy-start(bf16[256,2048]{1,0:T(8,128)(2,1)} %all-gather.2.cloned.1.call-done) | copy-start | bytes 3145732
  35.7 1.8 %copy-start.4 = (bf16[2048,128]{1,0:T(8,128)(2,1)S(1)}, bf16[2048,128]{1,0:T(8,128)(2,1)}, u32[]{:S(2)}) copy-start(bf16[2048,128]{1,0:T(8,128)(2,1)} %param.21) | copy-start | bytes 1572868
  39.8 40.4 %collective-permute-start = (bf16[2,128]{1,0:T(2,128)(2,1)S(1)}, bf16[2,128]{1,0:T(2,128)(2,1)S(1)}, u32[]{:S(2)}, u32[]{:S(2)}) collective-permute-start(bf16[2,128]{1,0:T(2,128)(2,1)S(1)} %slice.57), channel_id=1, source_target_pairs={{0,8},{8,16},{16,24},{1,9},{9,17},{17,25},{2,10},{10,18},{18,26},{... | collective-permute-start | bytes 1544 | tf_op jit(solution)/shard_map/ppermute | solution.py:13
  71.6 8.6 %copy-start.1 = (bf16[128,2048]{1,0:T(8,128)(2,1)S(1)}, bf16[128,2048]{1,0:T(8,128)(2,1)}, u32[]{:S(2)}) copy-start(bf16[128,2048]{1,0:T(8,128)(2,1)} %param.26) | copy-start | bytes 1572868
Sparse Core Ops, SparseCore 0:
  9.6 26.0 all-gather.1
  82.3 34.2 reduce-scatter.1
where the time goes:
time: 124 us; the launch traced here: 123 us
  waiting for transfers between devices  59.1 us (48%)
  blocking collectives  28.4 us (23%)
  between operations  13.5 us (11%)
  matrix products  7.38 us (6%)
  other arithmetic  6.81 us (5%)
  starting transfers between devices  3.44 us (3%)
  local copies, waits for them, and re-layouts  3.38 us (3%)
  loops' own time  1.32 us (1%)
    reduce_scatter x1, waiting for transfers between devices, shards(): lax.psum_scatter((jnp.dot(conv_out, w_out_conv, preferred_element_type=jn...  34.4 us
    all_gather x1, waiting for transfers between devices, shards(): normed = lax.all_gather(normed_own, ('fs', 'tp'), axis=0, tiled=True)  24.7 us
    all_gather x1, blocking collectives, shards(): value_piece = lax.all_gather(value_half, ('sp', 'tp'), axis=0, tiled=True)  14.2 us
    all_gather x1, blocking collectives, shards(): key_piece = lax.all_gather(key_half, ('sp', 'tp'), axis=0, tiled=True)  14.2 us
    ppermute x1, starting transfers between devices, passed_along(): return lax.ppermute(block, axis, route)  3.4 us
  transfers between devices with their start and end apart: 3, of which 2 were waited for; matrix products, arithmetic and copies ran while one was open for 7% of the time, Pallas kernels for 0%

commit v1 on v0

--- a/solution.py
+++ b/solution.py
@@ -1,10 +1,372 @@
+import functools
+import math
 import jax
 import jax.numpy as jnp
 from jax import lax
+from jax.experimental import pallas as pl
+from jax.experimental.pallas import tpu as pltpu
 from jax.sharding import PartitionSpec as P
 
 epsilon = 1e-06
 masked_score = -1e30
+log2e = math.log2(math.e)
+f32 = jnp.float32
+bf16 = jnp.bfloat16
+EDGE = 16
+RING = True
+NORM_WORK = 20000000000
+MASK_WORK = 2000000000
+SMALL_WORK = 2000000000
+
+
+def kernel_params(mib):
+    return pltpu.CompilerParams(vmem_limit_bytes=mib * 1024 * 1024)
+
+
+def shape_of(rows, cols, dtype=bf16):
+    return jax.ShapeDtypeStruct((rows, cols), dtype)
+
+
+def mask_kernel(out_ref):
+    query_place = lax.broadcasted_iota(jnp.int32, out_ref.shape, 0)
+    key_place = lax.broadcasted_iota(jnp.int32, out_ref.shape, 1)
+    out_ref[...] = jnp.where(query_place >= key_place, 0.0, masked_score)
+
+
+def norm_kernel(tokens_ref, gain_ref, out_ref):
+    rows = tokens_ref[...].astype(f32)
+    scale = lax.rsqrt(jnp.mean(rows * rows, axis=1, keepdims=True) + epsilon)
+    out_ref[...] = (rows * scale * gain_ref[...]).astype(bf16)
+
+
+def pair_kernel(n_fs, *refs):
+    chunks, (w_key, w_value, out_ref, rows_ref) = refs[:n_fs], refs[n_fs:]
+    step = chunks[0].shape[0]
+    f = lax.axis_index("fs")
+    for k in range(n_fs):
+        rows_ref[pl.ds(pl.multiple_of((f ^ k) * step, step), step)] = chunks[k][...]
+    weight = jnp.concatenate([w_key[...], w_value[...]], axis=1)
+    out_ref[...] = jnp.dot(rows_ref[...], weight, preferred_element_type=f32).astype(bf16)
+
+
+def join_kernel(n_fs, near_ref, far_ref, out_ref):
+    step = near_ref.shape[0] // n_fs
+    t = lax.axis_index("tp")
+    for lane, piece in ((t, near_ref), (1 - t, far_ref)):
+        for g in range(n_fs):
+            place = pl.ds(pl.multiple_of(g * 2 * step + lane * step, step), step)
+            out_ref[place] = piece[g * step : (g + 1) * step]
+
+
+def project_kernel(n_fs, *refs):
+    own, other = refs[:n_fs], refs[n_fs : 2 * n_fs]
+    w_query, w_post, w_pre, w_conv, near_ref = refs[2 * n_fs : 2 * n_fs + 5]
+    q_ref, post_ref, mixed_ref, rise_ref, rows_ref = refs[2 * n_fs + 5 :]
+    step = own[0].shape[0]
+    f = lax.axis_index("fs")
+    t = lax.axis_index("tp")
+    for k in range(n_fs):
+        place = (f ^ k) * (2 * step)
+        rows_ref[pl.ds(pl.multiple_of(place + t * step, step), step)] = own[k][...]
+        rows_ref[pl.ds(pl.multiple_of(place + (1 - t) * step, step), step)] = other[k][...]
+    rows = rows_ref[...]
+    weight = jnp.concatenate([w_pre[...], w_conv[...]], axis=1)
+    gated = jnp.dot(rows, weight, preferred_element_type=f32).astype(bf16).astype(f32)
+    channels = w_pre.shape[1]
+    mixed = (gated[:, :channels] * gated[:, channels:]).astype(bf16)
+    mixed_ref[...] = mixed
+    lane_rows = near_ref.shape[0]
+    rise_ref[:lane_rows] = near_ref[...]
+    rise_ref[lane_rows:, :channels] = mixed[mixed.shape[0] - EDGE :]
+    rise_ref[lane_rows:, channels:] = mixed[mixed.shape[0] - EDGE :]
+    q_ref[...] = jnp.dot(rows, w_query[...], preferred_element_type=f32).astype(bf16)
+    post_ref[...] = jnp.dot(rows, w_post[...], preferred_element_type=f32).astype(bf16)
+
+
+def conv_kernel(post_ref, mixed_ref, risen_ref, taps_ref, out_ref, extended_ref):
+    block_rows, channels = mixed_ref.shape
+    group = lax.axis_index("fs") * lax.axis_size("tp") + lax.axis_index("tp")
+    lanes = pl.ds(pl.multiple_of(group * channels, channels), channels)
+    edge = EDGE
+    taps = taps_ref.shape[0]
+    halo = risen_ref[risen_ref.shape[0] - edge :, :channels].astype(f32)
+    extended_ref[0:edge] = jnp.where(lax.axis_index("sp") > 0, halo, 0.0)
+    extended_ref[edge:] = mixed_ref[...].astype(f32)
+    tap_rows = taps_ref[:, lanes].astype(f32)
+    first = edge - (taps - 1)
+    conv_sum = tap_rows[0:1] * extended_ref[first : first + block_rows]
+    for i in range(1, taps):
+        conv_sum = conv_sum + tap_rows[i : i + 1] * extended_ref[first + i : first + i + block_rows]
+    out_ref[...] = (post_ref[...].astype(f32) * conv_sum).astype(bf16)
+
+
+def mixer_kernel(n_fs, parts, *refs):
+    q_ref, conv_in_ref, gates_ref, mask_ref, block_ref = refs[:5]
+    near_ref, far_ref, high_ref, low_ref = refs[5:9]
+    w_conv_ref, w_attn_ref, send_ref, keep_ref = refs[9:13]
+    key_ref, value_ref, gate_col_ref, tile_ref, conv_ref, sum_ref = refs[13:]
+    z = lax.axis_index("sp")
+    f = lax.axis_index("fs")
+    t = lax.axis_index("tp")
+    block_rows = conv_in_ref.shape[0]
+    step = block_rows // (2 * n_fs)
+    head_dim = block_ref.shape[1] // 2
+    heads = q_ref.shape[1] // head_dim
+    group = f * 2 + t
+    count = len(parts)
+    rows = count * 2 * step
+    for lane, piece in ((t, near_ref), (1 - t, far_ref)):
+        for g in range(n_fs):
+            place = pl.ds(pl.multiple_of(g * 2 * step + lane * step, step), step)
+            key_ref[place] = piece[g * step : (g + 1) * step, :head_dim]
+            value_ref[place] = piece[g * step : (g + 1) * step, head_dim:]
+    key_blocks = [block_ref[:, :head_dim], key_ref[...], high_ref[:, :head_dim], low_ref[:, :head_dim]]
+    value_blocks = [
+        block_ref[:, head_dim:],
+        value_ref[...],
+        high_ref[:, head_dim:],
+        low_ref[:, head_dim:],
+    ]
+    origins = [z, z - 1, z - 2 - t, z - 3 + t]
+    n_blocks = len(origins)
+
+    def gate_row(h, origin):
+        place = pl.multiple_of(jnp.maximum(origin, 0) * block_rows, block_rows)
+        return gates_ref[pl.ds(group * heads + h, 1), pl.ds(place, block_rows)] * log2e
+
+    for h in range(heads):
+        column = jnp.broadcast_to(gate_row(h, z), (8, block_rows)).T
+        gate_col_ref[h] = column
+    scale = head_dim ** (-0.5) * log2e
+    bases = [pl.multiple_of((f ^ part) * (2 * step), 2 * step) for part in parts]
+    for h in range(heads):
+        for i, base in enumerate(bases):
+            place = (h * count + i) * 2 * step
+            tile_ref[place : place + 2 * step] = q_ref[
+                pl.ds(base, 2 * step), h * head_dim : (h + 1) * head_dim
+            ]
+    mask = jnp.concatenate([mask_ref[pl.ds(base, 2 * step)] for base in bases], axis=0)
+    outs = []
+    for h in range(heads):
+        queries = tile_ref[h * rows : (h + 1) * rows]
+        gate_q = jnp.concatenate(
+            [gate_col_ref[h, pl.ds(base, 2 * step), 0:1] for base in bases], axis=0
+        )
+        scores = []
+        for k in range(n_blocks):
+            s = lax.dot_general(
+                queries,
+                key_blocks[k],
+                (((1,), (1,)), ((), ())),
+                preferred_element_type=f32,
+            )
+            gate_k = jnp.where(origins[k] >= 0, gate_row(h, origins[k]), -masked_score)
+            s = s * scale + gate_q - gate_k
+            if k == 0:
+                s = s + mask
+            scores.append(s)
+        top = scores[0]
+        for s in scores[1:]:
+            top = jnp.maximum(top, s)
+        top = jnp.max(top, axis=1, keepdims=True)
+        total = 0.0
+        weighted = 0.0
+        for k in range(n_blocks):
+            weight = jnp.exp2(scores[k] - top)
+            total = total + weight
+            weighted = weighted + jnp.dot(
+                weight.astype(bf16),
+                value_blocks[k],
+                preferred_element_type=f32,
+            )
+        den = jnp.sum(total, axis=1, keepdims=True)
+        outs.append((weighted / den).astype(bf16))
+    attn = jnp.concatenate(outs, axis=1)
+    for i, base in enumerate(bases):
+        conv_ref[i * 2 * step : (i + 1) * 2 * step] = conv_in_ref[pl.ds(base, 2 * step)]
+    out = jnp.dot(conv_ref[...], w_conv_ref[...], preferred_element_type=f32)
+    out = out + jnp.dot(attn, w_attn_ref[...], preferred_element_type=f32)
+    sum_ref[...] = out.astype(bf16)
+    for i in range(count):
+        place = i * 2 * step
+        mine = pl.ds(pl.multiple_of(place + t * step, step), step)
+        theirs = pl.ds(pl.multiple_of(place + (1 - t) * step, step), step)
+        keep_ref[i * step : (i + 1) * step] = sum_ref[mine]
+        send_ref[i * step : (i + 1) * step] = sum_ref[theirs]
+
+
+def pair_sum_kernel(keep_ref, got_ref, *outs):
+    step = outs[0].shape[0]
+    for i, out in enumerate(outs):
+        rows = slice(i * step, (i + 1) * step)
+        total = keep_ref[rows].astype(f32) + got_ref[rows].astype(f32)
+        out[...] = total.astype(out.dtype)
+
+
+def final_kernel(*refs):
+    total = refs[0][...].astype(f32)
+    for ref in refs[1:-1]:
+        total = total + ref[...].astype(f32)
+    refs[-1][...] = total.astype(bf16)
+
+
+def layer(
+    tokens,
+    norm_gain,
+    w_query,
+    w_key,
+    w_value,
+    w_conv_value,
+    w_conv_pre,
+    w_conv_post,
+    conv_taps,
+    log_gate_cache,
+    w_out_conv,
+    w_out_attn,
+):
+    n_sp, n_fs, n_tp = lax.axis_size("sp"), lax.axis_size("fs"), lax.axis_size("tp")
+    step, width = tokens.shape
+    lane_rows = n_fs * step
+    block_rows = n_tp * lane_rows
+    channels = w_conv_post.shape[1]
+    head_dim = w_key.shape[1]
+    heads = w_query.shape[1] // head_dim
+    partition = (tuple(range(n_fs - 1, -1, -1)),)
+
+    def swapped(x):
+        return lax.ppermute(x, "tp", [(0, 1), (1, 0)])
+
+    def crossed(x, k):
+        return lax.ppermute(x, "fs", [(i, i ^ k) for i in range(n_fs)])
+
+    def raised(x, shifts):
+        route = [
+            (i * n_tp + t, (i + shift) % n_sp * n_tp + t)
+            for t, shift in enumerate(shifts)
+            for i in range(n_sp)
+            if i + shift < n_sp or RING
+        ]
+        return lax.ppermute(x, ("sp", "tp"), route)
+
+    def call(kernel, out_shape, scratch, mib, *operands, in_specs=None, work=0):
+        extra = {} if in_specs is None else {"in_specs": in_specs}
+        if work:
+            extra["cost_estimate"] = pl.CostEstimate(
+                flops=work, transcendentals=0, bytes_accessed=0
+            )
+        return pl.pallas_call(
+            kernel,
+            out_shape=out_shape,
+            scratch_shapes=scratch,
+            compiler_params=kernel_params(mib),
+            **extra,
+        )(*operands)
+
+    mask = call(mask_kernel, shape_of(block_rows, block_rows, f32), [], 4, work=MASK_WORK)
+    normed = call(
+        norm_kernel,
+        shape_of(step, width),
+        [],
+        4,
+        tokens,
+        norm_gain.reshape(1, width),
+        work=NORM_WORK,
+    )
+    w_post, w_pre, w_conv = w_conv_post, w_conv_pre, w_conv_value
+    gates, taps = log_gate_cache, conv_taps
+    own = [normed] + [crossed(normed, k) for k in range(1, n_fs)]
+    other = [swapped(x) for x in own]
+    pair = call(
+        functools.partial(pair_kernel, n_fs),
+        shape_of(lane_rows, 2 * head_dim),
+        [pltpu.VMEM((lane_rows, width), bf16)],
+        8,
+        *own,
+        w_key,
+        w_value,
+        work=SMALL_WORK,
+    )
+    block = call(
+        functools.partial(join_kernel, n_fs),
+        shape_of(block_rows, 2 * head_dim),
+        [],
+        4,
+        pair,
+        swapped(pair),
+    )
+    high = raised(block, (2, 3))
+    queries, post, mixed, rise = call(
+        functools.partial(project_kernel, n_fs),
+        (
+            shape_of(block_rows, heads * head_dim),
+            shape_of(block_rows, channels),
+            shape_of(block_rows, channels),
+            shape_of(lane_rows + EDGE, 2 * head_dim),
+        ),
+        [pltpu.VMEM((block_rows, width), bf16)],
+        16,
+        *own,
+        *other,
+        w_query,
+        w_post,
+        w_pre,
+        w_conv,
+        pair,
+        work=SMALL_WORK,
+    )
+    near = raised(rise, (1, 1))
+    far = swapped(near)
+    low = swapped(high)
+    conv_out = call(
+        conv_kernel,
+        shape_of(block_rows, channels),
+        [pltpu.VMEM((block_rows + EDGE, channels), f32)],
+        4,
+        post,
+        mixed,
+        near,
+        taps,
+        work=SMALL_WORK,
+    )
+    sums = {}
+    for parts in partition:
+        count = len(parts)
+        send, keep = call(
+            functools.partial(mixer_kernel, n_fs, parts),
+            (shape_of(count * step, width), shape_of(count * step, width)),
+            [
+                pltpu.VMEM((block_rows, head_dim), bf16),
+                pltpu.VMEM((block_rows, head_dim), bf16),
+                pltpu.VMEM((heads, block_rows, 8), f32),
+                pltpu.VMEM((heads * count * 2 * step, head_dim), bf16),
+                pltpu.VMEM((count * 2 * step, channels), bf16),
+                pltpu.VMEM((count * 2 * step, width), bf16),
+            ],
+            16,
+            queries,
+            conv_out,
+            gates,
+            mask,
+            block,
+            near,
+            far,
+            high,
+            low,
+            w_out_conv,
+            w_out_attn,
+        )
+        got = swapped(send)
+        pieces = call(
+            pair_sum_kernel,
+            tuple(shape_of(step, width, f32 if k == 0 else bf16) for k in parts),
+            [],
+            8,
+            keep,
+            got,
+        )
+        for k, piece in zip(parts, pieces):
+            sums[k] = crossed(piece, k) if k else piece
+    return call(final_kernel, shape_of(step, width), [], 4, *[sums[k] for k in range(n_fs)])
 
 
 def passed_along(block, axis, distance):
@@ -115,7 +477,7 @@
             value_block = lax.dynamic_slice_in_dim(value_piece, sub_start, sub_width, 0)
             return (absorb(running, key_block, value_block, sub_start), None)
 
-        result, unused = lax.scan(
+        result, _ = lax.scan(
             absorb_step, current, jnp.arange(key_count // sub_width, dtype=jnp.int32)
         )
         return result
@@ -123,7 +485,7 @@
     def keep_state(current):
         return current
 
-    running_max, running_sum, weighted = lax.cond(
+    _, running_sum, weighted = lax.cond(
         jnp.int32(0) <= anchor + block_rows - 1, sweep_keys, keep_state, initial
     )
     attn_out = (
@@ -143,6 +505,7 @@
 
 
 def solution(mesh):
+    few = mesh.shape["sp"] == 4
     placed = (
         P(("sp", "fs", "tp"), None),
         P(),
@@ -158,5 +521,9 @@
         P(("fs", "tp"), None),
     )
     return jax.shard_map(
-        shards, mesh=mesh, in_specs=placed, out_specs=P(("sp", "fs", "tp"), None), check_vma=False
-    )
+        layer if few else shards,
+        mesh=mesh,
+        in_specs=placed,
+        out_specs=P(("sp", "fs", "tp"), None),
+        check_vma=False,
+    )

time: 124 us -> 41.7 us (0.34)
  waiting for transfers between devices: 59.1 us -> 21.2 us
  blocking collectives: 28.4 us -> 0 us
  between operations: 13.5 us -> 0.14 us
  starting transfers between devices: 3.44 us -> 13.8 us
  matrix products: 7.38 us -> 0 us
  other arithmetic: 6.81 us -> 0 us
  Pallas kernels: 0 us -> 4.58 us
  local copies, waits for them, and re-layouts: 3.38 us -> 1.77 us
  loops' own time: 1.32 us -> 0 us
    reduce_scatter x1 -> x0, waiting for transfers between devices: 34.4 us -> none  [shards(): lax.psum_scatter((jnp.dot(conv_out, w_out_conv, preferred_element_type=jn...]
    all_gather x2 -> x0, blocking collectives: 28.4 us -> none  [the longest x1 14.2 us: shards(): value_piece = lax.all_gather(value_half, ('sp', 'tp'), axis=0, tiled=True)]
    all_gather x1 -> x0, waiting for transfers between devices: 24.7 us -> none  [shards(): normed = lax.all_gather(normed_own, ('fs', 'tp'), axis=0, tiled=True)]
    ppermute x1 -> x16, waiting for transfers between devices: 0.01 us -> 21.2 us  [the longest x6 12.2 us: crossed(): return lax.ppermute(x, 'fs', [(i, i ^ k) for i in range(n_fs)])]
    ppermute x1 -> x16, starting transfers between devices: 3.4 us -> 13.8 us  [the longest x6 8.18 us: crossed(): return lax.ppermute(x, 'fs', [(i, i ^ k) for i in range(n_fs)])]
    dot_general x8 -> x0, matrix products: 7.38 us -> none  [the longest x1 2.22 us: shards(): jnp.dot(normed, local_weight, preferred_element_type=jnp.float32)]
    pallas_call x0 -> x9, Pallas kernels: none -> 4.58 us  [call(): pl.pallas_call(kernel, out_shape=out_shape, scratch_shapes=scratch, compi...]
    convert_element_type x5 -> x0, other arithmetic: 3.1 us -> none  [the longest x1 1.67 us: shards(): normed_own = (scaled * norm_gain).astype(jnp.bfloat16)]
  transfers between devices with their start and end apart: 3 -> 16, of which waited for: 2 -> 10; matrix products, arithmetic and copies ran while one was open for 7% -> 0% of each run, Pallas kernels for 0% -> 4%
where the time goes in v1:
time: 41.7 us; the launch traced here: 41.5 us
  waiting for transfers between devices  21.2 us (51%)
  starting transfers between devices  13.8 us (33%)
  Pallas kernels  4.58 us (11%)
  local copies, waits for them, and re-layouts  1.77 us (4%)
    ppermute x6, waiting for transfers between devices, crossed(): return lax.ppermute(x, 'fs', [(i, i ^ k) for i in range(n_fs)])  12.2 us
    ppermute x6, starting transfers between devices, crossed(): return lax.ppermute(x, 'fs', [(i, i ^ k) for i in range(n_fs)])  8.18 us
    ppermute x2, waiting for transfers between devices, raised(): return lax.ppermute(x, ('sp', 'tp'), route)  5.26 us
    pallas_call x9, Pallas kernels, call(): pl.pallas_call(kernel, out_shape=out_shape, scratch_shapes=scratch, compi...  4.58 us
    ppermute x2, starting transfers between devices, raised(): return lax.ppermute(x, ('sp', 'tp'), route)  4.46 us
    ppermute x8, waiting for transfers between devices, swapped(): return lax.ppermute(x, 'tp', [(0, 1), (1, 0)])  3.71 us
    unnamed x24, local copies, waits for them, and re-layouts  1.77 us
    ppermute x8, starting transfers between devices, swapped(): return lax.ppermute(x, 'tp', [(0, 1), (1, 0)])  1.21 us
  transfers between devices with their start and end apart: 16, of which 10 were waited for; matrix products, arithmetic and copies ran while one was open for 0% of the time, Pallas kernels for 4%

profile of v1, /device:TPU:0, one launch (start us, length us, event | category | flops | bytes accessed | tf_op | source)
XLA Modules:
  0.0 41.5 jit_solution(4618507208290522213)
XLA Ops:
  0.0 0.9 %copy-done.9 = bf16[32,2048]{1,0:T(8,128)(2,1)S(1)} copy-done((bf16[32,2048]{1,0:T(8,128)(2,1)S(1)}, bf16[32,2048]{1,0:T(8,128)(2,1)}, u32[]{:S(2)}) %copy-start.9) | copy-done | bytes 131096
  0.9 0.7 %copy-done.10 = f32[2048]{0:T(1024)S(1)} copy-done((f32[2048]{0:T(1024)S(1)}, f32[2048]{0:T(1024)}, u32[]{:S(2)}) %copy-start.10) | copy-done | bytes 8216
  1.6 0.1 shard_map.118.refs_0_
  1.8 4.0 %collective-permute-start.2 = (bf16[32,2048]{1,0:T(8,128)(2,1)S(1)}, bf16[32,2048]{1,0:T(8,128)(2,1)S(1)}, u32[]{:S(2)}, u32[]{:S(2)}) collective-permute-start(bf16[32,2048]{1,0:T(8,128)(2,1)S(1)} %shard_map.118.refs_0_), channel_id=1, source_target_pairs={{0,6},{2,4},{4,2},{6,0},{1,7},{3,5},{5,3},{7,1},{8,14},{10,12},{12... | collective-permute-start | bytes 393224 | tf_op jit(solution)/shard_map/ppermute | solution.py:240
  5.8 0.5 %collective-permute-start.1 = (bf16[32,2048]{1,0:T(8,128)(2,1)S(1)}, bf16[32,2048]{1,0:T(8,128)(2,1)S(1)}, u32[]{:S(2)}, u32[]{:S(2)}) collective-permute-start(bf16[32,2048]{1,0:T(8,128)(2,1)S(1)} %shard_map.118.refs_0_), channel_id=1, source_target_pairs={{0,4},{2,6},{4,0},{6,2},{1,5},{3,7},{5,1},{7,3},{8,12},{10,14},{12... | collective-permute-start | bytes 393224 | tf_op jit(solution)/shard_map/ppermute | solution.py:240
  6.3 0.1 collective-permute-start
  6.4 3.2 %collective-permute-done.2.refs_3_ = bf16[32,2048]{1,0:T(8,128)(2,1)S(1)} collective-permute-done((bf16[32,2048]{1,0:T(8,128)(2,1)S(1)}, bf16[32,2048]{1,0:T(8,128)(2,1)S(1)}, u32[]{:S(2)}, u32[]{:S(2)}) %collective-permute-start.2) | collective-permute-done | bytes 131104 | tf_op jit(solution)/shard_map/ppermute | solution.py:240
  9.7 2.4 %collective-permute-done.1.refs_2_ = bf16[32,2048]{1,0:T(8,128)(2,1)S(1)} collective-permute-done((bf16[32,2048]{1,0:T(8,128)(2,1)S(1)}, bf16[32,2048]{1,0:T(8,128)(2,1)S(1)}, u32[]{:S(2)}, u32[]{:S(2)}) %collective-permute-start.1) | collective-permute-done | bytes 131104 | tf_op jit(solution)/shard_map/ppermute | solution.py:240
  12.1 0.2 collective-permute-done.refs_1_
  12.3 0.3 collective-permute-start.4
  12.6 0.3 shard_map.119.refs_12_.near_ref
  12.9 0.3 collective-permute-start.8
  13.2 1.0 %collective-permute-done.8.far_ref = bf16[128,256]{1,0:T(8,128)(2,1)S(1)} collective-permute-done((bf16[128,256]{1,0:T(8,128)(2,1)S(1)}, bf16[128,256]{1,0:T(8,128)(2,1)S(1)}, u32[]{:S(2)}, u32[]{:S(2)}) %collective-permute-start.8) | collective-permute-done | bytes 65568 | tf_op jit(solution)/shard_map/ppermute | solution.py:237
  14.3 2.8 %collective-permute-start.10 = (bf16[256,256]{1,0:T(8,128)(2,1)S(1)}, bf16[256,256]{1,0:T(8,128)(2,1)S(1)}, u32[]{:S(2)}, u32[]{:S(2)}) collective-permute-start(bf16[256,256]{1,0:T(8,128)(2,1)S(1)} %shard_map.123.refs_4_), channel_id=1, source_target_pairs={{0,16},{8,24},{16,0},{24,8},{1,25},{9,1},{17,9},{25,17},{2,18},{10... | collective-permute-start | bytes 393224 | tf_op jit(solution)/shard_map/ppermute | solution.py:249
  17.2 1.0 %shard_map.120 = (bf16[256,256]{1,0:T(8,128)(2,1)S(1)}, bf16[256,128]{1,0:T(8,128)(2,1)S(1)}, bf16[256,128]{1,0:T(8,128)(2,1)S(1)}, bf16[144,256]{1,0:T(8,128)(2,1)S(1)}) custom-call(bf16[32,2048]{1,0:T(8,128)(2,1)S(1)} %shard_map.118.refs_0_, bf16[32,2048]{1,0:T(8,128)(2,1)S(1)} %collective-permute-done.refs_1_, ...), custom_call_target="tpu_custom_call" | custom-call | flops 2000000000 | tf_op jit(solution)/shard_map/pallas_call | solution.py:257
  18.2 1.6 %collective-permute-start.7 = (bf16[144,256]{1,0:T(8,128)(2,1)S(1)}, bf16[144,256]{1,0:T(8,128)(2,1)S(1)}, u32[]{:S(2)}, u32[]{:S(2)}) collective-permute-start(bf16[144,256]{1,0:T(8,128)(2,1)S(1)} %get-tuple-element.18), channel_id=1, source_target_pairs={{0,8},{8,16},{16,24},{24,0},{1,9},{9,17},{17,25},{25,1},{2,10},{10... | collective-permute-start | bytes 221192 | tf_op jit(solution)/shard_map/ppermute | solution.py:249
  19.9 2.6 %collective-permute-done.10.refs_7_ = bf16[256,256]{1,0:T(8,128)(2,1)S(1)} collective-permute-done((bf16[256,256]{1,0:T(8,128)(2,1)S(1)}, bf16[256,256]{1,0:T(8,128)(2,1)S(1)}, u32[]{:S(2)}, u32[]{:S(2)}) %collective-permute-start.10) | collective-permute-done | bytes 131104 | tf_op jit(solution)/shard_map/ppermute | solution.py:249
  22.5 2.6 %collective-permute-done.7.risen_ref.refs_5_ = bf16[144,256]{1,0:T(8,128)(2,1)S(1)} collective-permute-done((bf16[144,256]{1,0:T(8,128)(2,1)S(1)}, bf16[144,256]{1,0:T(8,128)(2,1)S(1)}, u32[]{:S(2)}, u32[]{:S(2)}) %collective-permute-start.7) | collective-permute-done | bytes 73760 | tf_op jit(solution)/shard_map/ppermute | solution.py:249
  25.1 0.0 collective-permute-start.9
  25.2 0.1 shard_map.121.refs_1_
  25.3 1.2 %collective-permute-done.9.refs_6_ = bf16[144,256]{1,0:T(8,128)(2,1)S(1)} collective-permute-done((bf16[144,256]{1,0:T(8,128)(2,1)S(1)}, bf16[144,256]{1,0:T(8,128)(2,1)S(1)}, u32[]{:S(2)}, u32[]{:S(2)}) %collective-permute-start.9) | collective-permute-done | bytes 73760 | tf_op jit(solution)/shard_map/ppermute | solution.py:237
  26.4 0.1 copy-done.1
  26.5 2.1 %shard_map.124 = (bf16[128,2048]{1,0:T(8,128)(2,1)S(1)}, bf16[128,2048]{1,0:T(8,128)(2,1)S(1)}) custom-call(bf16[256,256]{1,0:T(8,128)(2,1)S(1)} %get-tuple-element.15.refs_0_, bf16[256,128]{1,0:T(8,128)(2,1)S(1)} %shard_map.121.refs_1_, f32[16,1024]{1,0:T(8,128)S(1)} %copy-done.2, f32[256,256]{1,0:T(8,128)S(1)} %shard_map.122.refs_3_, ...), custom_call_target="tpu_custom_call" | custom-call | tf_op jit(solution)/shard_map/pallas_call | solution.py:257
  28.7 0.6 %collective-permute-start.12 = (bf16[128,2048]{1,0:T(8,128)(2,1)S(1)}, bf16[128,2048]{1,0:T(8,128)(2,1)S(1)}, u32[]{:S(2)}, u32[]{:S(2)}) collective-permute-start(bf16[128,2048]{1,0:T(8,128)(2,1)S(1)} %get-tuple-element.20), channel_id=1, source_target_pairs={{0,1},{1,0},{2,3},{3,2},{4,5},{5,4},{6,7},{7,6},{8,9},{9,8},{10,11... | collective-permute-start | bytes 1572872 | tf_op jit(solution)/shard_map/ppermute | solution.py:237
  29.3 1.5 %collective-permute-done.12.got_ref = bf16[128,2048]{1,0:T(8,128)(2,1)S(1)} collective-permute-done((bf16[128,2048]{1,0:T(8,128)(2,1)S(1)}, bf16[128,2048]{1,0:T(8,128)(2,1)S(1)}, u32[]{:S(2)}, u32[]{:S(2)}) %collective-permute-start.12) | collective-permute-done | bytes 524320 | tf_op jit(solution)/shard_map/ppermute | solution.py:237
  30.8 0.1 shard_map.125
  30.9 1.6 %collective-permute-start.13 = (bf16[32,2048]{1,0:T(8,128)(2,1)S(1)}, bf16[32,2048]{1,0:T(8,128)(2,1)S(1)}, u32[]{:S(2)}, u32[]{:S(2)}) collective-permute-start(bf16[32,2048]{1,0:T(8,128)(2,1)S(1)} %get-tuple-element.22), channel_id=1, source_target_pairs={{0,2},{2,0},{4,6},{6,4},{1,3},{3,1},{5,7},{7,5},{8,10},{10,8},{12,... | collective-permute-start | bytes 393224 | tf_op jit(solution)/shard_map/ppermute | solution.py:240
  32.5 0.8 %collective-permute-start.14 = (bf16[32,2048]{1,0:T(8,128)(2,1)S(1)}, bf16[32,2048]{1,0:T(8,128)(2,1)S(1)}, u32[]{:S(2)}, u32[]{:S(2)}) collective-permute-start(bf16[32,2048]{1,0:T(8,128)(2,1)S(1)} %get-tuple-element.23), channel_id=1, source_target_pairs={{0,4},{2,6},{4,0},{6,2},{1,5},{3,7},{5,1},{7,3},{8,12},{10,14},{12... | collective-permute-start | bytes 393224 | tf_op jit(solution)/shard_map/ppermute | solution.py:240
  33.3 1.2 %collective-permute-start.15 = (bf16[32,2048]{1,0:T(8,128)(2,1)S(1)}, bf16[32,2048]{1,0:T(8,128)(2,1)S(1)}, u32[]{:S(2)}, u32[]{:S(2)}) collective-permute-start(bf16[32,2048]{1,0:T(8,128)(2,1)S(1)} %get-tuple-element.24), channel_id=1, source_target_pairs={{0,6},{2,4},{4,2},{6,0},{1,7},{3,5},{5,3},{7,1},{8,14},{10,12},{12... | collective-permute-start | bytes 393224 | tf_op jit(solution)/shard_map/ppermute | solution.py:240
  34.5 2.7 %collective-permute-done.13.refs_1_ = bf16[32,2048]{1,0:T(8,128)(2,1)S(1)} collective-permute-done((bf16[32,2048]{1,0:T(8,128)(2,1)S(1)}, bf16[32,2048]{1,0:T(8,128)(2,1)S(1)}, u32[]{:S(2)}, u32[]{:S(2)}) %collective-permute-start.13) | collective-permute-done | bytes 131104 | tf_op jit(solution)/shard_map/ppermute | solution.py:240
  37.2 3.6 %collective-permute-done.14.refs_2_ = bf16[32,2048]{1,0:T(8,128)(2,1)S(1)} collective-permute-done((bf16[32,2048]{1,0:T(8,128)(2,1)S(1)}, bf16[32,2048]{1,0:T(8,128)(2,1)S(1)}, u32[]{:S(2)}, u32[]{:S(2)}) %collective-permute-start.14) | collective-permute-done | bytes 131104 | tf_op jit(solution)/shard_map/ppermute | solution.py:240
  40.8 0.7 %shard_map.126 = bf16[32,2048]{1,0:T(8,128)(2,1)} custom-call(f32[32,2048]{1,0:T(8,128)S(1)} %get-tuple-element.21.refs_0_, bf16[32,2048]{1,0:T(8,128)(2,1)S(1)} %collective-permute-done.13.refs_1_, bf16[32,2048]{1,0:T(8,128)(2,1)S(1)} %collective-permute-done.14.refs_2_, bf16[32,2048]{1,0:T(8,128)(2,1)S(1)} %collective-permute-done.15.refs_3_), custom_call_target="tpu_custom_call" | custom-call | tf_op jit(solution)/shard_map/pallas_call | solution.py:257
  (33 shorter events, 0.1 us)
Async XLA Ops:
  0.0 0.9 %copy-start.9 = (bf16[32,2048]{1,0:T(8,128)(2,1)S(1)}, bf16[32,2048]{1,0:T(8,128)(2,1)}, u32[]{:S(2)}) copy-start(bf16[32,2048]{1,0:T(8,128)(2,1)} %tokens_ref.1) | copy-start | bytes 393220
  0.9 0.7 %copy-start.10 = (f32[2048]{0:T(1024)S(1)}, f32[2048]{0:T(1024)}, u32[]{:S(2)}) copy-start(f32[2048]{0:T(1024)} %param.13) | copy-start | bytes 24580
  1.6 11.0 %copy-start.4 = (bf16[2048,128]{1,0:T(8,128)(2,1)S(1)}, bf16[2048,128]{1,0:T(8,128)(2,1)}, u32[]{:S(2)}) copy-start(bf16[2048,128]{1,0:T(8,128)(2,1)} %refs_4_.1) | copy-start | bytes 1572868
  1.6 11.0 %copy-start.5 = (bf16[2048,128]{1,0:T(8,128)(2,1)S(1)}, bf16[2048,128]{1,0:T(8,128)(2,1)}, u32[]{:S(2)}) copy-start(bf16[2048,128]{1,0:T(8,128)(2,1)} %refs_5_.1) | copy-start | bytes 1572868
  1.7 15.4 %copy-start.3 = (bf16[2048,256]{1,0:T(8,128)(2,1)S(1)}, bf16[2048,256]{1,0:T(8,128)(2,1)}, u32[]{:S(2)}) copy-start(bf16[2048,256]{1,0:T(8,128)(2,1)} %refs_8_.1) | copy-start | bytes 3145732
  1.8 15.4 %copy-start.6 = (bf16[2048,128]{1,0:T(8,128)(2,1)S(1)}, bf16[2048,128]{1,0:T(8,128)(2,1)}, u32[]{:S(2)}) copy-start(bf16[2048,128]{1,0:T(8,128)(2,1)} %refs_9_.2) | copy-start | bytes 1572868
  1.8 15.4 %copy-start.7 = (bf16[2048,128]{1,0:T(8,128)(2,1)S(1)}, bf16[2048,128]{1,0:T(8,128)(2,1)}, u32[]{:S(2)}) copy-start(bf16[2048,128]{1,0:T(8,128)(2,1)} %refs_10_.2) | copy-start | bytes 1572868
  1.8 15.4 %copy-start.8 = (bf16[2048,128]{1,0:T(8,128)(2,1)S(1)}, bf16[2048,128]{1,0:T(8,128)(2,1)}, u32[]{:S(2)}) copy-start(bf16[2048,128]{1,0:T(8,128)(2,1)} %refs_11_.1) | copy-start | bytes 1572868
  1.8 7.9 %collective-permute-start.2 = (bf16[32,2048]{1,0:T(8,128)(2,1)S(1)}, bf16[32,2048]{1,0:T(8,128)(2,1)S(1)}, u32[]{:S(2)}, u32[]{:S(2)}) collective-permute-start(bf16[32,2048]{1,0:T(8,128)(2,1)S(1)} %shard_map.118.refs_0_), channel_id=1, source_target_pairs={{0,6},{2,4},{4,2},{6,0},{1,7},{3,5},{5,3},{7,1},{8,14},{10,12},{12... | collective-permute-start | bytes 393224 | tf_op jit(solution)/shard_map/ppermute | solution.py:240
  5.8 6.3 %collective-permute-start.1 = (bf16[32,2048]{1,0:T(8,128)(2,1)S(1)}, bf16[32,2048]{1,0:T(8,128)(2,1)S(1)}, u32[]{:S(2)}, u32[]{:S(2)}) collective-permute-start(bf16[32,2048]{1,0:T(8,128)(2,1)S(1)} %shard_map.118.refs_0_), channel_id=1, source_target_pairs={{0,4},{2,6},{4,0},{6,2},{1,5},{3,7},{5,1},{7,3},{8,12},{10,14},{12... | collective-permute-start | bytes 393224 | tf_op jit(solution)/shard_map/ppermute | solution.py:240
  6.3 6.0 %collective-permute-start = (bf16[32,2048]{1,0:T(8,128)(2,1)S(1)}, bf16[32,2048]{1,0:T(8,128)(2,1)S(1)}, u32[]{:S(2)}, u32[]{:S(2)}) collective-permute-start(bf16[32,2048]{1,0:T(8,128)(2,1)S(1)} %shard_map.118.refs_0_), channel_id=1, source_target_pairs={{0,2},{2,0},{4,6},{6,4},{1,3},{3,1},{5,7},{7,5},{8,10},{10,8},{12,... | collective-permute-start | bytes 393224 | tf_op jit(solution)/shard_map/ppermute | solution.py:240
  6.4 10.7 %collective-permute-start.3 = (bf16[32,2048]{1,0:T(8,128)(2,1)S(1)}, bf16[32,2048]{1,0:T(8,128)(2,1)S(1)}, u32[]{:S(2)}, u32[]{:S(2)}) collective-permute-start(bf16[32,2048]{1,0:T(8,128)(2,1)S(1)} %shard_map.118.refs_0_), channel_id=1, source_target_pairs={{0,1},{1,0},{2,3},{3,2},{4,5},{5,4},{6,7},{7,6},{8,9},{9,8},{10,11... | collective-permute-start | bytes 393224 | tf_op jit(solution)/shard_map/ppermute | solution.py:237
  9.7 7.4 %collective-permute-start.6 = (bf16[32,2048]{1,0:T(8,128)(2,1)S(1)}, bf16[32,2048]{1,0:T(8,128)(2,1)S(1)}, u32[]{:S(2)}, u32[]{:S(2)}) collective-permute-start(bf16[32,2048]{1,0:T(8,128)(2,1)S(1)} %collective-permute-done.2.refs_3_), channel_id=1, source_target_pairs={{0,1},{1,0},{2,3},{3,2},{4,5},{5,4},{6,7},{7,6},{8,9},{9,8},{10,11... | collective-permute-start | bytes 393224 | tf_op jit(solution)/shard_map/ppermute | solution.py:237
  12.1 5.0 %collective-permute-start.5 = (bf16[32,2048]{1,0:T(8,128)(2,1)S(1)}, bf16[32,2048]{1,0:T(8,128)(2,1)S(1)}, u32[]{:S(2)}, u32[]{:S(2)}) collective-permute-start(bf16[32,2048]{1,0:T(8,128)(2,1)S(1)} %collective-permute-done.1.refs_2_), channel_id=1, source_target_pairs={{0,1},{1,0},{2,3},{3,2},{4,5},{5,4},{6,7},{7,6},{8,9},{9,8},{10,11... | collective-permute-start | bytes 393224 | tf_op jit(solution)/shard_map/ppermute | solution.py:237
  12.3 4.8 %collective-permute-start.4 = (bf16[32,2048]{1,0:T(8,128)(2,1)S(1)}, bf16[32,2048]{1,0:T(8,128)(2,1)S(1)}, u32[]{:S(2)}, u32[]{:S(2)}) collective-permute-start(bf16[32,2048]{1,0:T(8,128)(2,1)S(1)} %collective-permute-done.refs_1_), channel_id=1, source_target_pairs={{0,1},{1,0},{2,3},{3,2},{4,5},{5,4},{6,7},{7,6},{8,9},{9,8},{10,11... | collective-permute-start | bytes 393224 | tf_op jit(solution)/shard_map/ppermute | solution.py:237
  12.9 1.3 %collective-permute-start.8 = (bf16[128,256]{1,0:T(8,128)(2,1)S(1)}, bf16[128,256]{1,0:T(8,128)(2,1)S(1)}, u32[]{:S(2)}, u32[]{:S(2)}) collective-permute-start(bf16[128,256]{1,0:T(8,128)(2,1)S(1)} %shard_map.119.refs_12_.near_ref), channel_id=1, source_target_pairs={{0,1},{1,0},{2,3},{3,2},{4,5},{5,4},{6,7},{7,6},{8,9},{9,8},{10,11... | collective-permute-start | bytes 196616 | tf_op jit(solution)/shard_map/ppermute | solution.py:237
  14.3 8.2 %collective-permute-start.10 = (bf16[256,256]{1,0:T(8,128)(2,1)S(1)}, bf16[256,256]{1,0:T(8,128)(2,1)S(1)}, u32[]{:S(2)}, u32[]{:S(2)}) collective-permute-start(bf16[256,256]{1,0:T(8,128)(2,1)S(1)} %shard_map.123.refs_4_), channel_id=1, source_target_pairs={{0,16},{8,24},{16,0},{24,8},{1,25},{9,1},{17,9},{25,17},{2,18},{10... | collective-permute-start | bytes 393224 | tf_op jit(solution)/shard_map/ppermute | solution.py:249
  18.2 7.0 %copy-start.11 = (bf16[3,1024]{1,0:T(4,128)(2,1)S(1)}, bf16[3,1024]{1,0:T(4,128)(2,1)}, u32[]{:S(2)}) copy-start(bf16[3,1024]{1,0:T(4,128)(2,1)} %taps_ref.1) | copy-start | bytes 18436
  18.2 6.9 %collective-permute-start.7 = (bf16[144,256]{1,0:T(8,128)(2,1)S(1)}, bf16[144,256]{1,0:T(8,128)(2,1)S(1)}, u32[]{:S(2)}, u32[]{:S(2)}) collective-permute-start(bf16[144,256]{1,0:T(8,128)(2,1)S(1)} %get-tuple-element.18), channel_id=1, source_target_pairs={{0,8},{8,16},{16,24},{24,0},{1,9},{9,17},{17,25},{25,1},{2,10},{10... | collective-permute-start | bytes 221192 | tf_op jit(solution)/shard_map/ppermute | solution.py:249
  22.5 3.9 %collective-permute-start.11 = (bf16[256,256]{1,0:T(8,128)(2,1)S(1)}, bf16[256,256]{1,0:T(8,128)(2,1)S(1)}, u32[]{:S(2)}, u32[]{:S(2)}) collective-permute-start(bf16[256,256]{1,0:T(8,128)(2,1)S(1)} %collective-permute-done.10.refs_7_), channel_id=1, source_target_pairs={{0,1},{1,0},{2,3},{3,2},{4,5},{5,4},{6,7},{7,6},{8,9},{9,8},{10,11... | collective-permute-start | bytes 393224 | tf_op jit(solution)/shard_map/ppermute | solution.py:237
  25.1 1.3 %collective-permute-start.9 = (bf16[144,256]{1,0:T(8,128)(2,1)S(1)}, bf16[144,256]{1,0:T(8,128)(2,1)S(1)}, u32[]{:S(2)}, u32[]{:S(2)}) collective-permute-start(bf16[144,256]{1,0:T(8,128)(2,1)S(1)} %collective-permute-done.7.risen_ref.refs_5_), channel_id=1, source_target_pairs={{0,1},{1,0},{2,3},{3,2},{4,5},{5,4},{6,7},{7,6},{8,9},{9,8},{10,11... | collective-permute-start | bytes 221192 | tf_op jit(solution)/shard_map/ppermute | solution.py:237
  25.2 1.2 %copy-start = (bf16[256,2048]{1,0:T(8,128)(2,1)S(1)}, bf16[256,2048]{1,0:T(8,128)(2,1)}, u32[]{:S(2)}) copy-start(bf16[256,2048]{1,0:T(8,128)(2,1)} %refs_10_.3) | copy-start | bytes 3145732
  25.2 1.4 %copy-start.1 = (bf16[128,2048]{1,0:T(8,128)(2,1)S(1)}, bf16[128,2048]{1,0:T(8,128)(2,1)}, u32[]{:S(2)}) copy-start(bf16[128,2048]{1,0:T(8,128)(2,1)} %refs_9_.3) | copy-start | bytes 1572868
  25.2 1.4 %copy-start.2 = (f32[16,1024]{1,0:T(8,128)S(1)}, f32[16,1024]{1,0:T(8,128)}, u32[]{:S(2)}) copy-start(f32[16,1024]{1,0:T(8,128)} %refs_2_.1) | copy-start | bytes 196612
  28.7 2.1 %collective-permute-start.12 = (bf16[128,2048]{1,0:T(8,128)(2,1)S(1)}, bf16[128,2048]{1,0:T(8,128)(2,1)S(1)}, u32[]{:S(2)}, u32[]{:S(2)}) collective-permute-start(bf16[128,2048]{1,0:T(8,128)(2,1)S(1)} %get-tuple-element.20), channel_id=1, source_target_pairs={{0,1},{1,0},{2,3},{3,2},{4,5},{5,4},{6,7},{7,6},{8,9},{9,8},{10,11... | collective-permute-start | bytes 1572872 | tf_op jit(solution)/shard_map/ppermute | solution.py:237
  30.9 6.3 %collective-permute-start.13 = (bf16[32,2048]{1,0:T(8,128)(2,1)S(1)}, bf16[32,2048]{1,0:T(8,128)(2,1)S(1)}, u32[]{:S(2)}, u32[]{:S(2)}) collective-permute-start(bf16[32,2048]{1,0:T(8,128)(2,1)S(1)} %get-tuple-element.22), channel_id=1, source_target_pairs={{0,2},{2,0},{4,6},{6,4},{1,3},{3,1},{5,7},{7,5},{8,10},{10,8},{12,... | collective-permute-start | bytes 393224 | tf_op jit(solution)/shard_map/ppermute | solution.py:240
  32.5 8.3 %collective-permute-start.14 = (bf16[32,2048]{1,0:T(8,128)(2,1)S(1)}, bf16[32,2048]{1,0:T(8,128)(2,1)S(1)}, u32[]{:S(2)}, u32[]{:S(2)}) collective-permute-start(bf16[32,2048]{1,0:T(8,128)(2,1)S(1)} %get-tuple-element.23), channel_id=1, source_target_pairs={{0,4},{2,6},{4,0},{6,2},{1,5},{3,7},{5,1},{7,3},{8,12},{10,14},{12... | collective-permute-start | bytes 393224 | tf_op jit(solution)/shard_map/ppermute | solution.py:240
  33.3 7.5 %collective-permute-start.15 = (bf16[32,2048]{1,0:T(8,128)(2,1)S(1)}, bf16[32,2048]{1,0:T(8,128)(2,1)S(1)}, u32[]{:S(2)}, u32[]{:S(2)}) collective-permute-start(bf16[32,2048]{1,0:T(8,128)(2,1)S(1)} %get-tuple-element.24), channel_id=1, source_target_pairs={{0,6},{2,4},{4,2},{6,0},{1,7},{3,5},{5,3},{7,1},{8,14},{10,12},{12... | collective-permute-start | bytes 393224 | tf_op jit(solution)/shard_map/ppermute | solution.py:240

commit v2 on v1

--- a/solution.py
+++ b/solution.py
@@ -49,150 +49,168 @@
     out_ref[...] = jnp.dot(rows_ref[...], weight, preferred_element_type=f32).astype(bf16)
 
 
-def join_kernel(n_fs, near_ref, far_ref, out_ref):
-    step = near_ref.shape[0] // n_fs
+def place_pairs(pieces, key_ref, value_ref):
+    head_dim = key_ref.shape[1]
     t = lax.axis_index("tp")
-    for lane, piece in ((t, near_ref), (1 - t, far_ref)):
-        for g in range(n_fs):
-            place = pl.ds(pl.multiple_of(g * 2 * step + lane * step, step), step)
-            out_ref[place] = piece[g * step : (g + 1) * step]
+    n_fs = lax.axis_size("fs")
+    step = key_ref.shape[0] // (2 * n_fs * len(pieces))
+    for k, (near, far) in enumerate(pieces):
+        for lane, piece in ((t, near), (1 - t, far)):
+            for g in range(n_fs):
+                place = (k * n_fs + g) * 2 * step + lane * step
+                place = pl.ds(pl.multiple_of(place, step), step)
+                key_ref[place] = piece[g * step : (g + 1) * step, :head_dim]
+                value_ref[place] = piece[g * step : (g + 1) * step, head_dim:]
+
+
+def gate_row(gates_ref, h, heads, origin, block_rows):
+    group = lax.axis_index("fs") * lax.axis_size("tp") + lax.axis_index("tp")
+    place = pl.multiple_of(jnp.maximum(origin, 0) * block_rows, block_rows)
+    return gates_ref[pl.ds(group * heads + h, 1), pl.ds(place, block_rows)] * log2e
+
+
+def score(queries, keys, gate_q, gate_k, origin):
+    scale = queries.shape[1] ** (-0.5) * log2e
+    s = lax.dot_general(
+        queries, keys, (((1,), (1,)), ((), ())), preferred_element_type=f32
+    )
+    return s * scale + gate_q - jnp.where(origin >= 0, gate_k, -masked_score)
+
+
+def early_kernel(*refs):
+    q_ref, gates_ref, mask_ref = refs[:3]
+    acc_ref, stat_ref, column_ref, key_ref, value_ref, natural_ref = refs[-6:]
+    halves = refs[3:-6]
+    place_pairs(tuple(zip(halves[::2], halves[1::2])), key_ref, value_ref)
+    z = lax.axis_index("sp")
+    block_rows = q_ref.shape[0]
+    head_dim = key_ref.shape[1]
+    heads = q_ref.shape[1] // head_dim
+    origins = [z] + [z - k for k in range(2, len(halves) // 2 + 1)]
+    n_fs = lax.axis_size("fs")
+    step = block_rows // (2 * n_fs)
+    places = row_places(n_fs, step)
+    for h in range(heads):
+        row = gate_row(gates_ref, h, heads, z, block_rows)
+        natural_ref[...] = jnp.broadcast_to(row, (8, block_rows)).T
+        for i, place in enumerate(places):
+            column_ref[h, i * step : (i + 1) * step] = natural_ref[pl.ds(place, step)]
+    tile = block_rows // 2
+    masks = []
+    for i in range(0, 2 * n_fs, n_fs):
+        piece = [mask_ref[pl.ds(place, step)] for place in places[i : i + n_fs]]
+        masks.append(jnp.concatenate(piece, axis=0))
+    for h in range(heads):
+        for i in range(0, block_rows, tile):
+            queries = q_ref[i : i + tile, h * head_dim : (h + 1) * head_dim]
+            gate_q = column_ref[h, i : i + tile, 0:1]
+            scores = []
+            for k, origin in enumerate(origins):
+                gate_k = gate_row(gates_ref, h, heads, origin, block_rows)
+                keys = key_ref[k * block_rows : (k + 1) * block_rows]
+                s = score(queries, keys, gate_q, gate_k, origin)
+                scores.append(s + masks[i // tile] if k == 0 else s)
+            top = functools.reduce(jnp.maximum, scores)
+            top = jnp.max(top, axis=1, keepdims=True)
+            total = 0.0
+            weighted = 0.0
+            for k, s in enumerate(scores):
+                weight = jnp.exp2(s - top)
+                total = total + weight
+                weighted = weighted + jnp.dot(
+                    weight.astype(bf16),
+                    value_ref[k * block_rows : (k + 1) * block_rows],
+                    preferred_element_type=f32,
+                )
+            den = jnp.sum(total, axis=1, keepdims=True)
+            place = h * block_rows + i
+            acc_ref[place : place + tile] = weighted
+            lane = lax.broadcasted_iota(jnp.int32, (tile, head_dim), 1)
+            stat_ref[place : place + tile] = jnp.where(lane == 0, top, den)
+
+
+def row_places(n_fs, step):
+    f = lax.axis_index("fs")
+    t = lax.axis_index("tp")
+    return [
+        pl.multiple_of((f ^ k) * 2 * step + lane * step, step)
+        for lane in (1 - t, t)
+        for k in range(n_fs - 1, -1, -1)
+    ]
 
 
 def project_kernel(n_fs, *refs):
     own, other = refs[:n_fs], refs[n_fs : 2 * n_fs]
-    w_query, w_post, w_pre, w_conv, near_ref = refs[2 * n_fs : 2 * n_fs + 5]
-    q_ref, post_ref, mixed_ref, rise_ref, rows_ref = refs[2 * n_fs + 5 :]
+    w_query, w_post, w_pre, w_conv, pair_ref = refs[2 * n_fs : 2 * n_fs + 5]
+    q_ref, post_ref, mixed_ref, rise_ref = refs[2 * n_fs + 5 :]
     step = own[0].shape[0]
-    f = lax.axis_index("fs")
-    t = lax.axis_index("tp")
-    for k in range(n_fs):
-        place = (f ^ k) * (2 * step)
-        rows_ref[pl.ds(pl.multiple_of(place + t * step, step), step)] = own[k][...]
-        rows_ref[pl.ds(pl.multiple_of(place + (1 - t) * step, step), step)] = other[k][...]
-    rows = rows_ref[...]
+    rows = jnp.concatenate([ref[...] for ref in (*other[::-1], *own[::-1])], axis=0)
     weight = jnp.concatenate([w_pre[...], w_conv[...]], axis=1)
     gated = jnp.dot(rows, weight, preferred_element_type=f32).astype(bf16).astype(f32)
     channels = w_pre.shape[1]
     mixed = (gated[:, :channels] * gated[:, channels:]).astype(bf16)
-    mixed_ref[...] = mixed
-    lane_rows = near_ref.shape[0]
-    rise_ref[:lane_rows] = near_ref[...]
-    rise_ref[lane_rows:, :channels] = mixed[mixed.shape[0] - EDGE :]
-    rise_ref[lane_rows:, channels:] = mixed[mixed.shape[0] - EDGE :]
+    for i, place in enumerate(row_places(n_fs, step)):
+        mixed_ref[pl.ds(place, step)] = mixed[i * step : (i + 1) * step]
+    lane_rows = pair_ref.shape[0]
+    rise_ref[:lane_rows] = pair_ref[...]
+    last = mixed_ref[mixed_ref.shape[0] - EDGE :]
+    rise_ref[lane_rows:] = jnp.concatenate([last] * (rise_ref.shape[1] // channels), axis=1)
     q_ref[...] = jnp.dot(rows, w_query[...], preferred_element_type=f32).astype(bf16)
     post_ref[...] = jnp.dot(rows, w_post[...], preferred_element_type=f32).astype(bf16)
 
 
-def conv_kernel(post_ref, mixed_ref, risen_ref, taps_ref, out_ref, extended_ref):
+def stack_kernel(top_ref, low_ref, out_ref):
+    out_ref[: top_ref.shape[0]] = top_ref[...]
+    out_ref[top_ref.shape[0] :] = low_ref[...]
+
+
+def conv_kernel(n_fs, post_ref, mixed_ref, risen_ref, taps_ref, out_ref, extended_ref, sum_ref):
     block_rows, channels = mixed_ref.shape
     group = lax.axis_index("fs") * lax.axis_size("tp") + lax.axis_index("tp")
     lanes = pl.ds(pl.multiple_of(group * channels, channels), channels)
-    edge = EDGE
     taps = taps_ref.shape[0]
-    halo = risen_ref[risen_ref.shape[0] - edge :, :channels].astype(f32)
-    extended_ref[0:edge] = jnp.where(lax.axis_index("sp") > 0, halo, 0.0)
-    extended_ref[edge:] = mixed_ref[...].astype(f32)
+    halo = risen_ref[risen_ref.shape[0] - EDGE :, :channels].astype(f32)
+    extended_ref[0:EDGE] = jnp.where(lax.axis_index("sp") > 0, halo, 0.0)
+    extended_ref[EDGE:] = mixed_ref[...].astype(f32)
     tap_rows = taps_ref[:, lanes].astype(f32)
-    first = edge - (taps - 1)
+    first = EDGE - (taps - 1)
     conv_sum = tap_rows[0:1] * extended_ref[first : first + block_rows]
     for i in range(1, taps):
         conv_sum = conv_sum + tap_rows[i : i + 1] * extended_ref[first + i : first + i + block_rows]
-    out_ref[...] = (post_ref[...].astype(f32) * conv_sum).astype(bf16)
-
-
-def mixer_kernel(n_fs, parts, *refs):
-    q_ref, conv_in_ref, gates_ref, mask_ref, block_ref = refs[:5]
-    near_ref, far_ref, high_ref, low_ref = refs[5:9]
-    w_conv_ref, w_attn_ref, send_ref, keep_ref = refs[9:13]
-    key_ref, value_ref, gate_col_ref, tile_ref, conv_ref, sum_ref = refs[13:]
-    z = lax.axis_index("sp")
-    f = lax.axis_index("fs")
-    t = lax.axis_index("tp")
-    block_rows = conv_in_ref.shape[0]
+    sum_ref[...] = conv_sum
     step = block_rows // (2 * n_fs)
-    head_dim = block_ref.shape[1] // 2
+    for i, place in enumerate(row_places(n_fs, step)):
+        rows = slice(i * step, (i + 1) * step)
+        out_ref[rows] = (post_ref[rows].astype(f32) * sum_ref[pl.ds(place, step)]).astype(bf16)
+
+
+def mixer_kernel(first, *refs):
+    q_ref, conv_ref, gates_ref, column_ref, acc_ref, stat_ref = refs[:6]
+    near_ref, far_ref, weight_ref, out_ref, key_ref, value_ref = refs[6:]
+    place_pairs(((near_ref, far_ref),), key_ref, value_ref)
+    block_rows = q_ref.shape[0]
+    head_dim = key_ref.shape[1]
     heads = q_ref.shape[1] // head_dim
-    group = f * 2 + t
-    count = len(parts)
-    rows = count * 2 * step
-    for lane, piece in ((t, near_ref), (1 - t, far_ref)):
-        for g in range(n_fs):
-            place = pl.ds(pl.multiple_of(g * 2 * step + lane * step, step), step)
-            key_ref[place] = piece[g * step : (g + 1) * step, :head_dim]
-            value_ref[place] = piece[g * step : (g + 1) * step, head_dim:]
-    key_blocks = [block_ref[:, :head_dim], key_ref[...], high_ref[:, :head_dim], low_ref[:, :head_dim]]
-    value_blocks = [
-        block_ref[:, head_dim:],
-        value_ref[...],
-        high_ref[:, head_dim:],
-        low_ref[:, head_dim:],
-    ]
-    origins = [z, z - 1, z - 2 - t, z - 3 + t]
-    n_blocks = len(origins)
-
-    def gate_row(h, origin):
-        place = pl.multiple_of(jnp.maximum(origin, 0) * block_rows, block_rows)
-        return gates_ref[pl.ds(group * heads + h, 1), pl.ds(place, block_rows)] * log2e
-
+    rows = out_ref.shape[0]
+    origin = lax.axis_index("sp") - 1
+    outs = [conv_ref[first : first + rows]]
     for h in range(heads):
-        column = jnp.broadcast_to(gate_row(h, z), (8, block_rows)).T
-        gate_col_ref[h] = column
-    scale = head_dim ** (-0.5) * log2e
-    bases = [pl.multiple_of((f ^ part) * (2 * step), 2 * step) for part in parts]
-    for h in range(heads):
-        for i, base in enumerate(bases):
-            place = (h * count + i) * 2 * step
-            tile_ref[place : place + 2 * step] = q_ref[
-                pl.ds(base, 2 * step), h * head_dim : (h + 1) * head_dim
-            ]
-    mask = jnp.concatenate([mask_ref[pl.ds(base, 2 * step)] for base in bases], axis=0)
-    outs = []
-    for h in range(heads):
-        queries = tile_ref[h * rows : (h + 1) * rows]
-        gate_q = jnp.concatenate(
-            [gate_col_ref[h, pl.ds(base, 2 * step), 0:1] for base in bases], axis=0
-        )
-        scores = []
-        for k in range(n_blocks):
-            s = lax.dot_general(
-                queries,
-                key_blocks[k],
-                (((1,), (1,)), ((), ())),
-                preferred_element_type=f32,
-            )
-            gate_k = jnp.where(origins[k] >= 0, gate_row(h, origins[k]), -masked_score)
-            s = s * scale + gate_q - gate_k
-            if k == 0:
-                s = s + mask
-            scores.append(s)
-        top = scores[0]
-        for s in scores[1:]:
-            top = jnp.maximum(top, s)
-        top = jnp.max(top, axis=1, keepdims=True)
-        total = 0.0
-        weighted = 0.0
-        for k in range(n_blocks):
-            weight = jnp.exp2(scores[k] - top)
-            total = total + weight
-            weighted = weighted + jnp.dot(
-                weight.astype(bf16),
-                value_blocks[k],
-                preferred_element_type=f32,
-            )
-        den = jnp.sum(total, axis=1, keepdims=True)
-        outs.append((weighted / den).astype(bf16))
-    attn = jnp.concatenate(outs, axis=1)
-    for i, base in enumerate(bases):
-        conv_ref[i * 2 * step : (i + 1) * 2 * step] = conv_in_ref[pl.ds(base, 2 * step)]
-    out = jnp.dot(conv_ref[...], w_conv_ref[...], preferred_element_type=f32)
-    out = out + jnp.dot(attn, w_attn_ref[...], preferred_element_type=f32)
-    sum_ref[...] = out.astype(bf16)
-    for i in range(count):
-        place = i * 2 * step
-        mine = pl.ds(pl.multiple_of(place + t * step, step), step)
-        theirs = pl.ds(pl.multiple_of(place + (1 - t) * step, step), step)
-        keep_ref[i * step : (i + 1) * step] = sum_ref[mine]
-        send_ref[i * step : (i + 1) * step] = sum_ref[theirs]
+        queries = q_ref[first : first + rows, h * head_dim : (h + 1) * head_dim]
+        gate_q = column_ref[h, first : first + rows, 0:1]
+        gate_k = gate_row(gates_ref, h, heads, origin, block_rows)
+        s = score(queries, key_ref[...], gate_q, gate_k, origin)
+        place = h * block_rows + first
+        held_top = stat_ref[place : place + rows, 0:1]
+        held_den = stat_ref[place : place + rows, 1:2]
+        top = jnp.maximum(held_top, jnp.max(s, axis=1, keepdims=True))
+        fade = jnp.exp2(held_top - top)
+        weight = jnp.exp2(s - top)
+        den = held_den * fade + jnp.sum(weight, axis=1, keepdims=True)
+        weighted = jnp.dot(weight.astype(bf16), value_ref[...], preferred_element_type=f32)
+        held = acc_ref[place : place + rows]
+        outs.append(((held * fade + weighted) / den).astype(bf16))
+    out = jnp.dot(jnp.concatenate(outs, axis=1), weight_ref[...], preferred_element_type=f32)
+    out_ref[...] = out.astype(bf16)
 
 
 def pair_sum_kernel(keep_ref, got_ref, *outs):
@@ -231,7 +249,6 @@
     channels = w_conv_post.shape[1]
     head_dim = w_key.shape[1]
     heads = w_query.shape[1] // head_dim
-    partition = (tuple(range(n_fs - 1, -1, -1)),)
 
     def swapped(x):
         return lax.ppermute(x, "tp", [(0, 1), (1, 0)])
@@ -239,14 +256,9 @@
     def crossed(x, k):
         return lax.ppermute(x, "fs", [(i, i ^ k) for i in range(n_fs)])
 
-    def raised(x, shifts):
-        route = [
-            (i * n_tp + t, (i + shift) % n_sp * n_tp + t)
-            for t, shift in enumerate(shifts)
-            for i in range(n_sp)
-            if i + shift < n_sp or RING
-        ]
-        return lax.ppermute(x, ("sp", "tp"), route)
+    def raised(x, shift):
+        route = [(i, (i + shift) % n_sp) for i in range(n_sp) if i + shift < n_sp or RING]
+        return lax.ppermute(x, "sp", route)
 
     def call(kernel, out_shape, scratch, mib, *operands, in_specs=None, work=0):
         extra = {} if in_specs is None else {"in_specs": in_specs}
@@ -286,15 +298,10 @@
         w_value,
         work=SMALL_WORK,
     )
-    block = call(
-        functools.partial(join_kernel, n_fs),
-        shape_of(block_rows, 2 * head_dim),
-        [],
-        4,
-        pair,
-        swapped(pair),
-    )
-    high = raised(block, (2, 3))
+    halves = [pair, swapped(pair)]
+    for shift in range(2, n_sp):
+        piece = raised(pair, shift)
+        halves += [piece, swapped(piece)]
     queries, post, mixed, rise = call(
         functools.partial(project_kernel, n_fs),
         (
@@ -303,7 +310,7 @@
             shape_of(block_rows, channels),
             shape_of(lane_rows + EDGE, 2 * head_dim),
         ),
-        [pltpu.VMEM((block_rows, width), bf16)],
+        [],
         16,
         *own,
         *other,
@@ -314,13 +321,28 @@
         pair,
         work=SMALL_WORK,
     )
-    near = raised(rise, (1, 1))
+    near = raised(rise, 1)
     far = swapped(near)
-    low = swapped(high)
+    acc, stat, column = call(
+        early_kernel,
+        (
+            shape_of(heads * block_rows, head_dim, f32),
+            shape_of(heads * block_rows, head_dim, f32),
+            jax.ShapeDtypeStruct((heads, block_rows, 8), f32),
+        ),
+        [pltpu.VMEM((len(halves) * lane_rows, head_dim), bf16)] * 2
+        + [pltpu.VMEM((block_rows, 8), f32)],
+        16,
+        queries,
+        gates,
+        mask,
+        *halves,
+        work=SMALL_WORK,
+    )
     conv_out = call(
-        conv_kernel,
+        functools.partial(conv_kernel, n_fs),
         shape_of(block_rows, channels),
-        [pltpu.VMEM((block_rows + EDGE, channels), f32)],
+        [pltpu.VMEM((block_rows + EDGE, channels), f32), pltpu.VMEM((block_rows, channels), f32)],
         4,
         post,
         mixed,
@@ -328,45 +350,47 @@
         taps,
         work=SMALL_WORK,
     )
-    sums = {}
-    for parts in partition:
-        count = len(parts)
-        send, keep = call(
-            functools.partial(mixer_kernel, n_fs, parts),
-            (shape_of(count * step, width), shape_of(count * step, width)),
-            [
-                pltpu.VMEM((block_rows, head_dim), bf16),
-                pltpu.VMEM((block_rows, head_dim), bf16),
-                pltpu.VMEM((heads, block_rows, 8), f32),
-                pltpu.VMEM((heads * count * 2 * step, head_dim), bf16),
-                pltpu.VMEM((count * 2 * step, channels), bf16),
-                pltpu.VMEM((count * 2 * step, width), bf16),
-            ],
+    w_out = call(
+        stack_kernel,
+        shape_of(w_out_conv.shape[0] + w_out_attn.shape[0], width),
+        [],
+        8,
+        w_out_conv,
+        w_out_attn,
+    )
+
+    def mixed_rows(first):
+        return call(
+            functools.partial(mixer_kernel, first),
+            shape_of(lane_rows, width),
+            [pltpu.VMEM((block_rows, head_dim), bf16)] * 2,
             16,
             queries,
             conv_out,
             gates,
-            mask,
-            block,
+            column,
+            acc,
+            stat,
             near,
             far,
-            high,
-            low,
-            w_out_conv,
-            w_out_attn,
+            w_out,
+            work=SMALL_WORK,
         )
-        got = swapped(send)
-        pieces = call(
-            pair_sum_kernel,
-            tuple(shape_of(step, width, f32 if k == 0 else bf16) for k in parts),
-            [],
-            8,
-            keep,
-            got,
-        )
-        for k, piece in zip(parts, pieces):
-            sums[k] = crossed(piece, k) if k else piece
-    return call(final_kernel, shape_of(step, width), [], 4, *[sums[k] for k in range(n_fs)])
+
+    send = mixed_rows(0)
+    got = swapped(send)
+    keep = mixed_rows(lane_rows)
+    parts = range(n_fs - 1, -1, -1)
+    pieces = call(
+        pair_sum_kernel,
+        tuple(shape_of(step, width, bf16 if k else f32) for k in parts),
+        [],
+        8,
+        keep,
+        got,
+    )
+    sums = [crossed(piece, k) if k else piece for k, piece in zip(parts, pieces)]
+    return call(final_kernel, shape_of(step, width), [], 4, *sums)
 
 
 def passed_along(block, axis, distance):

time: 41.7 us -> 44.2 us (1.060)
  Pallas kernels: 4.58 us -> 6.52 us
  waiting for transfers between devices: 21.2 us -> 22.4 us
  starting transfers between devices: 13.8 us -> 13.2 us
    ppermute x2 -> x3, waiting for transfers between devices: 5.26 us -> 8.95 us  [raised(): return lax.ppermute(x, 'sp', route)]
    ppermute x8 -> x9, waiting for transfers between devices: 3.71 us -> 1.71 us  [swapped(): return lax.ppermute(x, 'tp', [(0, 1), (1, 0)])]
    pallas_call x9 -> x11, Pallas kernels: 4.58 us -> 6.52 us  [call(): pl.pallas_call(kernel, out_shape=out_shape, scratch_shapes=scratch, compi...]
    ppermute x2 -> x3, starting transfers between devices: 4.46 us -> 3.72 us  [raised(): return lax.ppermute(x, 'sp', route)]
    ppermute x8 -> x9, starting transfers between devices: 1.21 us -> 1.25 us  [swapped(): return lax.ppermute(x, 'tp', [(0, 1), (1, 0)])]
  transfers between devices with their start and end apart: 16 -> 18, of which waited for: 10 -> 11; matrix products, arithmetic and copies ran while one was open for 0% -> 0% of each run, Pallas kernels for 4% -> 10%
where the time goes in v2:
time: 44.2 us; the launch traced here: 44 us
  waiting for transfers between devices  22.4 us (51%)
  starting transfers between devices  13.2 us (30%)
  Pallas kernels  6.52 us (15%)
  local copies, waits for them, and re-layouts  1.66 us (4%)
    ppermute x6, waiting for transfers between devices, crossed(): return lax.ppermute(x, 'fs', [(i, i ^ k) for i in range(n_fs)])  11.8 us
    ppermute x3, waiting for transfers between devices, raised(): return lax.ppermute(x, 'sp', route)  8.95 us
    ppermute x6, starting transfers between devices, crossed(): return lax.ppermute(x, 'fs', [(i, i ^ k) for i in range(n_fs)])  8.18 us
    pallas_call x11, Pallas kernels, call(): pl.pallas_call(kernel, out_shape=out_shape, scratch_shapes=scratch, compi...  6.52 us
    ppermute x3, starting transfers between devices, raised(): return lax.ppermute(x, 'sp', route)  3.72 us
    ppermute x9, waiting for transfers between devices, swapped(): return lax.ppermute(x, 'tp', [(0, 1), (1, 0)])  1.71 us
    unnamed x24, local copies, waits for them, and re-layouts  1.66 us
    ppermute x9, starting transfers between devices, swapped(): return lax.ppermute(x, 'tp', [(0, 1), (1, 0)])  1.25 us
  transfers between devices with their start and end apart: 18, of which 11 were waited for; matrix products, arithmetic and copies ran while one was open for 0% of the time, Pallas kernels for 10%

profile of v2, /device:TPU:0, one launch (start us, length us, event | category | flops | bytes accessed | tf_op | source)
XLA Modules:
  0.0 44.0 jit_solution(3386684694052662974)
XLA Ops:
  0.0 0.9 %copy-done.8 = bf16[32,2048]{1,0:T(8,128)(2,1)S(1)} copy-done((bf16[32,2048]{1,0:T(8,128)(2,1)S(1)}, bf16[32,2048]{1,0:T(8,128)(2,1)}, u32[]{:S(2)}) %copy-start.8) | copy-done | bytes 131096
  0.9 0.7 %copy-done.10 = f32[2048]{0:T(1024)S(1)} copy-done((f32[2048]{0:T(1024)S(1)}, f32[2048]{0:T(1024)}, u32[]{:S(2)}) %copy-start.10) | copy-done | bytes 8216
  1.6 0.1 shard_map.118.refs_0_
  1.7 4.0 %collective-permute-start.2 = (bf16[32,2048]{1,0:T(8,128)(2,1)S(1)}, bf16[32,2048]{1,0:T(8,128)(2,1)S(1)}, u32[]{:S(2)}, u32[]{:S(2)}) collective-permute-start(bf16[32,2048]{1,0:T(8,128)(2,1)S(1)} %shard_map.118.refs_0_), channel_id=1, source_target_pairs={{0,6},{2,4},{4,2},{6,0},{1,7},{3,5},{5,3},{7,1},{8,14},{10,12},{12... | collective-permute-start | bytes 393224 | tf_op jit(solution)/shard_map/ppermute | solution.py:257
  5.7 0.5 %collective-permute-start.1 = (bf16[32,2048]{1,0:T(8,128)(2,1)S(1)}, bf16[32,2048]{1,0:T(8,128)(2,1)S(1)}, u32[]{:S(2)}, u32[]{:S(2)}) collective-permute-start(bf16[32,2048]{1,0:T(8,128)(2,1)S(1)} %shard_map.118.refs_0_), channel_id=1, source_target_pairs={{0,4},{2,6},{4,0},{6,2},{1,5},{3,7},{5,1},{7,3},{8,12},{10,14},{12... | collective-permute-start | bytes 393224 | tf_op jit(solution)/shard_map/ppermute | solution.py:257
  6.2 0.1 collective-permute-start
  6.4 3.2 %collective-permute-done.2.refs_3_ = bf16[32,2048]{1,0:T(8,128)(2,1)S(1)} collective-permute-done((bf16[32,2048]{1,0:T(8,128)(2,1)S(1)}, bf16[32,2048]{1,0:T(8,128)(2,1)S(1)}, u32[]{:S(2)}, u32[]{:S(2)}) %collective-permute-start.2) | collective-permute-done | bytes 131104 | tf_op jit(solution)/shard_map/ppermute | solution.py:257
  9.6 2.4 %collective-permute-done.1.refs_2_ = bf16[32,2048]{1,0:T(8,128)(2,1)S(1)} collective-permute-done((bf16[32,2048]{1,0:T(8,128)(2,1)S(1)}, bf16[32,2048]{1,0:T(8,128)(2,1)S(1)}, u32[]{:S(2)}, u32[]{:S(2)}) %collective-permute-start.1) | collective-permute-done | bytes 131104 | tf_op jit(solution)/shard_map/ppermute | solution.py:257
  12.0 0.2 collective-permute-done.refs_1_
  12.3 0.3 shard_map.119.refs_12_.refs_3_
  12.6 3.7 %collective-permute-start.11 = (bf16[128,256]{1,0:T(8,128)(2,1)S(1)}, bf16[128,256]{1,0:T(8,128)(2,1)S(1)}, u32[]{:S(2)}, u32[]{:S(2)}) collective-permute-start(bf16[128,256]{1,0:T(8,128)(2,1)S(1)} %shard_map.119.refs_12_.refs_3_), channel_id=1, source_target_pairs={{0,24},{8,0},{16,8},{24,16},{1,25},{9,1},{17,9},{25,17},{2,26},{10... | collective-permute-start | bytes 196616 | tf_op jit(solution)/shard_map/ppermute | solution.py:261
  16.3 0.5 %collective-permute-start.5 = (bf16[32,2048]{1,0:T(8,128)(2,1)S(1)}, bf16[32,2048]{1,0:T(8,128)(2,1)S(1)}, u32[]{:S(2)}, u32[]{:S(2)}) collective-permute-start(bf16[32,2048]{1,0:T(8,128)(2,1)S(1)} %collective-permute-done.1.refs_2_), channel_id=1, source_target_pairs={{0,1},{1,0},{2,3},{3,2},{4,5},{5,4},{6,7},{7,6},{8,9},{9,8},{10,11... | collective-permute-start | bytes 393224 | tf_op jit(solution)/shard_map/ppermute | solution.py:254
  16.9 0.1 shard_map.124.refs_8_
  17.0 1.4 %collective-permute-done.11.refs_7_ = bf16[128,256]{1,0:T(8,128)(2,1)S(1)} collective-permute-done((bf16[128,256]{1,0:T(8,128)(2,1)S(1)}, bf16[128,256]{1,0:T(8,128)(2,1)S(1)}, u32[]{:S(2)}, u32[]{:S(2)}) %collective-permute-start.11) | collective-permute-done | bytes 65568 | tf_op jit(solution)/shard_map/ppermute | solution.py:261
  18.5 3.0 %collective-permute-done.9.refs_5_ = bf16[128,256]{1,0:T(8,128)(2,1)S(1)} collective-permute-done((bf16[128,256]{1,0:T(8,128)(2,1)S(1)}, bf16[128,256]{1,0:T(8,128)(2,1)S(1)}, u32[]{:S(2)}, u32[]{:S(2)}) %collective-permute-start.9) | collective-permute-done | bytes 65568 | tf_op jit(solution)/shard_map/ppermute | solution.py:261
  21.5 0.5 %collective-permute-start.10 = (bf16[128,256]{1,0:T(8,128)(2,1)S(1)}, bf16[128,256]{1,0:T(8,128)(2,1)S(1)}, u32[]{:S(2)}, u32[]{:S(2)}) collective-permute-start(bf16[128,256]{1,0:T(8,128)(2,1)S(1)} %collective-permute-done.9.refs_5_), channel_id=1, source_target_pairs={{0,1},{1,0},{2,3},{3,2},{4,5},{5,4},{6,7},{7,6},{8,9},{9,8},{10,11... | collective-permute-start | bytes 196616 | tf_op jit(solution)/shard_map/ppermute | solution.py:254
  22.0 1.0 %shard_map.120 = (bf16[256,256]{1,0:T(8,128)(2,1)S(1)}, bf16[256,128]{1,0:T(8,128)(2,1)S(1)}, bf16[256,128]{1,0:T(8,128)(2,1)S(1)}, bf16[144,256]{1,0:T(8,128)(2,1)S(1)}) custom-call(bf16[32,2048]{1,0:T(8,128)(2,1)S(1)} %shard_map.118.refs_0_, bf16[32,2048]{1,0:T(8,128)(2,1)S(1)} %collective-permute-done.refs_1_, ...), custom_call_target="tpu_custom_call" | custom-call | flops 2000000000 | tf_op jit(solution)/shard_map/pallas_call | solution.py:269
  23.2 1.6 %shard_map.123 = (f32[512,128]{1,0:T(8,128)S(1)}, f32[512,128]{1,0:T(8,128)S(1)}, f32[2,256,8]{2,1,0:T(8,128)S(1)}) custom-call(bf16[256,256]{1,0:T(8,128)(2,1)S(1)} %get-tuple-element.16.refs_0_, f32[16,1024]{1,0:T(8,128)S(1)} %copy-done.9, f32[256,256]{1,0:T(8,128)S(1)} %shard_map.122.refs_2_, bf16[128,256]{1,0:T(8,128)(2,1)S(1)} %shard_map.119.refs_12_.refs_3_, ...), custom_call_target="tpu_custom_call" | custom-call | flops 2000000000 | tf_op jit(solution)/shard_map/pallas_call | solution.py:269
  24.7 4.5 %collective-permute-done.7.risen_ref.refs_6_ = bf16[144,256]{1,0:T(8,128)(2,1)S(1)} collective-permute-done((bf16[144,256]{1,0:T(8,128)(2,1)S(1)}, bf16[144,256]{1,0:T(8,128)(2,1)S(1)}, u32[]{:S(2)}, u32[]{:S(2)}) %collective-permute-start.7) | collective-permute-done | bytes 73760 | tf_op jit(solution)/shard_map/ppermute | solution.py:261
  29.3 1.2 %collective-permute-done.13.refs_7_ = bf16[144,256]{1,0:T(8,128)(2,1)S(1)} collective-permute-done((bf16[144,256]{1,0:T(8,128)(2,1)S(1)}, bf16[144,256]{1,0:T(8,128)(2,1)S(1)}, u32[]{:S(2)}, u32[]{:S(2)}) %collective-permute-start.13) | collective-permute-done | bytes 73760 | tf_op jit(solution)/shard_map/ppermute | solution.py:254
  30.5 1.3 %shard_map.126 = bf16[128,2048]{1,0:T(8,128)(2,1)S(1)} custom-call(bf16[256,256]{1,0:T(8,128)(2,1)S(1)} %get-tuple-element.16.refs_0_, bf16[256,128]{1,0:T(8,128)(2,1)S(1)} %shard_map.121.refs_1_, f32[16,1024]{1,0:T(8,128)S(1)} %copy-done.9, f32[2,256,8]{2,1,0:T(8,128)S(1)} %get-tuple-element.20.refs_3_, f32[512,128]{1,0:T(8,128)S(1)} %get-tuple-element.21.refs_4_, ...), custom_call_target="tpu_custom_call" | custom-call | flops 2000000000 | tf_op jit(solution)/shard_map/pallas_call | solution.py:269
  31.8 0.2 collective-permute-start.14
  32.0 1.2 %shard_map.125.keep_ref = bf16[128,2048]{1,0:T(8,128)(2,1)S(1)} custom-call(bf16[256,256]{1,0:T(8,128)(2,1)S(1)} %get-tuple-element.16.refs_0_, bf16[256,128]{1,0:T(8,128)(2,1)S(1)} %shard_map.121.refs_1_, f32[16,1024]{1,0:T(8,128)S(1)} %copy-done.9, f32[2,256,8]{2,1,0:T(8,128)S(1)} %get-tuple-element.20.refs_3_, f32[512,128]{1,0:T(8,128)S(1)} %get-tuple-element.21.refs_4_, ...), custom_call_target="tpu_custom_call" | custom-call | flops 2000000000 | tf_op jit(solution)/shard_map/pallas_call | solution.py:269
  33.2 0.5 %collective-permute-done.14.got_ref = bf16[128,2048]{1,0:T(8,128)(2,1)S(1)} collective-permute-done((bf16[128,2048]{1,0:T(8,128)(2,1)S(1)}, bf16[128,2048]{1,0:T(8,128)(2,1)S(1)}, u32[]{:S(2)}, u32[]{:S(2)}) %collective-permute-start.14) | collective-permute-done | bytes 524320 | tf_op jit(solution)/shard_map/ppermute | solution.py:254
  33.7 0.1 shard_map.127
  33.9 1.7 %collective-permute-start.15 = (bf16[32,2048]{1,0:T(8,128)(2,1)S(1)}, bf16[32,2048]{1,0:T(8,128)(2,1)S(1)}, u32[]{:S(2)}, u32[]{:S(2)}) collective-permute-start(bf16[32,2048]{1,0:T(8,128)(2,1)S(1)} %get-tuple-element.23), channel_id=1, source_target_pairs={{0,6},{2,4},{4,2},{6,0},{1,7},{3,5},{5,3},{7,1},{8,14},{10,12},{12... | collective-permute-start | bytes 393224 | tf_op jit(solution)/shard_map/ppermute | solution.py:257
  35.6 1.3 %collective-permute-start.16 = (bf16[32,2048]{1,0:T(8,128)(2,1)S(1)}, bf16[32,2048]{1,0:T(8,128)(2,1)S(1)}, u32[]{:S(2)}, u32[]{:S(2)}) collective-permute-start(bf16[32,2048]{1,0:T(8,128)(2,1)S(1)} %get-tuple-element.24), channel_id=1, source_target_pairs={{0,4},{2,6},{4,0},{6,2},{1,5},{3,7},{5,1},{7,3},{8,12},{10,14},{12... | collective-permute-start | bytes 393224 | tf_op jit(solution)/shard_map/ppermute | solution.py:257
  36.9 0.5 %collective-permute-start.17 = (bf16[32,2048]{1,0:T(8,128)(2,1)S(1)}, bf16[32,2048]{1,0:T(8,128)(2,1)S(1)}, u32[]{:S(2)}, u32[]{:S(2)}) collective-permute-start(bf16[32,2048]{1,0:T(8,128)(2,1)S(1)} %get-tuple-element.25), channel_id=1, source_target_pairs={{0,2},{2,0},{4,6},{6,4},{1,3},{3,1},{5,7},{7,5},{8,10},{10,8},{12,... | collective-permute-start | bytes 393224 | tf_op jit(solution)/shard_map/ppermute | solution.py:257
  37.4 3.8 %collective-permute-done.15.refs_0_ = bf16[32,2048]{1,0:T(8,128)(2,1)S(1)} collective-permute-done((bf16[32,2048]{1,0:T(8,128)(2,1)S(1)}, bf16[32,2048]{1,0:T(8,128)(2,1)S(1)}, u32[]{:S(2)}, u32[]{:S(2)}) %collective-permute-start.15) | collective-permute-done | bytes 131104 | tf_op jit(solution)/shard_map/ppermute | solution.py:257
  41.2 2.0 %collective-permute-done.16.refs_1_ = bf16[32,2048]{1,0:T(8,128)(2,1)S(1)} collective-permute-done((bf16[32,2048]{1,0:T(8,128)(2,1)S(1)}, bf16[32,2048]{1,0:T(8,128)(2,1)S(1)}, u32[]{:S(2)}, u32[]{:S(2)}) %collective-permute-start.16) | collective-permute-done | bytes 131104 | tf_op jit(solution)/shard_map/ppermute | solution.py:257
  43.2 0.1 collective-permute-done.17.refs_2_
  43.3 0.7 %shard_map.128 = bf16[32,2048]{1,0:T(8,128)(2,1)} custom-call(bf16[32,2048]{1,0:T(8,128)(2,1)S(1)} %collective-permute-done.15.refs_0_, bf16[32,2048]{1,0:T(8,128)(2,1)S(1)} %collective-permute-done.16.refs_1_, bf16[32,2048]{1,0:T(8,128)(2,1)S(1)} %collective-permute-done.17.refs_2_, f32[32,2048]{1,0:T(8,128)S(1)} %get-tuple-element.26.refs_3_), custom_call_target="tpu_custom_call" | custom-call | tf_op jit(solution)/shard_map/pallas_call | solution.py:269
  (39 shorter events, 0.2 us)
Async XLA Ops:
  0.0 0.9 %copy-start.8 = (bf16[32,2048]{1,0:T(8,128)(2,1)S(1)}, bf16[32,2048]{1,0:T(8,128)(2,1)}, u32[]{:S(2)}) copy-start(bf16[32,2048]{1,0:T(8,128)(2,1)} %tokens_ref.1) | copy-start | bytes 393220
  0.9 0.7 %copy-start.10 = (f32[2048]{0:T(1024)S(1)}, f32[2048]{0:T(1024)}, u32[]{:S(2)}) copy-start(f32[2048]{0:T(1024)} %param.13) | copy-start | bytes 24580
  1.6 10.7 %copy-start.3 = (bf16[2048,128]{1,0:T(8,128)(2,1)S(1)}, bf16[2048,128]{1,0:T(8,128)(2,1)}, u32[]{:S(2)}) copy-start(bf16[2048,128]{1,0:T(8,128)(2,1)} %refs_4_.1) | copy-start | bytes 1572868
  1.6 10.7 %copy-start.4 = (bf16[2048,128]{1,0:T(8,128)(2,1)S(1)}, bf16[2048,128]{1,0:T(8,128)(2,1)}, u32[]{:S(2)}) copy-start(bf16[2048,128]{1,0:T(8,128)(2,1)} %refs_5_.1) | copy-start | bytes 1572868
  1.7 7.9 %collective-permute-start.2 = (bf16[32,2048]{1,0:T(8,128)(2,1)S(1)}, bf16[32,2048]{1,0:T(8,128)(2,1)S(1)}, u32[]{:S(2)}, u32[]{:S(2)}) collective-permute-start(bf16[32,2048]{1,0:T(8,128)(2,1)S(1)} %shard_map.118.refs_0_), channel_id=1, source_target_pairs={{0,6},{2,4},{4,2},{6,0},{1,7},{3,5},{5,3},{7,1},{8,14},{10,12},{12... | collective-permute-start | bytes 393224 | tf_op jit(solution)/shard_map/ppermute | solution.py:257
  5.7 6.3 %collective-permute-start.1 = (bf16[32,2048]{1,0:T(8,128)(2,1)S(1)}, bf16[32,2048]{1,0:T(8,128)(2,1)S(1)}, u32[]{:S(2)}, u32[]{:S(2)}) collective-permute-start(bf16[32,2048]{1,0:T(8,128)(2,1)S(1)} %shard_map.118.refs_0_), channel_id=1, source_target_pairs={{0,4},{2,6},{4,0},{6,2},{1,5},{3,7},{5,1},{7,3},{8,12},{10,14},{12... | collective-permute-start | bytes 393224 | tf_op jit(solution)/shard_map/ppermute | solution.py:257
  6.2 6.0 %collective-permute-start = (bf16[32,2048]{1,0:T(8,128)(2,1)S(1)}, bf16[32,2048]{1,0:T(8,128)(2,1)S(1)}, u32[]{:S(2)}, u32[]{:S(2)}) collective-permute-start(bf16[32,2048]{1,0:T(8,128)(2,1)S(1)} %shard_map.118.refs_0_), channel_id=1, source_target_pairs={{0,2},{2,0},{4,6},{6,4},{1,3},{3,1},{5,7},{7,5},{8,10},{10,8},{12,... | collective-permute-start | bytes 393224 | tf_op jit(solution)/shard_map/ppermute | solution.py:257
  6.4 10.4 %collective-permute-start.3 = (bf16[32,2048]{1,0:T(8,128)(2,1)S(1)}, bf16[32,2048]{1,0:T(8,128)(2,1)S(1)}, u32[]{:S(2)}, u32[]{:S(2)}) collective-permute-start(bf16[32,2048]{1,0:T(8,128)(2,1)S(1)} %shard_map.118.refs_0_), channel_id=1, source_target_pairs={{0,1},{1,0},{2,3},{3,2},{4,5},{5,4},{6,7},{7,6},{8,9},{9,8},{10,11... | collective-permute-start | bytes 393224 | tf_op jit(solution)/shard_map/ppermute | solution.py:254
  12.6 4.2 %copy-start = (bf16[256,2048]{1,0:T(8,128)(2,1)S(1)}, bf16[256,2048]{1,0:T(8,128)(2,1)}, u32[]{:S(2)}) copy-start(bf16[256,2048]{1,0:T(8,128)(2,1)} %low_ref.1) | copy-start | bytes 3145732
  12.6 4.2 %copy-start.1 = (bf16[128,2048]{1,0:T(8,128)(2,1)S(1)}, bf16[128,2048]{1,0:T(8,128)(2,1)}, u32[]{:S(2)}) copy-start(bf16[128,2048]{1,0:T(8,128)(2,1)} %top_ref.1) | copy-start | bytes 1572868
  12.6 5.8 %collective-permute-start.11 = (bf16[128,256]{1,0:T(8,128)(2,1)S(1)}, bf16[128,256]{1,0:T(8,128)(2,1)S(1)}, u32[]{:S(2)}, u32[]{:S(2)}) collective-permute-start(bf16[128,256]{1,0:T(8,128)(2,1)S(1)} %shard_map.119.refs_12_.refs_3_), channel_id=1, source_target_pairs={{0,24},{8,0},{16,8},{24,16},{1,25},{9,1},{17,9},{25,17},{2,26},{10... | collective-permute-start | bytes 196616 | tf_op jit(solution)/shard_map/ppermute | solution.py:261
  16.3 5.2 %collective-permute-start.9 = (bf16[128,256]{1,0:T(8,128)(2,1)S(1)}, bf16[128,256]{1,0:T(8,128)(2,1)S(1)}, u32[]{:S(2)}, u32[]{:S(2)}) collective-permute-start(bf16[128,256]{1,0:T(8,128)(2,1)S(1)} %shard_map.119.refs_12_.refs_3_), channel_id=1, source_target_pairs={{0,16},{8,24},{16,0},{24,8},{1,17},{9,25},{17,1},{25,9},{2,18},{10... | collective-permute-start | bytes 196616 | tf_op jit(solution)/shard_map/ppermute | solution.py:261
  16.3 5.2 %collective-permute-start.6 = (bf16[32,2048]{1,0:T(8,128)(2,1)S(1)}, bf16[32,2048]{1,0:T(8,128)(2,1)S(1)}, u32[]{:S(2)}, u32[]{:S(2)}) collective-permute-start(bf16[32,2048]{1,0:T(8,128)(2,1)S(1)} %collective-permute-done.2.refs_3_), channel_id=1, source_target_pairs={{0,1},{1,0},{2,3},{3,2},{4,5},{5,4},{6,7},{7,6},{8,9},{9,8},{10,11... | collective-permute-start | bytes 393224 | tf_op jit(solution)/shard_map/ppermute | solution.py:254
  16.3 5.7 %collective-permute-start.5 = (bf16[32,2048]{1,0:T(8,128)(2,1)S(1)}, bf16[32,2048]{1,0:T(8,128)(2,1)S(1)}, u32[]{:S(2)}, u32[]{:S(2)}) collective-permute-start(bf16[32,2048]{1,0:T(8,128)(2,1)S(1)} %collective-permute-done.1.refs_2_), channel_id=1, source_target_pairs={{0,1},{1,0},{2,3},{3,2},{4,5},{5,4},{6,7},{7,6},{8,9},{9,8},{10,11... | collective-permute-start | bytes 393224 | tf_op jit(solution)/shard_map/ppermute | solution.py:254
  16.8 5.2 %collective-permute-start.4 = (bf16[32,2048]{1,0:T(8,128)(2,1)S(1)}, bf16[32,2048]{1,0:T(8,128)(2,1)S(1)}, u32[]{:S(2)}, u32[]{:S(2)}) collective-permute-start(bf16[32,2048]{1,0:T(8,128)(2,1)S(1)} %collective-permute-done.refs_1_), channel_id=1, source_target_pairs={{0,1},{1,0},{2,3},{3,2},{4,5},{5,4},{6,7},{7,6},{8,9},{9,8},{10,11... | collective-permute-start | bytes 393224 | tf_op jit(solution)/shard_map/ppermute | solution.py:254
  16.9 5.1 %copy-start.2 = (bf16[2048,256]{1,0:T(8,128)(2,1)S(1)}, bf16[2048,256]{1,0:T(8,128)(2,1)}, u32[]{:S(2)}) copy-start(bf16[2048,256]{1,0:T(8,128)(2,1)} %refs_8_.1) | copy-start | bytes 3145732
  16.9 5.1 %copy-start.5 = (bf16[2048,128]{1,0:T(8,128)(2,1)S(1)}, bf16[2048,128]{1,0:T(8,128)(2,1)}, u32[]{:S(2)}) copy-start(bf16[2048,128]{1,0:T(8,128)(2,1)} %refs_9_.1) | copy-start | bytes 1572868
  16.9 5.1 %copy-start.6 = (bf16[2048,128]{1,0:T(8,128)(2,1)S(1)}, bf16[2048,128]{1,0:T(8,128)(2,1)}, u32[]{:S(2)}) copy-start(bf16[2048,128]{1,0:T(8,128)(2,1)} %refs_10_.1) | copy-start | bytes 1572868
  16.9 5.1 %copy-start.7 = (bf16[2048,128]{1,0:T(8,128)(2,1)S(1)}, bf16[2048,128]{1,0:T(8,128)(2,1)}, u32[]{:S(2)}) copy-start(bf16[2048,128]{1,0:T(8,128)(2,1)} %refs_11_.1) | copy-start | bytes 1572868
  17.0 6.1 %copy-start.9 = (f32[16,1024]{1,0:T(8,128)S(1)}, f32[16,1024]{1,0:T(8,128)}, u32[]{:S(2)}) copy-start(f32[16,1024]{1,0:T(8,128)} %refs_2_.3) | copy-start | bytes 196612
  18.5 4.6 %collective-permute-start.8 = (bf16[128,256]{1,0:T(8,128)(2,1)S(1)}, bf16[128,256]{1,0:T(8,128)(2,1)S(1)}, u32[]{:S(2)}, u32[]{:S(2)}) collective-permute-start(bf16[128,256]{1,0:T(8,128)(2,1)S(1)} %shard_map.119.refs_12_.refs_3_), channel_id=1, source_target_pairs={{0,1},{1,0},{2,3},{3,2},{4,5},{5,4},{6,7},{7,6},{8,9},{9,8},{10,11... | collective-permute-start | bytes 196616 | tf_op jit(solution)/shard_map/ppermute | solution.py:254
  21.5 1.6 %collective-permute-start.12 = (bf16[128,256]{1,0:T(8,128)(2,1)S(1)}, bf16[128,256]{1,0:T(8,128)(2,1)S(1)}, u32[]{:S(2)}, u32[]{:S(2)}) collective-permute-start(bf16[128,256]{1,0:T(8,128)(2,1)S(1)} %collective-permute-done.11.refs_7_), channel_id=1, source_target_pairs={{0,1},{1,0},{2,3},{3,2},{4,5},{5,4},{6,7},{7,6},{8,9},{9,8},{10,11... | collective-permute-start | bytes 196616 | tf_op jit(solution)/shard_map/ppermute | solution.py:254
  21.5 1.6 %collective-permute-start.10 = (bf16[128,256]{1,0:T(8,128)(2,1)S(1)}, bf16[128,256]{1,0:T(8,128)(2,1)S(1)}, u32[]{:S(2)}, u32[]{:S(2)}) collective-permute-start(bf16[128,256]{1,0:T(8,128)(2,1)S(1)} %collective-permute-done.9.refs_5_), channel_id=1, source_target_pairs={{0,1},{1,0},{2,3},{3,2},{4,5},{5,4},{6,7},{7,6},{8,9},{9,8},{10,11... | collective-permute-start | bytes 196616 | tf_op jit(solution)/shard_map/ppermute | solution.py:254
  23.0 6.2 %collective-permute-start.7 = (bf16[144,256]{1,0:T(8,128)(2,1)S(1)}, bf16[144,256]{1,0:T(8,128)(2,1)S(1)}, u32[]{:S(2)}, u32[]{:S(2)}) collective-permute-start(bf16[144,256]{1,0:T(8,128)(2,1)S(1)} %get-tuple-element.19), channel_id=1, source_target_pairs={{0,8},{8,16},{16,24},{24,0},{1,9},{9,17},{17,25},{25,1},{2,10},{10... | collective-permute-start | bytes 221192 | tf_op jit(solution)/shard_map/ppermute | solution.py:261
  23.1 6.1 %copy-start.11 = (bf16[3,1024]{1,0:T(4,128)(2,1)S(1)}, bf16[3,1024]{1,0:T(4,128)(2,1)}, u32[]{:S(2)}) copy-start(bf16[3,1024]{1,0:T(4,128)(2,1)} %taps_ref.1) | copy-start | bytes 18436
  29.2 1.3 %collective-permute-start.13 = (bf16[144,256]{1,0:T(8,128)(2,1)S(1)}, bf16[144,256]{1,0:T(8,128)(2,1)S(1)}, u32[]{:S(2)}, u32[]{:S(2)}) collective-permute-start(bf16[144,256]{1,0:T(8,128)(2,1)S(1)} %collective-permute-done.7.risen_ref.refs_6_), channel_id=1, source_target_pairs={{0,1},{1,0},{2,3},{3,2},{4,5},{5,4},{6,7},{7,6},{8,9},{9,8},{10,11... | collective-permute-start | bytes 221192 | tf_op jit(solution)/shard_map/ppermute | solution.py:254
  31.8 2.0 %collective-permute-start.14 = (bf16[128,2048]{1,0:T(8,128)(2,1)S(1)}, bf16[128,2048]{1,0:T(8,128)(2,1)S(1)}, u32[]{:S(2)}, u32[]{:S(2)}) collective-permute-start(bf16[128,2048]{1,0:T(8,128)(2,1)S(1)} %shard_map.126), channel_id=1, source_target_pairs={{0,1},{1,0},{2,3},{3,2},{4,5},{5,4},{6,7},{7,6},{8,9},{9,8},{10,11... | collective-permute-start | bytes 1572872 | tf_op jit(solution)/shard_map/ppermute | solution.py:254
  33.9 7.3 %collective-permute-start.15 = (bf16[32,2048]{1,0:T(8,128)(2,1)S(1)}, bf16[32,2048]{1,0:T(8,128)(2,1)S(1)}, u32[]{:S(2)}, u32[]{:S(2)}) collective-permute-start(bf16[32,2048]{1,0:T(8,128)(2,1)S(1)} %get-tuple-element.23), channel_id=1, source_target_pairs={{0,6},{2,4},{4,2},{6,0},{1,7},{3,5},{5,3},{7,1},{8,14},{10,12},{12... | collective-permute-start | bytes 393224 | tf_op jit(solution)/shard_map/ppermute | solution.py:257
  35.6 7.6 %collective-permute-start.16 = (bf16[32,2048]{1,0:T(8,128)(2,1)S(1)}, bf16[32,2048]{1,0:T(8,128)(2,1)S(1)}, u32[]{:S(2)}, u32[]{:S(2)}) collective-permute-start(bf16[32,2048]{1,0:T(8,128)(2,1)S(1)} %get-tuple-element.24), channel_id=1, source_target_pairs={{0,4},{2,6},{4,0},{6,2},{1,5},{3,7},{5,1},{7,3},{8,12},{10,14},{12... | collective-permute-start | bytes 393224 | tf_op jit(solution)/shard_map/ppermute | solution.py:257
  36.9 6.4 %collective-permute-start.17 = (bf16[32,2048]{1,0:T(8,128)(2,1)S(1)}, bf16[32,2048]{1,0:T(8,128)(2,1)S(1)}, u32[]{:S(2)}, u32[]{:S(2)}) collective-permute-start(bf16[32,2048]{1,0:T(8,128)(2,1)S(1)} %get-tuple-element.25), channel_id=1, source_target_pairs={{0,2},{2,0},{4,6},{6,4},{1,3},{3,1},{5,7},{7,5},{8,10},{10,8},{12,... | collective-permute-start | bytes 393224 | tf_op jit(solution)/shard_map/ppermute | solution.py:257

commit v3 on v2

--- a/solution.py
+++ b/solution.py
@@ -13,7 +13,7 @@
 f32 = jnp.float32
 bf16 = jnp.bfloat16
 EDGE = 16
-RING = True
+RING = (False, False, True, True)
 NORM_WORK = 20000000000
 MASK_WORK = 2000000000
 SMALL_WORK = 2000000000
@@ -77,16 +77,40 @@
     return s * scale + gate_q - jnp.where(origin >= 0, gate_k, -masked_score)
 
 
+def fold_blocks(q_ref, gates_ref, column_ref, blocks, masks, acc_ref, stat_ref):
+    block_rows = q_ref.shape[0]
+    head_dim = acc_ref.shape[1]
+    heads = q_ref.shape[1] // head_dim
+    tile = block_rows // 2
+    for h in range(heads):
+        for i in range(0, block_rows, tile):
+            queries = q_ref[i : i + tile, h * head_dim : (h + 1) * head_dim]
+            gate_q = column_ref[h, i : i + tile, 0:1]
+            scores = []
+            for k, (keys, values, origin) in enumerate(blocks):
+                gate_k = gate_row(gates_ref, h, heads, origin, block_rows)
+                s = score(queries, keys, gate_q, gate_k, origin)
+                scores.append(s if k else s + masks[i // tile])
+            top = jnp.max(functools.reduce(jnp.maximum, scores), axis=1, keepdims=True)
+            weights = [jnp.exp2(s - top) for s in scores]
+            den = jnp.sum(sum(weights), axis=1, keepdims=True)
+            weighted = sum(
+                jnp.dot(weight.astype(bf16), values, preferred_element_type=f32)
+                for weight, (keys, values, origin) in zip(weights, blocks)
+            )
+            place = slice(h * block_rows + i, h * block_rows + i + tile)
+            acc_ref[place] = weighted
+            lane = lax.broadcasted_iota(jnp.int32, (tile, head_dim), 1)
+            stat_ref[place] = jnp.where(lane == 0, top, den)
+
+
 def early_kernel(*refs):
     q_ref, gates_ref, mask_ref = refs[:3]
     acc_ref, stat_ref, column_ref, key_ref, value_ref, natural_ref = refs[-6:]
-    halves = refs[3:-6]
-    place_pairs(tuple(zip(halves[::2], halves[1::2])), key_ref, value_ref)
+    pieces = tuple(zip(refs[3:-6:2], refs[4:-6:2]))
     z = lax.axis_index("sp")
     block_rows = q_ref.shape[0]
-    head_dim = key_ref.shape[1]
-    heads = q_ref.shape[1] // head_dim
-    origins = [z] + [z - k for k in range(2, len(halves) // 2 + 1)]
+    heads = column_ref.shape[0]
     n_fs = lax.axis_size("fs")
     step = block_rows // (2 * n_fs)
     places = row_places(n_fs, step)
@@ -95,38 +119,22 @@
         natural_ref[...] = jnp.broadcast_to(row, (8, block_rows)).T
         for i, place in enumerate(places):
             column_ref[h, i * step : (i + 1) * step] = natural_ref[pl.ds(place, step)]
-    tile = block_rows // 2
-    masks = []
-    for i in range(0, 2 * n_fs, n_fs):
-        piece = [mask_ref[pl.ds(place, step)] for place in places[i : i + n_fs]]
-        masks.append(jnp.concatenate(piece, axis=0))
-    for h in range(heads):
-        for i in range(0, block_rows, tile):
-            queries = q_ref[i : i + tile, h * head_dim : (h + 1) * head_dim]
-            gate_q = column_ref[h, i : i + tile, 0:1]
-            scores = []
-            for k, origin in enumerate(origins):
-                gate_k = gate_row(gates_ref, h, heads, origin, block_rows)
-                keys = key_ref[k * block_rows : (k + 1) * block_rows]
-                s = score(queries, keys, gate_q, gate_k, origin)
-                scores.append(s + masks[i // tile] if k == 0 else s)
-            top = functools.reduce(jnp.maximum, scores)
-            top = jnp.max(top, axis=1, keepdims=True)
-            total = 0.0
-            weighted = 0.0
-            for k, s in enumerate(scores):
-                weight = jnp.exp2(s - top)
-                total = total + weight
-                weighted = weighted + jnp.dot(
-                    weight.astype(bf16),
-                    value_ref[k * block_rows : (k + 1) * block_rows],
-                    preferred_element_type=f32,
-                )
-            den = jnp.sum(total, axis=1, keepdims=True)
-            place = h * block_rows + i
-            acc_ref[place : place + tile] = weighted
-            lane = lax.broadcasted_iota(jnp.int32, (tile, head_dim), 1)
-            stat_ref[place : place + tile] = jnp.where(lane == 0, top, den)
+
+    def fold(count):
+        masks = []
+        for i in range(0, 2 * n_fs, n_fs):
+            piece = [mask_ref[pl.ds(place, step)] for place in places[i : i + n_fs]]
+            masks.append(jnp.concatenate(piece, axis=0))
+        rows = slice(0, count * block_rows)
+        place_pairs(pieces[:count], key_ref.at[rows], value_ref.at[rows])
+        blocks = []
+        for k in range(count):
+            rows = slice(k * block_rows, (k + 1) * block_rows)
+            blocks.append((key_ref[rows], value_ref[rows], z - k - min(k, 1)))
+        fold_blocks(q_ref, gates_ref, column_ref, blocks, masks, acc_ref, stat_ref)
+
+    for count in range(1, len(pieces) + 1):
+        pl.when(jnp.maximum(z, 1) == count)(functools.partial(fold, count))
 
 
 def row_places(n_fs, step):
@@ -186,30 +194,44 @@
 
 def mixer_kernel(first, *refs):
     q_ref, conv_ref, gates_ref, column_ref, acc_ref, stat_ref = refs[:6]
-    near_ref, far_ref, weight_ref, out_ref, key_ref, value_ref = refs[6:]
-    place_pairs(((near_ref, far_ref),), key_ref, value_ref)
+    near_ref, far_ref, weight_ref, out_ref, key_ref, value_ref, row_ref = refs[6:]
     block_rows = q_ref.shape[0]
     head_dim = key_ref.shape[1]
+    channels = conv_ref.shape[1]
     heads = q_ref.shape[1] // head_dim
     rows = out_ref.shape[0]
     origin = lax.axis_index("sp") - 1
-    outs = [conv_ref[first : first + rows]]
-    for h in range(heads):
-        queries = q_ref[first : first + rows, h * head_dim : (h + 1) * head_dim]
-        gate_q = column_ref[h, first : first + rows, 0:1]
-        gate_k = gate_row(gates_ref, h, heads, origin, block_rows)
-        s = score(queries, key_ref[...], gate_q, gate_k, origin)
-        place = h * block_rows + first
-        held_top = stat_ref[place : place + rows, 0:1]
-        held_den = stat_ref[place : place + rows, 1:2]
-        top = jnp.maximum(held_top, jnp.max(s, axis=1, keepdims=True))
-        fade = jnp.exp2(held_top - top)
-        weight = jnp.exp2(s - top)
-        den = held_den * fade + jnp.sum(weight, axis=1, keepdims=True)
-        weighted = jnp.dot(weight.astype(bf16), value_ref[...], preferred_element_type=f32)
-        held = acc_ref[place : place + rows]
-        outs.append(((held * fade + weighted) / den).astype(bf16))
-    out = jnp.dot(jnp.concatenate(outs, axis=1), weight_ref[...], preferred_element_type=f32)
+    row_ref[:, :channels] = conv_ref[first : first + rows]
+
+    def put(h, value):
+        place = channels + h * head_dim
+        row_ref[:, place : place + head_dim] = value.astype(bf16)
+
+    @pl.when(origin < 0)
+    def alone():
+        for h in range(heads):
+            place = h * block_rows + first
+            put(h, acc_ref[place : place + rows] / stat_ref[place : place + rows, 1:2])
+
+    @pl.when(origin >= 0)
+    def joined():
+        place_pairs(((near_ref, far_ref),), key_ref, value_ref)
+        for h in range(heads):
+            queries = q_ref[first : first + rows, h * head_dim : (h + 1) * head_dim]
+            gate_q = column_ref[h, first : first + rows, 0:1]
+            gate_k = gate_row(gates_ref, h, heads, origin, block_rows)
+            s = score(queries, key_ref[...], gate_q, gate_k, origin)
+            place = h * block_rows + first
+            held_top = stat_ref[place : place + rows, 0:1]
+            held_den = stat_ref[place : place + rows, 1:2]
+            top = jnp.maximum(held_top, jnp.max(s, axis=1, keepdims=True))
+            fade = jnp.exp2(held_top - top)
+            weight = jnp.exp2(s - top)
+            den = held_den * fade + jnp.sum(weight, axis=1, keepdims=True)
+            weighted = jnp.dot(weight.astype(bf16), value_ref[...], preferred_element_type=f32)
+            put(h, (acc_ref[place : place + rows] * fade + weighted) / den)
+
+    out = jnp.dot(row_ref[...], weight_ref[...], preferred_element_type=f32)
     out_ref[...] = out.astype(bf16)
 
 
@@ -257,7 +279,7 @@
         return lax.ppermute(x, "fs", [(i, i ^ k) for i in range(n_fs)])
 
     def raised(x, shift):
-        route = [(i, (i + shift) % n_sp) for i in range(n_sp) if i + shift < n_sp or RING]
+        route = [(i, (i + shift) % n_sp) for i in range(n_sp) if i + shift < n_sp or RING[shift]]
         return lax.ppermute(x, "sp", route)
 
     def call(kernel, out_shape, scratch, mib, *operands, in_specs=None, work=0):
@@ -363,7 +385,8 @@
         return call(
             functools.partial(mixer_kernel, first),
             shape_of(lane_rows, width),
-            [pltpu.VMEM((block_rows, head_dim), bf16)] * 2,
+            [pltpu.VMEM((block_rows, head_dim), bf16)] * 2
+            + [pltpu.VMEM((lane_rows, channels + heads * head_dim), bf16)],
             16,
             queries,
             conv_out,

time: 44.2 us -> 42.1 us (0.952)
  the two profiles are of different devices: /device:TPU:0 before, /device:TPU:27 now
where the time goes in v3:
time: 42.1 us; the launch traced here: 41.8 us
  waiting for transfers between devices  17.4 us (41%)
  starting transfers between devices  15.7 us (37%)
  Pallas kernels  6.81 us (16%)
  local copies, waits for them, and re-layouts  1.66 us (4%)
    ppermute x6, waiting for transfers between devices, crossed(): return lax.ppermute(x, 'fs', [(i, i ^ k) for i in range(n_fs)])  11.4 us
    ppermute x9, starting transfers between devices, swapped(): return lax.ppermute(x, 'tp', [(0, 1), (1, 0)])  8.72 us
    pallas_call x11, Pallas kernels, call(): pl.pallas_call(kernel, out_shape=out_shape, scratch_shapes=scratch, compi...  6.81 us
    ppermute x6, starting transfers between devices, crossed(): return lax.ppermute(x, 'fs', [(i, i ^ k) for i in range(n_fs)])  5.43 us
    ppermute x3, waiting for transfers between devices, raised(): return lax.ppermute(x, 'sp', route)  4.87 us
    unnamed x24, local copies, waits for them, and re-layouts  1.66 us
    ppermute x3, starting transfers between devices, raised(): return lax.ppermute(x, 'sp', route)  1.57 us
    ppermute x9, waiting for transfers between devices, swapped(): return lax.ppermute(x, 'tp', [(0, 1), (1, 0)])  1.1 us
  transfers between devices with their start and end apart: 18, of which 8 were waited for; matrix products, arithmetic and copies ran while one was open for 0% of the time, Pallas kernels for 11%

profile of v3, /device:TPU:27, one launch (start us, length us, event | category | flops | bytes accessed | tf_op | source)
XLA Modules:
  0.0 41.8 jit_solution(13400981311668990834)
XLA Ops:
  0.0 0.9 %copy-done.8 = bf16[32,2048]{1,0:T(8,128)(2,1)S(1)} copy-done((bf16[32,2048]{1,0:T(8,128)(2,1)S(1)}, bf16[32,2048]{1,0:T(8,128)(2,1)}, u32[]{:S(2)}) %copy-start.8) | copy-done | bytes 131096
  0.9 0.7 %copy-done.10 = f32[2048]{0:T(1024)S(1)} copy-done((f32[2048]{0:T(1024)S(1)}, f32[2048]{0:T(1024)}, u32[]{:S(2)}) %copy-start.10) | copy-done | bytes 8216
  1.6 0.1 shard_map.118.refs_0_
  1.7 1.3 %collective-permute-start.2 = (bf16[32,2048]{1,0:T(8,128)(2,1)S(1)}, bf16[32,2048]{1,0:T(8,128)(2,1)S(1)}, u32[]{:S(2)}, u32[]{:S(2)}) collective-permute-start(bf16[32,2048]{1,0:T(8,128)(2,1)S(1)} %shard_map.118.refs_0_), channel_id=1, source_target_pairs={{0,6},{2,4},{4,2},{6,0},{1,7},{3,5},{5,3},{7,1},{8,14},{10,12},{12... | collective-permute-start | bytes 393224 | tf_op jit(solution)/shard_map/ppermute | solution.py:279
  3.0 0.2 collective-permute-start.1
  3.2 1.2 %collective-permute-start = (bf16[32,2048]{1,0:T(8,128)(2,1)S(1)}, bf16[32,2048]{1,0:T(8,128)(2,1)S(1)}, u32[]{:S(2)}, u32[]{:S(2)}) collective-permute-start(bf16[32,2048]{1,0:T(8,128)(2,1)S(1)} %shard_map.118.refs_0_), channel_id=1, source_target_pairs={{0,2},{2,0},{4,6},{6,4},{1,3},{3,1},{5,7},{7,5},{8,10},{10,8},{12,... | collective-permute-start | bytes 393224 | tf_op jit(solution)/shard_map/ppermute | solution.py:279
  4.5 1.5 %collective-permute-start.3 = (bf16[32,2048]{1,0:T(8,128)(2,1)S(1)}, bf16[32,2048]{1,0:T(8,128)(2,1)S(1)}, u32[]{:S(2)}, u32[]{:S(2)}) collective-permute-start(bf16[32,2048]{1,0:T(8,128)(2,1)S(1)} %shard_map.118.refs_0_), channel_id=1, source_target_pairs={{0,1},{1,0},{2,3},{3,2},{4,5},{5,4},{6,7},{7,6},{8,9},{9,8},{10,11... | collective-permute-start | bytes 393224 | tf_op jit(solution)/shard_map/ppermute | solution.py:276
  6.0 1.1 %collective-permute-done.2.refs_3_ = bf16[32,2048]{1,0:T(8,128)(2,1)S(1)} collective-permute-done((bf16[32,2048]{1,0:T(8,128)(2,1)S(1)}, bf16[32,2048]{1,0:T(8,128)(2,1)S(1)}, u32[]{:S(2)}, u32[]{:S(2)}) %collective-permute-start.2) | collective-permute-done | bytes 131104 | tf_op jit(solution)/shard_map/ppermute | solution.py:279
  7.1 3.8 %collective-permute-done.1.refs_2_ = bf16[32,2048]{1,0:T(8,128)(2,1)S(1)} collective-permute-done((bf16[32,2048]{1,0:T(8,128)(2,1)S(1)}, bf16[32,2048]{1,0:T(8,128)(2,1)S(1)}, u32[]{:S(2)}, u32[]{:S(2)}) %collective-permute-start.1) | collective-permute-done | bytes 131104 | tf_op jit(solution)/shard_map/ppermute | solution.py:279
  10.9 0.3 shard_map.119.refs_12_.refs_3_
  11.3 0.2 collective-permute-start.11
  11.6 1.1 %collective-permute-start.6 = (bf16[32,2048]{1,0:T(8,128)(2,1)S(1)}, bf16[32,2048]{1,0:T(8,128)(2,1)S(1)}, u32[]{:S(2)}, u32[]{:S(2)}) collective-permute-start(bf16[32,2048]{1,0:T(8,128)(2,1)S(1)} %collective-permute-done.2.refs_3_), channel_id=1, source_target_pairs={{0,1},{1,0},{2,3},{3,2},{4,5},{5,4},{6,7},{7,6},{8,9},{9,8},{10,11... | collective-permute-start | bytes 393224 | tf_op jit(solution)/shard_map/ppermute | solution.py:276
  12.7 0.5 %collective-permute-start.4 = (bf16[32,2048]{1,0:T(8,128)(2,1)S(1)}, bf16[32,2048]{1,0:T(8,128)(2,1)S(1)}, u32[]{:S(2)}, u32[]{:S(2)}) collective-permute-start(bf16[32,2048]{1,0:T(8,128)(2,1)S(1)} %collective-permute-done.refs_1_), channel_id=1, source_target_pairs={{0,1},{1,0},{2,3},{3,2},{4,5},{5,4},{6,7},{7,6},{8,9},{9,8},{10,11... | collective-permute-start | bytes 393224 | tf_op jit(solution)/shard_map/ppermute | solution.py:276
  13.5 2.8 %collective-permute-done.11.refs_7_ = bf16[128,256]{1,0:T(8,128)(2,1)S(1)} collective-permute-done((bf16[128,256]{1,0:T(8,128)(2,1)S(1)}, bf16[128,256]{1,0:T(8,128)(2,1)S(1)}, u32[]{:S(2)}, u32[]{:S(2)}) %collective-permute-start.11) | collective-permute-done | bytes 65568 | tf_op jit(solution)/shard_map/ppermute | solution.py:283
  16.3 2.2 %collective-permute-start.8 = (bf16[128,256]{1,0:T(8,128)(2,1)S(1)}, bf16[128,256]{1,0:T(8,128)(2,1)S(1)}, u32[]{:S(2)}, u32[]{:S(2)}) collective-permute-start(bf16[128,256]{1,0:T(8,128)(2,1)S(1)} %shard_map.119.refs_12_.refs_3_), channel_id=1, source_target_pairs={{0,1},{1,0},{2,3},{3,2},{4,5},{5,4},{6,7},{7,6},{8,9},{9,8},{10,11... | collective-permute-start | bytes 196616 | tf_op jit(solution)/shard_map/ppermute | solution.py:276
  18.5 1.3 %collective-permute-start.12 = (bf16[128,256]{1,0:T(8,128)(2,1)S(1)}, bf16[128,256]{1,0:T(8,128)(2,1)S(1)}, u32[]{:S(2)}, u32[]{:S(2)}) collective-permute-start(bf16[128,256]{1,0:T(8,128)(2,1)S(1)} %collective-permute-done.11.refs_7_), channel_id=1, source_target_pairs={{0,1},{1,0},{2,3},{3,2},{4,5},{5,4},{6,7},{7,6},{8,9},{9,8},{10,11... | collective-permute-start | bytes 196616 | tf_op jit(solution)/shard_map/ppermute | solution.py:276
  19.8 1.0 %shard_map.120 = (bf16[256,256]{1,0:T(8,128)(2,1)S(1)}, bf16[256,128]{1,0:T(8,128)(2,1)S(1)}, bf16[256,128]{1,0:T(8,128)(2,1)S(1)}, bf16[144,256]{1,0:T(8,128)(2,1)S(1)}) custom-call(bf16[32,2048]{1,0:T(8,128)(2,1)S(1)} %shard_map.118.refs_0_, bf16[32,2048]{1,0:T(8,128)(2,1)S(1)} %collective-permute-done.refs_1_, ...), custom_call_target="tpu_custom_call" | custom-call | flops 2000000000 | tf_op jit(solution)/shard_map/pallas_call | solution.py:291
  20.8 1.3 %collective-permute-start.7 = (bf16[144,256]{1,0:T(8,128)(2,1)S(1)}, bf16[144,256]{1,0:T(8,128)(2,1)S(1)}, u32[]{:S(2)}, u32[]{:S(2)}) collective-permute-start(bf16[144,256]{1,0:T(8,128)(2,1)S(1)} %get-tuple-element.19), channel_id=1, source_target_pairs={{0,8},{8,16},{16,24},{1,9},{9,17},{17,25},{2,10},{10,18},{18,26},{... | collective-permute-start | bytes 221192 | tf_op jit(solution)/shard_map/ppermute | solution.py:283
  22.2 1.7 %shard_map.123 = (f32[512,128]{1,0:T(8,128)S(1)}, f32[512,128]{1,0:T(8,128)S(1)}, f32[2,256,8]{2,1,0:T(8,128)S(1)}) custom-call(bf16[256,256]{1,0:T(8,128)(2,1)S(1)} %get-tuple-element.16.refs_0_, f32[16,1024]{1,0:T(8,128)S(1)} %copy-done.9, f32[256,256]{1,0:T(8,128)S(1)} %shard_map.122.refs_2_, bf16[128,256]{1,0:T(8,128)(2,1)S(1)} %shard_map.119.refs_12_.refs_3_, ...), custom_call_target="tpu_custom_call" | custom-call | flops 2000000000 | tf_op jit(solution)/shard_map/pallas_call | solution.py:291
  23.9 2.0 %collective-permute-done.7.risen_ref.refs_6_ = bf16[144,256]{1,0:T(8,128)(2,1)S(1)} collective-permute-done((bf16[144,256]{1,0:T(8,128)(2,1)S(1)}, bf16[144,256]{1,0:T(8,128)(2,1)S(1)}, u32[]{:S(2)}, u32[]{:S(2)}) %collective-permute-start.7) | collective-permute-done | bytes 73760 | tf_op jit(solution)/shard_map/ppermute | solution.py:283
  25.9 1.6 %collective-permute-start.13 = (bf16[144,256]{1,0:T(8,128)(2,1)S(1)}, bf16[144,256]{1,0:T(8,128)(2,1)S(1)}, u32[]{:S(2)}, u32[]{:S(2)}) collective-permute-start(bf16[144,256]{1,0:T(8,128)(2,1)S(1)} %collective-permute-done.7.risen_ref.refs_6_), channel_id=1, source_target_pairs={{0,1},{1,0},{2,3},{3,2},{4,5},{5,4},{6,7},{7,6},{8,9},{9,8},{10,11... | collective-permute-start | bytes 221192 | tf_op jit(solution)/shard_map/ppermute | solution.py:276
  27.7 0.8 %collective-permute-done.13.refs_7_ = bf16[144,256]{1,0:T(8,128)(2,1)S(1)} collective-permute-done((bf16[144,256]{1,0:T(8,128)(2,1)S(1)}, bf16[144,256]{1,0:T(8,128)(2,1)S(1)}, u32[]{:S(2)}, u32[]{:S(2)}) %collective-permute-start.13) | collective-permute-done | bytes 73760 | tf_op jit(solution)/shard_map/ppermute | solution.py:276
  28.5 1.3 %shard_map.126 = bf16[128,2048]{1,0:T(8,128)(2,1)S(1)} custom-call(bf16[256,256]{1,0:T(8,128)(2,1)S(1)} %get-tuple-element.16.refs_0_, bf16[256,128]{1,0:T(8,128)(2,1)S(1)} %shard_map.121.refs_1_, f32[16,1024]{1,0:T(8,128)S(1)} %copy-done.9, f32[2,256,8]{2,1,0:T(8,128)S(1)} %get-tuple-element.20.refs_3_, f32[512,128]{1,0:T(8,128)S(1)} %get-tuple-element.21.refs_4_, ...), custom_call_target="tpu_custom_call" | custom-call | flops 2000000000 | tf_op jit(solution)/shard_map/pallas_call | solution.py:291
  29.8 0.4 collective-permute-start.14
  30.2 1.3 %shard_map.125.keep_ref = bf16[128,2048]{1,0:T(8,128)(2,1)S(1)} custom-call(bf16[256,256]{1,0:T(8,128)(2,1)S(1)} %get-tuple-element.16.refs_0_, bf16[256,128]{1,0:T(8,128)(2,1)S(1)} %shard_map.121.refs_1_, f32[16,1024]{1,0:T(8,128)S(1)} %copy-done.9, f32[2,256,8]{2,1,0:T(8,128)S(1)} %get-tuple-element.20.refs_3_, f32[512,128]{1,0:T(8,128)S(1)} %get-tuple-element.21.refs_4_, ...), custom_call_target="tpu_custom_call" | custom-call | flops 2000000000 | tf_op jit(solution)/shard_map/pallas_call | solution.py:291
  31.6 0.2 collective-permute-done.14.got_ref
  31.9 1.3 %collective-permute-start.15 = (bf16[32,2048]{1,0:T(8,128)(2,1)S(1)}, bf16[32,2048]{1,0:T(8,128)(2,1)S(1)}, u32[]{:S(2)}, u32[]{:S(2)}) collective-permute-start(bf16[32,2048]{1,0:T(8,128)(2,1)S(1)} %get-tuple-element.23), channel_id=1, source_target_pairs={{0,6},{2,4},{4,2},{6,0},{1,7},{3,5},{5,3},{7,1},{8,14},{10,12},{12... | collective-permute-start | bytes 393224 | tf_op jit(solution)/shard_map/ppermute | solution.py:279
  33.2 0.2 collective-permute-start.16
  33.4 1.2 %collective-permute-start.17 = (bf16[32,2048]{1,0:T(8,128)(2,1)S(1)}, bf16[32,2048]{1,0:T(8,128)(2,1)S(1)}, u32[]{:S(2)}, u32[]{:S(2)}) collective-permute-start(bf16[32,2048]{1,0:T(8,128)(2,1)S(1)} %get-tuple-element.25), channel_id=1, source_target_pairs={{0,2},{2,0},{4,6},{6,4},{1,3},{3,1},{5,7},{7,5},{8,10},{10,8},{12,... | collective-permute-start | bytes 393224 | tf_op jit(solution)/shard_map/ppermute | solution.py:279
  34.6 3.0 %collective-permute-done.15.refs_0_ = bf16[32,2048]{1,0:T(8,128)(2,1)S(1)} collective-permute-done((bf16[32,2048]{1,0:T(8,128)(2,1)S(1)}, bf16[32,2048]{1,0:T(8,128)(2,1)S(1)}, u32[]{:S(2)}, u32[]{:S(2)}) %collective-permute-start.15) | collective-permute-done | bytes 131104 | tf_op jit(solution)/shard_map/ppermute | solution.py:279
  37.6 3.5 %collective-permute-done.16.refs_1_ = bf16[32,2048]{1,0:T(8,128)(2,1)S(1)} collective-permute-done((bf16[32,2048]{1,0:T(8,128)(2,1)S(1)}, bf16[32,2048]{1,0:T(8,128)(2,1)S(1)}, u32[]{:S(2)}, u32[]{:S(2)}) %collective-permute-start.16) | collective-permute-done | bytes 131104 | tf_op jit(solution)/shard_map/ppermute | solution.py:279
  41.1 0.7 %shard_map.128 = bf16[32,2048]{1,0:T(8,128)(2,1)} custom-call(bf16[32,2048]{1,0:T(8,128)(2,1)S(1)} %collective-permute-done.15.refs_0_, bf16[32,2048]{1,0:T(8,128)(2,1)S(1)} %collective-permute-done.16.refs_1_, bf16[32,2048]{1,0:T(8,128)(2,1)S(1)} %collective-permute-done.17.refs_2_, f32[32,2048]{1,0:T(8,128)S(1)} %get-tuple-element.26.refs_3_), custom_call_target="tpu_custom_call" | custom-call | tf_op jit(solution)/shard_map/pallas_call | solution.py:291
  (39 shorter events, 0.5 us)
Async XLA Ops:
  0.0 0.9 %copy-start.8 = (bf16[32,2048]{1,0:T(8,128)(2,1)S(1)}, bf16[32,2048]{1,0:T(8,128)(2,1)}, u32[]{:S(2)}) copy-start(bf16[32,2048]{1,0:T(8,128)(2,1)} %tokens_ref.1) | copy-start | bytes 393220
  0.9 0.7 %copy-start.10 = (f32[2048]{0:T(1024)S(1)}, f32[2048]{0:T(1024)}, u32[]{:S(2)}) copy-start(f32[2048]{0:T(1024)} %param.13) | copy-start | bytes 24580
  1.6 9.3 %copy-start.3 = (bf16[2048,128]{1,0:T(8,128)(2,1)S(1)}, bf16[2048,128]{1,0:T(8,128)(2,1)}, u32[]{:S(2)}) copy-start(bf16[2048,128]{1,0:T(8,128)(2,1)} %refs_4_.1) | copy-start | bytes 1572868
  1.6 9.3 %copy-start.4 = (bf16[2048,128]{1,0:T(8,128)(2,1)S(1)}, bf16[2048,128]{1,0:T(8,128)(2,1)}, u32[]{:S(2)}) copy-start(bf16[2048,128]{1,0:T(8,128)(2,1)} %refs_5_.1) | copy-start | bytes 1572868
  1.7 5.3 %collective-permute-start.2 = (bf16[32,2048]{1,0:T(8,128)(2,1)S(1)}, bf16[32,2048]{1,0:T(8,128)(2,1)S(1)}, u32[]{:S(2)}, u32[]{:S(2)}) collective-permute-start(bf16[32,2048]{1,0:T(8,128)(2,1)S(1)} %shard_map.118.refs_0_), channel_id=1, source_target_pairs={{0,6},{2,4},{4,2},{6,0},{1,7},{3,5},{5,3},{7,1},{8,14},{10,12},{12... | collective-permute-start | bytes 393224 | tf_op jit(solution)/shard_map/ppermute | solution.py:279
  3.0 7.9 %collective-permute-start.1 = (bf16[32,2048]{1,0:T(8,128)(2,1)S(1)}, bf16[32,2048]{1,0:T(8,128)(2,1)S(1)}, u32[]{:S(2)}, u32[]{:S(2)}) collective-permute-start(bf16[32,2048]{1,0:T(8,128)(2,1)S(1)} %shard_map.118.refs_0_), channel_id=1, source_target_pairs={{0,4},{2,6},{4,0},{6,2},{1,5},{3,7},{5,1},{7,3},{8,12},{10,14},{12... | collective-permute-start | bytes 393224 | tf_op jit(solution)/shard_map/ppermute | solution.py:279
  3.2 7.7 %collective-permute-start = (bf16[32,2048]{1,0:T(8,128)(2,1)S(1)}, bf16[32,2048]{1,0:T(8,128)(2,1)S(1)}, u32[]{:S(2)}, u32[]{:S(2)}) collective-permute-start(bf16[32,2048]{1,0:T(8,128)(2,1)S(1)} %shard_map.118.refs_0_), channel_id=1, source_target_pairs={{0,2},{2,0},{4,6},{6,4},{1,3},{3,1},{5,7},{7,5},{8,10},{10,8},{12,... | collective-permute-start | bytes 393224 | tf_op jit(solution)/shard_map/ppermute | solution.py:279
  4.5 8.3 %collective-permute-start.3 = (bf16[32,2048]{1,0:T(8,128)(2,1)S(1)}, bf16[32,2048]{1,0:T(8,128)(2,1)S(1)}, u32[]{:S(2)}, u32[]{:S(2)}) collective-permute-start(bf16[32,2048]{1,0:T(8,128)(2,1)S(1)} %shard_map.118.refs_0_), channel_id=1, source_target_pairs={{0,1},{1,0},{2,3},{3,2},{4,5},{5,4},{6,7},{7,6},{8,9},{9,8},{10,11... | collective-permute-start | bytes 393224 | tf_op jit(solution)/shard_map/ppermute | solution.py:276
  11.3 2.0 %copy-start = (bf16[256,2048]{1,0:T(8,128)(2,1)S(1)}, bf16[256,2048]{1,0:T(8,128)(2,1)}, u32[]{:S(2)}) copy-start(bf16[256,2048]{1,0:T(8,128)(2,1)} %low_ref.1) | copy-start | bytes 3145732
  11.3 2.0 %copy-start.1 = (bf16[128,2048]{1,0:T(8,128)(2,1)S(1)}, bf16[128,2048]{1,0:T(8,128)(2,1)}, u32[]{:S(2)}) copy-start(bf16[128,2048]{1,0:T(8,128)(2,1)} %top_ref.1) | copy-start | bytes 1572868
  11.3 5.0 %collective-permute-start.11 = (bf16[128,256]{1,0:T(8,128)(2,1)S(1)}, bf16[128,256]{1,0:T(8,128)(2,1)S(1)}, u32[]{:S(2)}, u32[]{:S(2)}) collective-permute-start(bf16[128,256]{1,0:T(8,128)(2,1)S(1)} %shard_map.119.refs_12_.refs_3_), channel_id=1, source_target_pairs={{0,24},{8,0},{16,8},{24,16},{1,25},{9,1},{17,9},{25,17},{2,26},{10... | collective-permute-start | bytes 196616 | tf_op jit(solution)/shard_map/ppermute | solution.py:283
  11.5 6.9 %collective-permute-start.9 = (bf16[128,256]{1,0:T(8,128)(2,1)S(1)}, bf16[128,256]{1,0:T(8,128)(2,1)S(1)}, u32[]{:S(2)}, u32[]{:S(2)}) collective-permute-start(bf16[128,256]{1,0:T(8,128)(2,1)S(1)} %shard_map.119.refs_12_.refs_3_), channel_id=1, source_target_pairs={{0,16},{8,24},{16,0},{24,8},{1,17},{9,25},{17,1},{25,9},{2,18},{10... | collective-permute-start | bytes 196616 | tf_op jit(solution)/shard_map/ppermute | solution.py:283
  11.6 8.2 %collective-permute-start.6 = (bf16[32,2048]{1,0:T(8,128)(2,1)S(1)}, bf16[32,2048]{1,0:T(8,128)(2,1)S(1)}, u32[]{:S(2)}, u32[]{:S(2)}) collective-permute-start(bf16[32,2048]{1,0:T(8,128)(2,1)S(1)} %collective-permute-done.2.refs_3_), channel_id=1, source_target_pairs={{0,1},{1,0},{2,3},{3,2},{4,5},{5,4},{6,7},{7,6},{8,9},{9,8},{10,11... | collective-permute-start | bytes 393224 | tf_op jit(solution)/shard_map/ppermute | solution.py:276
  12.7 7.1 %collective-permute-start.5 = (bf16[32,2048]{1,0:T(8,128)(2,1)S(1)}, bf16[32,2048]{1,0:T(8,128)(2,1)S(1)}, u32[]{:S(2)}, u32[]{:S(2)}) collective-permute-start(bf16[32,2048]{1,0:T(8,128)(2,1)S(1)} %collective-permute-done.1.refs_2_), channel_id=1, source_target_pairs={{0,1},{1,0},{2,3},{3,2},{4,5},{5,4},{6,7},{7,6},{8,9},{9,8},{10,11... | collective-permute-start | bytes 393224 | tf_op jit(solution)/shard_map/ppermute | solution.py:276
  12.7 7.1 %collective-permute-start.4 = (bf16[32,2048]{1,0:T(8,128)(2,1)S(1)}, bf16[32,2048]{1,0:T(8,128)(2,1)S(1)}, u32[]{:S(2)}, u32[]{:S(2)}) collective-permute-start(bf16[32,2048]{1,0:T(8,128)(2,1)S(1)} %collective-permute-done.refs_1_), channel_id=1, source_target_pairs={{0,1},{1,0},{2,3},{3,2},{4,5},{5,4},{6,7},{7,6},{8,9},{9,8},{10,11... | collective-permute-start | bytes 393224 | tf_op jit(solution)/shard_map/ppermute | solution.py:276
  13.3 6.5 %copy-start.2 = (bf16[2048,256]{1,0:T(8,128)(2,1)S(1)}, bf16[2048,256]{1,0:T(8,128)(2,1)}, u32[]{:S(2)}) copy-start(bf16[2048,256]{1,0:T(8,128)(2,1)} %refs_8_.1) | copy-start | bytes 3145732
  13.3 6.5 %copy-start.5 = (bf16[2048,128]{1,0:T(8,128)(2,1)S(1)}, bf16[2048,128]{1,0:T(8,128)(2,1)}, u32[]{:S(2)}) copy-start(bf16[2048,128]{1,0:T(8,128)(2,1)} %refs_9_.1) | copy-start | bytes 1572868
  13.3 6.5 %copy-start.6 = (bf16[2048,128]{1,0:T(8,128)(2,1)S(1)}, bf16[2048,128]{1,0:T(8,128)(2,1)}, u32[]{:S(2)}) copy-start(bf16[2048,128]{1,0:T(8,128)(2,1)} %refs_10_.1) | copy-start | bytes 1572868
  13.3 6.5 %copy-start.7 = (bf16[2048,128]{1,0:T(8,128)(2,1)S(1)}, bf16[2048,128]{1,0:T(8,128)(2,1)}, u32[]{:S(2)}) copy-start(bf16[2048,128]{1,0:T(8,128)(2,1)} %refs_11_.1) | copy-start | bytes 1572868
  13.5 8.7 %copy-start.9 = (f32[16,1024]{1,0:T(8,128)S(1)}, f32[16,1024]{1,0:T(8,128)}, u32[]{:S(2)}) copy-start(f32[16,1024]{1,0:T(8,128)} %refs_2_.3) | copy-start | bytes 196612
  16.3 5.8 %collective-permute-start.8 = (bf16[128,256]{1,0:T(8,128)(2,1)S(1)}, bf16[128,256]{1,0:T(8,128)(2,1)S(1)}, u32[]{:S(2)}, u32[]{:S(2)}) collective-permute-start(bf16[128,256]{1,0:T(8,128)(2,1)S(1)} %shard_map.119.refs_12_.refs_3_), channel_id=1, source_target_pairs={{0,1},{1,0},{2,3},{3,2},{4,5},{5,4},{6,7},{7,6},{8,9},{9,8},{10,11... | collective-permute-start | bytes 196616 | tf_op jit(solution)/shard_map/ppermute | solution.py:276
  18.5 3.7 %collective-permute-start.12 = (bf16[128,256]{1,0:T(8,128)(2,1)S(1)}, bf16[128,256]{1,0:T(8,128)(2,1)S(1)}, u32[]{:S(2)}, u32[]{:S(2)}) collective-permute-start(bf16[128,256]{1,0:T(8,128)(2,1)S(1)} %collective-permute-done.11.refs_7_), channel_id=1, source_target_pairs={{0,1},{1,0},{2,3},{3,2},{4,5},{5,4},{6,7},{7,6},{8,9},{9,8},{10,11... | collective-permute-start | bytes 196616 | tf_op jit(solution)/shard_map/ppermute | solution.py:276
  19.8 2.4 %collective-permute-start.10 = (bf16[128,256]{1,0:T(8,128)(2,1)S(1)}, bf16[128,256]{1,0:T(8,128)(2,1)S(1)}, u32[]{:S(2)}, u32[]{:S(2)}) collective-permute-start(bf16[128,256]{1,0:T(8,128)(2,1)S(1)} %collective-permute-done.9.refs_5_), channel_id=1, source_target_pairs={{0,1},{1,0},{2,3},{3,2},{4,5},{5,4},{6,7},{7,6},{8,9},{9,8},{10,11... | collective-permute-start | bytes 196616 | tf_op jit(solution)/shard_map/ppermute | solution.py:276
  20.8 5.1 %collective-permute-start.7 = (bf16[144,256]{1,0:T(8,128)(2,1)S(1)}, bf16[144,256]{1,0:T(8,128)(2,1)S(1)}, u32[]{:S(2)}, u32[]{:S(2)}) collective-permute-start(bf16[144,256]{1,0:T(8,128)(2,1)S(1)} %get-tuple-element.19), channel_id=1, source_target_pairs={{0,8},{8,16},{16,24},{1,9},{9,17},{17,25},{2,10},{10,18},{18,26},{... | collective-permute-start | bytes 221192 | tf_op jit(solution)/shard_map/ppermute | solution.py:283
  22.2 5.4 %copy-start.11 = (bf16[3,1024]{1,0:T(4,128)(2,1)S(1)}, bf16[3,1024]{1,0:T(4,128)(2,1)}, u32[]{:S(2)}) copy-start(bf16[3,1024]{1,0:T(4,128)(2,1)} %taps_ref.1) | copy-start | bytes 18436
  25.9 2.6 %collective-permute-start.13 = (bf16[144,256]{1,0:T(8,128)(2,1)S(1)}, bf16[144,256]{1,0:T(8,128)(2,1)S(1)}, u32[]{:S(2)}, u32[]{:S(2)}) collective-permute-start(bf16[144,256]{1,0:T(8,128)(2,1)S(1)} %collective-permute-done.7.risen_ref.refs_6_), channel_id=1, source_target_pairs={{0,1},{1,0},{2,3},{3,2},{4,5},{5,4},{6,7},{7,6},{8,9},{9,8},{10,11... | collective-permute-start | bytes 221192 | tf_op jit(solution)/shard_map/ppermute | solution.py:276
  29.8 2.0 %collective-permute-start.14 = (bf16[128,2048]{1,0:T(8,128)(2,1)S(1)}, bf16[128,2048]{1,0:T(8,128)(2,1)S(1)}, u32[]{:S(2)}, u32[]{:S(2)}) collective-permute-start(bf16[128,2048]{1,0:T(8,128)(2,1)S(1)} %shard_map.126), channel_id=1, source_target_pairs={{0,1},{1,0},{2,3},{3,2},{4,5},{5,4},{6,7},{7,6},{8,9},{9,8},{10,11... | collective-permute-start | bytes 1572872 | tf_op jit(solution)/shard_map/ppermute | solution.py:276
  31.9 5.7 %collective-permute-start.15 = (bf16[32,2048]{1,0:T(8,128)(2,1)S(1)}, bf16[32,2048]{1,0:T(8,128)(2,1)S(1)}, u32[]{:S(2)}, u32[]{:S(2)}) collective-permute-start(bf16[32,2048]{1,0:T(8,128)(2,1)S(1)} %get-tuple-element.23), channel_id=1, source_target_pairs={{0,6},{2,4},{4,2},{6,0},{1,7},{3,5},{5,3},{7,1},{8,14},{10,12},{12... | collective-permute-start | bytes 393224 | tf_op jit(solution)/shard_map/ppermute | solution.py:279
  33.2 7.9 %collective-permute-start.16 = (bf16[32,2048]{1,0:T(8,128)(2,1)S(1)}, bf16[32,2048]{1,0:T(8,128)(2,1)S(1)}, u32[]{:S(2)}, u32[]{:S(2)}) collective-permute-start(bf16[32,2048]{1,0:T(8,128)(2,1)S(1)} %get-tuple-element.24), channel_id=1, source_target_pairs={{0,4},{2,6},{4,0},{6,2},{1,5},{3,7},{5,1},{7,3},{8,12},{10,14},{12... | collective-permute-start | bytes 393224 | tf_op jit(solution)/shard_map/ppermute | solution.py:279
  33.4 7.7 %collective-permute-start.17 = (bf16[32,2048]{1,0:T(8,128)(2,1)S(1)}, bf16[32,2048]{1,0:T(8,128)(2,1)S(1)}, u32[]{:S(2)}, u32[]{:S(2)}) collective-permute-start(bf16[32,2048]{1,0:T(8,128)(2,1)S(1)} %get-tuple-element.25), channel_id=1, source_target_pairs={{0,2},{2,0},{4,6},{6,4},{1,3},{3,1},{5,7},{7,5},{8,10},{10,8},{12,... | collective-permute-start | bytes 393224 | tf_op jit(solution)/shard_map/ppermute | solution.py:279

commit v4 on v3

--- a/solution.py
+++ b/solution.py
@@ -77,37 +77,61 @@
     return s * scale + gate_q - jnp.where(origin >= 0, gate_k, -masked_score)
 
 
-def fold_blocks(q_ref, gates_ref, column_ref, blocks, masks, acc_ref, stat_ref):
+def faded(s, top):
+    return jnp.exp2(s - jnp.concatenate([top] * (s.shape[1] // top.shape[1]), axis=1))
+
+
+def fold_blocks(q_ref, gates_ref, column_ref, blocks, masks, held, outs):
+    acc_ref, top_ref, den_ref = outs
     block_rows = q_ref.shape[0]
     head_dim = acc_ref.shape[1]
     heads = q_ref.shape[1] // head_dim
     tile = block_rows // 2
-    for h in range(heads):
-        for i in range(0, block_rows, tile):
-            queries = q_ref[i : i + tile, h * head_dim : (h + 1) * head_dim]
-            gate_q = column_ref[h, i : i + tile, 0:1]
-            scores = []
-            for k, (keys, values, origin) in enumerate(blocks):
-                gate_k = gate_row(gates_ref, h, heads, origin, block_rows)
-                s = score(queries, keys, gate_q, gate_k, origin)
-                scores.append(s if k else s + masks[i // tile])
-            top = jnp.max(functools.reduce(jnp.maximum, scores), axis=1, keepdims=True)
-            weights = [jnp.exp2(s - top) for s in scores]
-            den = jnp.sum(sum(weights), axis=1, keepdims=True)
-            weighted = sum(
-                jnp.dot(weight.astype(bf16), values, preferred_element_type=f32)
-                for weight, (keys, values, origin) in zip(weights, blocks)
-            )
-            place = slice(h * block_rows + i, h * block_rows + i + tile)
-            acc_ref[place] = weighted
-            lane = lax.broadcasted_iota(jnp.int32, (tile, head_dim), 1)
-            stat_ref[place] = jnp.where(lane == 0, top, den)
+    tiles = [(h, i) for h in range(heads) for i in range(0, block_rows, tile)]
+    places = [slice(h * block_rows + i, h * block_rows + i + tile) for h, i in tiles]
+    scores = []
+    for h, i in tiles:
+        queries = q_ref[i : i + tile, h * head_dim : (h + 1) * head_dim]
+        gate_q = column_ref[h, i : i + tile, 0:1]
+        row = []
+        for keys, values, origin in blocks:
+            gate_k = gate_row(gates_ref, h, heads, origin, block_rows)
+            s = score(queries, keys, gate_q, gate_k, origin)
+            row.append(s + masks[i // tile] if masks else s)
+        scores.append(row)
+    wide = (tile, head_dim)
+    tops = [
+        jnp.broadcast_to(
+            jnp.max(functools.reduce(jnp.maximum, row), axis=1, keepdims=True), wide
+        )
+        for row in scores
+    ]
+    if held:
+        held_tops = [held[1][place] for place in places]
+        tops = [jnp.maximum(top, held_top) for top, held_top in zip(tops, held_tops)]
+        fades = [jnp.exp2(held_top - top) for top, held_top in zip(tops, held_tops)]
+    weights = [[faded(s, top) for s in row] for row, top in zip(scores, tops)]
+    dens = [
+        jnp.broadcast_to(jnp.sum(sum(row), axis=1, keepdims=True), wide) for row in weights
+    ]
+    for n, place in enumerate(places):
+        total = sum(
+            jnp.dot(weight.astype(bf16), values, preferred_element_type=f32)
+            for weight, (keys, values, origin) in zip(weights[n], blocks)
+        )
+        den = dens[n]
+        if held:
+            total = total + held[0][place] * fades[n]
+            den = den + held[2][place] * fades[n]
+        acc_ref[place] = total
+        top_ref[place] = tops[n]
+        den_ref[place] = den
 
 
 def early_kernel(*refs):
-    q_ref, gates_ref, mask_ref = refs[:3]
-    acc_ref, stat_ref, column_ref, key_ref, value_ref, natural_ref = refs[-6:]
-    pieces = tuple(zip(refs[3:-6:2], refs[4:-6:2]))
+    q_ref, gates_ref, mask_ref, near_ref, far_ref = refs[:5]
+    outs, (column_ref, key_ref, value_ref, natural_ref) = refs[5:8], refs[8:]
+    place_pairs(((near_ref, far_ref),), key_ref, value_ref)
     z = lax.axis_index("sp")
     block_rows = q_ref.shape[0]
     heads = column_ref.shape[0]
@@ -119,22 +143,37 @@
         natural_ref[...] = jnp.broadcast_to(row, (8, block_rows)).T
         for i, place in enumerate(places):
             column_ref[h, i * step : (i + 1) * step] = natural_ref[pl.ds(place, step)]
+    masks = []
+    for i in range(0, 2 * n_fs, n_fs):
+        piece = [mask_ref[pl.ds(place, step)] for place in places[i : i + n_fs]]
+        masks.append(jnp.concatenate(piece, axis=0))
+    blocks = [(key_ref[...], value_ref[...], z)]
+    fold_blocks(q_ref, gates_ref, column_ref, blocks, masks, None, outs)
+
+
+def later_kernel(*refs):
+    q_ref, gates_ref, column_ref = refs[:3]
+    held, outs, (key_ref, value_ref) = refs[3:6], refs[-5:-2], refs[-2:]
+    pieces = tuple(zip(refs[6:-5:2], refs[7:-5:2]))
+    z = lax.axis_index("sp")
+    block_rows = q_ref.shape[0]
+
+    def keep():
+        for source, out in zip(held, outs):
+            out[...] = source[...]
 
     def fold(count):
-        masks = []
-        for i in range(0, 2 * n_fs, n_fs):
-            piece = [mask_ref[pl.ds(place, step)] for place in places[i : i + n_fs]]
-            masks.append(jnp.concatenate(piece, axis=0))
         rows = slice(0, count * block_rows)
         place_pairs(pieces[:count], key_ref.at[rows], value_ref.at[rows])
         blocks = []
         for k in range(count):
             rows = slice(k * block_rows, (k + 1) * block_rows)
-            blocks.append((key_ref[rows], value_ref[rows], z - k - min(k, 1)))
-        fold_blocks(q_ref, gates_ref, column_ref, blocks, masks, acc_ref, stat_ref)
-
+            blocks.append((key_ref[rows], value_ref[rows], z - 2 - k))
+        fold_blocks(q_ref, gates_ref, column_ref, blocks, None, held, outs)
+
+    pl.when(z < 2)(keep)
     for count in range(1, len(pieces) + 1):
-        pl.when(jnp.maximum(z, 1) == count)(functools.partial(fold, count))
+        pl.when(z - 1 == count)(functools.partial(fold, count))
 
 
 def row_places(n_fs, step):
@@ -193,8 +232,8 @@
 
 
 def mixer_kernel(first, *refs):
-    q_ref, conv_ref, gates_ref, column_ref, acc_ref, stat_ref = refs[:6]
-    near_ref, far_ref, weight_ref, out_ref, key_ref, value_ref, row_ref = refs[6:]
+    q_ref, conv_ref, gates_ref, column_ref, acc_ref, top_ref, den_ref = refs[:7]
+    near_ref, far_ref, weight_ref, out_ref, key_ref, value_ref, row_ref = refs[7:]
     block_rows = q_ref.shape[0]
     head_dim = key_ref.shape[1]
     channels = conv_ref.shape[1]
@@ -211,25 +250,37 @@
     def alone():
         for h in range(heads):
             place = h * block_rows + first
-            put(h, acc_ref[place : place + rows] / stat_ref[place : place + rows, 1:2])
+            put(h, acc_ref[place : place + rows] / den_ref[place : place + rows])
 
     @pl.when(origin >= 0)
     def joined():
         place_pairs(((near_ref, far_ref),), key_ref, value_ref)
+        places = [h * block_rows + first for h in range(heads)]
+        scores = []
         for h in range(heads):
             queries = q_ref[first : first + rows, h * head_dim : (h + 1) * head_dim]
             gate_q = column_ref[h, first : first + rows, 0:1]
             gate_k = gate_row(gates_ref, h, heads, origin, block_rows)
-            s = score(queries, key_ref[...], gate_q, gate_k, origin)
-            place = h * block_rows + first
-            held_top = stat_ref[place : place + rows, 0:1]
-            held_den = stat_ref[place : place + rows, 1:2]
-            top = jnp.maximum(held_top, jnp.max(s, axis=1, keepdims=True))
-            fade = jnp.exp2(held_top - top)
-            weight = jnp.exp2(s - top)
-            den = held_den * fade + jnp.sum(weight, axis=1, keepdims=True)
-            weighted = jnp.dot(weight.astype(bf16), value_ref[...], preferred_element_type=f32)
-            put(h, (acc_ref[place : place + rows] * fade + weighted) / den)
+            scores.append(score(queries, key_ref[...], gate_q, gate_k, origin))
+        wide = (rows, head_dim)
+        held_tops = [top_ref[place : place + rows] for place in places]
+        tops = [
+            jnp.maximum(top, jnp.broadcast_to(jnp.max(s, axis=1, keepdims=True), wide))
+            for top, s in zip(held_tops, scores)
+        ]
+        fades = [jnp.exp2(held_top - top) for held_top, top in zip(held_tops, tops)]
+        weights = [faded(s, top) for s, top in zip(scores, tops)]
+        dens = [
+            den_ref[place : place + rows] * fade
+            + jnp.broadcast_to(jnp.sum(weight, axis=1, keepdims=True), wide)
+            for place, fade, weight in zip(places, fades, weights)
+        ]
+        sums = [
+            jnp.dot(weight.astype(bf16), value_ref[...], preferred_element_type=f32)
+            for weight in weights
+        ]
+        for h, place in enumerate(places):
+            put(h, (acc_ref[place : place + rows] * fades[h] + sums[h]) / dens[h])
 
     out = jnp.dot(row_ref[...], weight_ref[...], preferred_element_type=f32)
     out_ref[...] = out.astype(bf16)
@@ -345,20 +396,28 @@
     )
     near = raised(rise, 1)
     far = swapped(near)
-    acc, stat, column = call(
+    held_shapes = (shape_of(heads * block_rows, head_dim, f32),) * 3
+    *held, column = call(
         early_kernel,
-        (
-            shape_of(heads * block_rows, head_dim, f32),
-            shape_of(heads * block_rows, head_dim, f32),
-            jax.ShapeDtypeStruct((heads, block_rows, 8), f32),
-        ),
-        [pltpu.VMEM((len(halves) * lane_rows, head_dim), bf16)] * 2
-        + [pltpu.VMEM((block_rows, 8), f32)],
+        (*held_shapes, jax.ShapeDtypeStruct((heads, block_rows, 8), f32)),
+        [pltpu.VMEM((block_rows, head_dim), bf16)] * 2 + [pltpu.VMEM((block_rows, 8), f32)],
         16,
         queries,
         gates,
         mask,
-        *halves,
+        *halves[:2],
+        work=SMALL_WORK,
+    )
+    held = call(
+        later_kernel,
+        held_shapes,
+        [pltpu.VMEM(((n_sp - 2) * block_rows, head_dim), bf16)] * 2,
+        16,
+        queries,
+        gates,
+        column,
+        *held,
+        *halves[2:],
         work=SMALL_WORK,
     )
     conv_out = call(
@@ -392,8 +451,7 @@
             conv_out,
             gates,
             column,
-            acc,
-            stat,
+            *held,
             near,
             far,
             w_out,

time: 42.1 us -> 41.6 us (0.988)
  the two profiles are of different devices: /device:TPU:27 before, /device:TPU:0 now
where the time goes in v4:
time: 41.6 us; the launch traced here: 40.8 us
  waiting for transfers between devices  19.7 us (47%)
  starting transfers between devices  14.9 us (36%)
  Pallas kernels  4.31 us (10%)
  local copies, waits for them, and re-layouts  1.66 us (4%)
    ppermute x6, waiting for transfers between devices, crossed(): return lax.ppermute(x, 'fs', [(i, i ^ k) for i in range(n_fs)])  11.8 us
    ppermute x6, starting transfers between devices, crossed(): return lax.ppermute(x, 'fs', [(i, i ^ k) for i in range(n_fs)])  8.18 us
    ppermute x3, waiting for transfers between devices, raised(): return lax.ppermute(x, 'sp', route)  5.47 us
    ppermute x3, starting transfers between devices, raised(): return lax.ppermute(x, 'sp', route)  5.46 us
    pallas_call x12, Pallas kernels, call(): pl.pallas_call(kernel, out_shape=out_shape, scratch_shapes=scratch, compi...  4.31 us
    ppermute x9, waiting for transfers between devices, swapped(): return lax.ppermute(x, 'tp', [(0, 1), (1, 0)])  2.46 us
    unnamed x24, local copies, waits for them, and re-layouts  1.66 us
    ppermute x9, starting transfers between devices, swapped(): return lax.ppermute(x, 'tp', [(0, 1), (1, 0)])  1.25 us
  transfers between devices with their start and end apart: 18, of which 11 were waited for; matrix products, arithmetic and copies ran while one was open for 0% of the time, Pallas kernels for 7%

profile of v4, /device:TPU:0, one launch (start us, length us, event | category | flops | bytes accessed | tf_op | source)
XLA Modules:
  0.0 40.8 jit_solution(11649318946742228452)
XLA Ops:
  0.0 0.9 %copy-done.8 = bf16[32,2048]{1,0:T(8,128)(2,1)S(1)} copy-done((bf16[32,2048]{1,0:T(8,128)(2,1)S(1)}, bf16[32,2048]{1,0:T(8,128)(2,1)}, u32[]{:S(2)}) %copy-start.8) | copy-done | bytes 131096
  0.9 0.7 %copy-done.10 = f32[2048]{0:T(1024)S(1)} copy-done((f32[2048]{0:T(1024)S(1)}, f32[2048]{0:T(1024)}, u32[]{:S(2)}) %copy-start.10) | copy-done | bytes 8216
  1.6 0.1 shard_map.118.refs_0_
  1.7 4.0 %collective-permute-start.2 = (bf16[32,2048]{1,0:T(8,128)(2,1)S(1)}, bf16[32,2048]{1,0:T(8,128)(2,1)S(1)}, u32[]{:S(2)}, u32[]{:S(2)}) collective-permute-start(bf16[32,2048]{1,0:T(8,128)(2,1)S(1)} %shard_map.118.refs_0_), channel_id=1, source_target_pairs={{0,6},{2,4},{4,2},{6,0},{1,7},{3,5},{5,3},{7,1},{8,14},{10,12},{12... | collective-permute-start | bytes 393224 | tf_op jit(solution)/shard_map/ppermute | solution.py:330
  5.7 0.5 %collective-permute-start.1 = (bf16[32,2048]{1,0:T(8,128)(2,1)S(1)}, bf16[32,2048]{1,0:T(8,128)(2,1)S(1)}, u32[]{:S(2)}, u32[]{:S(2)}) collective-permute-start(bf16[32,2048]{1,0:T(8,128)(2,1)S(1)} %shard_map.118.refs_0_), channel_id=1, source_target_pairs={{0,4},{2,6},{4,0},{6,2},{1,5},{3,7},{5,1},{7,3},{8,12},{10,14},{12... | collective-permute-start | bytes 393224 | tf_op jit(solution)/shard_map/ppermute | solution.py:330
  6.2 0.1 collective-permute-start
  6.4 3.2 %collective-permute-done.2.refs_3_ = bf16[32,2048]{1,0:T(8,128)(2,1)S(1)} collective-permute-done((bf16[32,2048]{1,0:T(8,128)(2,1)S(1)}, bf16[32,2048]{1,0:T(8,128)(2,1)S(1)}, u32[]{:S(2)}, u32[]{:S(2)}) %collective-permute-start.2) | collective-permute-done | bytes 131104 | tf_op jit(solution)/shard_map/ppermute | solution.py:330
  9.6 2.4 %collective-permute-done.1.refs_2_ = bf16[32,2048]{1,0:T(8,128)(2,1)S(1)} collective-permute-done((bf16[32,2048]{1,0:T(8,128)(2,1)S(1)}, bf16[32,2048]{1,0:T(8,128)(2,1)S(1)}, u32[]{:S(2)}, u32[]{:S(2)}) %collective-permute-start.1) | collective-permute-done | bytes 131104 | tf_op jit(solution)/shard_map/ppermute | solution.py:330
  12.0 0.2 collective-permute-done.refs_1_
  12.3 0.3 shard_map.119.refs_12_.refs_3_
  12.6 3.7 %collective-permute-start.11 = (bf16[128,256]{1,0:T(8,128)(2,1)S(1)}, bf16[128,256]{1,0:T(8,128)(2,1)S(1)}, u32[]{:S(2)}, u32[]{:S(2)}) collective-permute-start(bf16[128,256]{1,0:T(8,128)(2,1)S(1)} %shard_map.119.refs_12_.refs_3_), channel_id=1, source_target_pairs={{0,24},{8,0},{16,8},{24,16},{1,25},{9,1},{17,9},{25,17},{2,26},{10... | collective-permute-start | bytes 196616 | tf_op jit(solution)/shard_map/ppermute | solution.py:334
  16.3 0.5 %collective-permute-start.5 = (bf16[32,2048]{1,0:T(8,128)(2,1)S(1)}, bf16[32,2048]{1,0:T(8,128)(2,1)S(1)}, u32[]{:S(2)}, u32[]{:S(2)}) collective-permute-start(bf16[32,2048]{1,0:T(8,128)(2,1)S(1)} %collective-permute-done.1.refs_2_), channel_id=1, source_target_pairs={{0,1},{1,0},{2,3},{3,2},{4,5},{5,4},{6,7},{7,6},{8,9},{9,8},{10,11... | collective-permute-start | bytes 393224 | tf_op jit(solution)/shard_map/ppermute | solution.py:327
  16.9 0.1 shard_map.125.refs_9_
  17.0 1.4 %collective-permute-done.11.refs_8_ = bf16[128,256]{1,0:T(8,128)(2,1)S(1)} collective-permute-done((bf16[128,256]{1,0:T(8,128)(2,1)S(1)}, bf16[128,256]{1,0:T(8,128)(2,1)S(1)}, u32[]{:S(2)}, u32[]{:S(2)}) %collective-permute-start.11) | collective-permute-done | bytes 65568 | tf_op jit(solution)/shard_map/ppermute | solution.py:334
  18.5 3.0 %collective-permute-done.9.refs_6_ = bf16[128,256]{1,0:T(8,128)(2,1)S(1)} collective-permute-done((bf16[128,256]{1,0:T(8,128)(2,1)S(1)}, bf16[128,256]{1,0:T(8,128)(2,1)S(1)}, u32[]{:S(2)}, u32[]{:S(2)}) %collective-permute-start.9) | collective-permute-done | bytes 65568 | tf_op jit(solution)/shard_map/ppermute | solution.py:334
  21.5 0.5 %collective-permute-start.10 = (bf16[128,256]{1,0:T(8,128)(2,1)S(1)}, bf16[128,256]{1,0:T(8,128)(2,1)S(1)}, u32[]{:S(2)}, u32[]{:S(2)}) collective-permute-start(bf16[128,256]{1,0:T(8,128)(2,1)S(1)} %collective-permute-done.9.refs_6_), channel_id=1, source_target_pairs={{0,1},{1,0},{2,3},{3,2},{4,5},{5,4},{6,7},{7,6},{8,9},{9,8},{10,11... | collective-permute-start | bytes 196616 | tf_op jit(solution)/shard_map/ppermute | solution.py:327
  22.0 1.0 %shard_map.120 = (bf16[256,256]{1,0:T(8,128)(2,1)S(1)}, bf16[256,128]{1,0:T(8,128)(2,1)S(1)}, bf16[256,128]{1,0:T(8,128)(2,1)S(1)}, bf16[144,256]{1,0:T(8,128)(2,1)S(1)}) custom-call(bf16[32,2048]{1,0:T(8,128)(2,1)S(1)} %shard_map.118.refs_0_, bf16[32,2048]{1,0:T(8,128)(2,1)S(1)} %collective-permute-done.refs_1_, ...), custom_call_target="tpu_custom_call" | custom-call | flops 2000000000 | tf_op jit(solution)/shard_map/pallas_call | solution.py:342
  23.0 1.8 %collective-permute-start.7 = (bf16[144,256]{1,0:T(8,128)(2,1)S(1)}, bf16[144,256]{1,0:T(8,128)(2,1)S(1)}, u32[]{:S(2)}, u32[]{:S(2)}) collective-permute-start(bf16[144,256]{1,0:T(8,128)(2,1)S(1)} %get-tuple-element.23), channel_id=1, source_target_pairs={{0,8},{8,16},{16,24},{1,9},{9,17},{17,25},{2,10},{10,18},{18,26},{... | collective-permute-start | bytes 221192 | tf_op jit(solution)/shard_map/ppermute | solution.py:334
  24.9 0.8 %shard_map.123 = (f32[512,128]{1,0:T(8,128)S(1)}, f32[512,128]{1,0:T(8,128)S(1)}, f32[512,128]{1,0:T(8,128)S(1)}, f32[2,256,8]{2,1,0:T(8,128)S(1)}) custom-call(bf16[256,256]{1,0:T(8,128)(2,1)S(1)} %get-tuple-element.20.refs_0_, f32[16,1024]{1,0:T(8,128)S(1)} %copy-done.9, f32[256,256]{1,0:T(8,128)S(1)} %shard_map.122.refs_2_, ...), custom_call_target="tpu_custom_call" | custom-call | flops 2000000000 | tf_op jit(solution)/shard_map/pallas_call | solution.py:342
  25.8 1.0 %collective-permute-done.7.risen_ref.refs_7_ = bf16[144,256]{1,0:T(8,128)(2,1)S(1)} collective-permute-done((bf16[144,256]{1,0:T(8,128)(2,1)S(1)}, bf16[144,256]{1,0:T(8,128)(2,1)S(1)}, u32[]{:S(2)}, u32[]{:S(2)}) %collective-permute-start.7) | collective-permute-done | bytes 73760 | tf_op jit(solution)/shard_map/ppermute | solution.py:334
  26.9 1.2 %collective-permute-done.13.refs_8_ = bf16[144,256]{1,0:T(8,128)(2,1)S(1)} collective-permute-done((bf16[144,256]{1,0:T(8,128)(2,1)S(1)}, bf16[144,256]{1,0:T(8,128)(2,1)S(1)}, u32[]{:S(2)}, u32[]{:S(2)}) %collective-permute-start.13) | collective-permute-done | bytes 73760 | tf_op jit(solution)/shard_map/ppermute | solution.py:327
  28.1 0.5 %shard_map.127 = bf16[128,2048]{1,0:T(8,128)(2,1)S(1)} custom-call(bf16[256,256]{1,0:T(8,128)(2,1)S(1)} %get-tuple-element.20.refs_0_, bf16[256,128]{1,0:T(8,128)(2,1)S(1)} %shard_map.121.refs_1_, f32[16,1024]{1,0:T(8,128)S(1)} %copy-done.9, f32[2,256,8]{2,1,0:T(8,128)S(1)} %get-tuple-element.24.refs_2_.refs_3_, f32[512,128]{1,0:T(8,128)S(1)} %get-tuple-element.28.refs_4_, ...), custom_call_target="tpu_custom_call" | custom-call | flops 2000000000 | tf_op jit(solution)/shard_map/pallas_call | solution.py:342
  28.6 0.2 collective-permute-start.14
  28.8 0.5 %shard_map.126.keep_ref = bf16[128,2048]{1,0:T(8,128)(2,1)S(1)} custom-call(bf16[256,256]{1,0:T(8,128)(2,1)S(1)} %get-tuple-element.20.refs_0_, bf16[256,128]{1,0:T(8,128)(2,1)S(1)} %shard_map.121.refs_1_, f32[16,1024]{1,0:T(8,128)S(1)} %copy-done.9, f32[2,256,8]{2,1,0:T(8,128)S(1)} %get-tuple-element.24.refs_2_.refs_3_, ...), custom_call_target="tpu_custom_call" | custom-call | flops 2000000000 | tf_op jit(solution)/shard_map/pallas_call | solution.py:342
  29.3 1.3 %collective-permute-done.14.got_ref = bf16[128,2048]{1,0:T(8,128)(2,1)S(1)} collective-permute-done((bf16[128,2048]{1,0:T(8,128)(2,1)S(1)}, bf16[128,2048]{1,0:T(8,128)(2,1)S(1)}, u32[]{:S(2)}, u32[]{:S(2)}) %collective-permute-start.14) | collective-permute-done | bytes 524320 | tf_op jit(solution)/shard_map/ppermute | solution.py:327
  30.5 0.1 shard_map.128
  30.7 1.2 %collective-permute-start.15 = (bf16[32,2048]{1,0:T(8,128)(2,1)S(1)}, bf16[32,2048]{1,0:T(8,128)(2,1)S(1)}, u32[]{:S(2)}, u32[]{:S(2)}) collective-permute-start(bf16[32,2048]{1,0:T(8,128)(2,1)S(1)} %get-tuple-element.31), channel_id=1, source_target_pairs={{0,6},{2,4},{4,2},{6,0},{1,7},{3,5},{5,3},{7,1},{8,14},{10,12},{12... | collective-permute-start | bytes 393224 | tf_op jit(solution)/shard_map/ppermute | solution.py:330
  31.9 1.8 %collective-permute-start.16 = (bf16[32,2048]{1,0:T(8,128)(2,1)S(1)}, bf16[32,2048]{1,0:T(8,128)(2,1)S(1)}, u32[]{:S(2)}, u32[]{:S(2)}) collective-permute-start(bf16[32,2048]{1,0:T(8,128)(2,1)S(1)} %get-tuple-element.32), channel_id=1, source_target_pairs={{0,4},{2,6},{4,0},{6,2},{1,5},{3,7},{5,1},{7,3},{8,12},{10,14},{12... | collective-permute-start | bytes 393224 | tf_op jit(solution)/shard_map/ppermute | solution.py:330
  33.7 0.5 %collective-permute-start.17 = (bf16[32,2048]{1,0:T(8,128)(2,1)S(1)}, bf16[32,2048]{1,0:T(8,128)(2,1)S(1)}, u32[]{:S(2)}, u32[]{:S(2)}) collective-permute-start(bf16[32,2048]{1,0:T(8,128)(2,1)S(1)} %get-tuple-element.33), channel_id=1, source_target_pairs={{0,2},{2,0},{4,6},{6,4},{1,3},{3,1},{5,7},{7,5},{8,10},{10,8},{12,... | collective-permute-start | bytes 393224 | tf_op jit(solution)/shard_map/ppermute | solution.py:330
  34.2 3.8 %collective-permute-done.15.refs_0_ = bf16[32,2048]{1,0:T(8,128)(2,1)S(1)} collective-permute-done((bf16[32,2048]{1,0:T(8,128)(2,1)S(1)}, bf16[32,2048]{1,0:T(8,128)(2,1)S(1)}, u32[]{:S(2)}, u32[]{:S(2)}) %collective-permute-start.15) | collective-permute-done | bytes 131104 | tf_op jit(solution)/shard_map/ppermute | solution.py:330
  38.0 2.0 %collective-permute-done.16.refs_1_ = bf16[32,2048]{1,0:T(8,128)(2,1)S(1)} collective-permute-done((bf16[32,2048]{1,0:T(8,128)(2,1)S(1)}, bf16[32,2048]{1,0:T(8,128)(2,1)S(1)}, u32[]{:S(2)}, u32[]{:S(2)}) %collective-permute-start.16) | collective-permute-done | bytes 131104 | tf_op jit(solution)/shard_map/ppermute | solution.py:330
  40.1 0.7 %shard_map.129 = bf16[32,2048]{1,0:T(8,128)(2,1)} custom-call(bf16[32,2048]{1,0:T(8,128)(2,1)S(1)} %collective-permute-done.15.refs_0_, bf16[32,2048]{1,0:T(8,128)(2,1)S(1)} %collective-permute-done.16.refs_1_, bf16[32,2048]{1,0:T(8,128)(2,1)S(1)} %collective-permute-done.17.refs_2_, f32[32,2048]{1,0:T(8,128)S(1)} %get-tuple-element.34.refs_3_), custom_call_target="tpu_custom_call" | custom-call | tf_op jit(solution)/shard_map/pallas_call | solution.py:342
  (40 shorter events, 0.4 us)
Async XLA Ops:
  0.0 0.9 %copy-start.8 = (bf16[32,2048]{1,0:T(8,128)(2,1)S(1)}, bf16[32,2048]{1,0:T(8,128)(2,1)}, u32[]{:S(2)}) copy-start(bf16[32,2048]{1,0:T(8,128)(2,1)} %tokens_ref.1) | copy-start | bytes 393220
  0.9 0.7 %copy-start.10 = (f32[2048]{0:T(1024)S(1)}, f32[2048]{0:T(1024)}, u32[]{:S(2)}) copy-start(f32[2048]{0:T(1024)} %param.13) | copy-start | bytes 24580
  1.6 10.7 %copy-start.3 = (bf16[2048,128]{1,0:T(8,128)(2,1)S(1)}, bf16[2048,128]{1,0:T(8,128)(2,1)}, u32[]{:S(2)}) copy-start(bf16[2048,128]{1,0:T(8,128)(2,1)} %refs_4_.1) | copy-start | bytes 1572868
  1.6 10.7 %copy-start.4 = (bf16[2048,128]{1,0:T(8,128)(2,1)S(1)}, bf16[2048,128]{1,0:T(8,128)(2,1)}, u32[]{:S(2)}) copy-start(bf16[2048,128]{1,0:T(8,128)(2,1)} %refs_5_.1) | copy-start | bytes 1572868
  1.7 7.9 %collective-permute-start.2 = (bf16[32,2048]{1,0:T(8,128)(2,1)S(1)}, bf16[32,2048]{1,0:T(8,128)(2,1)S(1)}, u32[]{:S(2)}, u32[]{:S(2)}) collective-permute-start(bf16[32,2048]{1,0:T(8,128)(2,1)S(1)} %shard_map.118.refs_0_), channel_id=1, source_target_pairs={{0,6},{2,4},{4,2},{6,0},{1,7},{3,5},{5,3},{7,1},{8,14},{10,12},{12... | collective-permute-start | bytes 393224 | tf_op jit(solution)/shard_map/ppermute | solution.py:330
  5.7 6.3 %collective-permute-start.1 = (bf16[32,2048]{1,0:T(8,128)(2,1)S(1)}, bf16[32,2048]{1,0:T(8,128)(2,1)S(1)}, u32[]{:S(2)}, u32[]{:S(2)}) collective-permute-start(bf16[32,2048]{1,0:T(8,128)(2,1)S(1)} %shard_map.118.refs_0_), channel_id=1, source_target_pairs={{0,4},{2,6},{4,0},{6,2},{1,5},{3,7},{5,1},{7,3},{8,12},{10,14},{12... | collective-permute-start | bytes 393224 | tf_op jit(solution)/shard_map/ppermute | solution.py:330
  6.2 6.0 %collective-permute-start = (bf16[32,2048]{1,0:T(8,128)(2,1)S(1)}, bf16[32,2048]{1,0:T(8,128)(2,1)S(1)}, u32[]{:S(2)}, u32[]{:S(2)}) collective-permute-start(bf16[32,2048]{1,0:T(8,128)(2,1)S(1)} %shard_map.118.refs_0_), channel_id=1, source_target_pairs={{0,2},{2,0},{4,6},{6,4},{1,3},{3,1},{5,7},{7,5},{8,10},{10,8},{12,... | collective-permute-start | bytes 393224 | tf_op jit(solution)/shard_map/ppermute | solution.py:330
  6.4 10.4 %collective-permute-start.3 = (bf16[32,2048]{1,0:T(8,128)(2,1)S(1)}, bf16[32,2048]{1,0:T(8,128)(2,1)S(1)}, u32[]{:S(2)}, u32[]{:S(2)}) collective-permute-start(bf16[32,2048]{1,0:T(8,128)(2,1)S(1)} %shard_map.118.refs_0_), channel_id=1, source_target_pairs={{0,1},{1,0},{2,3},{3,2},{4,5},{5,4},{6,7},{7,6},{8,9},{9,8},{10,11... | collective-permute-start | bytes 393224 | tf_op jit(solution)/shard_map/ppermute | solution.py:327
  12.6 4.2 %copy-start = (bf16[256,2048]{1,0:T(8,128)(2,1)S(1)}, bf16[256,2048]{1,0:T(8,128)(2,1)}, u32[]{:S(2)}) copy-start(bf16[256,2048]{1,0:T(8,128)(2,1)} %low_ref.1) | copy-start | bytes 3145732
  12.6 4.2 %copy-start.1 = (bf16[128,2048]{1,0:T(8,128)(2,1)S(1)}, bf16[128,2048]{1,0:T(8,128)(2,1)}, u32[]{:S(2)}) copy-start(bf16[128,2048]{1,0:T(8,128)(2,1)} %top_ref.1) | copy-start | bytes 1572868
  12.6 5.8 %collective-permute-start.11 = (bf16[128,256]{1,0:T(8,128)(2,1)S(1)}, bf16[128,256]{1,0:T(8,128)(2,1)S(1)}, u32[]{:S(2)}, u32[]{:S(2)}) collective-permute-start(bf16[128,256]{1,0:T(8,128)(2,1)S(1)} %shard_map.119.refs_12_.refs_3_), channel_id=1, source_target_pairs={{0,24},{8,0},{16,8},{24,16},{1,25},{9,1},{17,9},{25,17},{2,26},{10... | collective-permute-start | bytes 196616 | tf_op jit(solution)/shard_map/ppermute | solution.py:334
  16.3 5.2 %collective-permute-start.9 = (bf16[128,256]{1,0:T(8,128)(2,1)S(1)}, bf16[128,256]{1,0:T(8,128)(2,1)S(1)}, u32[]{:S(2)}, u32[]{:S(2)}) collective-permute-start(bf16[128,256]{1,0:T(8,128)(2,1)S(1)} %shard_map.119.refs_12_.refs_3_), channel_id=1, source_target_pairs={{0,16},{8,24},{16,0},{24,8},{1,17},{9,25},{17,1},{25,9},{2,18},{10... | collective-permute-start | bytes 196616 | tf_op jit(solution)/shard_map/ppermute | solution.py:334
  16.3 5.2 %collective-permute-start.6 = (bf16[32,2048]{1,0:T(8,128)(2,1)S(1)}, bf16[32,2048]{1,0:T(8,128)(2,1)S(1)}, u32[]{:S(2)}, u32[]{:S(2)}) collective-permute-start(bf16[32,2048]{1,0:T(8,128)(2,1)S(1)} %collective-permute-done.2.refs_3_), channel_id=1, source_target_pairs={{0,1},{1,0},{2,3},{3,2},{4,5},{5,4},{6,7},{7,6},{8,9},{9,8},{10,11... | collective-permute-start | bytes 393224 | tf_op jit(solution)/shard_map/ppermute | solution.py:327
  16.3 5.7 %collective-permute-start.5 = (bf16[32,2048]{1,0:T(8,128)(2,1)S(1)}, bf16[32,2048]{1,0:T(8,128)(2,1)S(1)}, u32[]{:S(2)}, u32[]{:S(2)}) collective-permute-start(bf16[32,2048]{1,0:T(8,128)(2,1)S(1)} %collective-permute-done.1.refs_2_), channel_id=1, source_target_pairs={{0,1},{1,0},{2,3},{3,2},{4,5},{5,4},{6,7},{7,6},{8,9},{9,8},{10,11... | collective-permute-start | bytes 393224 | tf_op jit(solution)/shard_map/ppermute | solution.py:327
  16.8 5.2 %collective-permute-start.4 = (bf16[32,2048]{1,0:T(8,128)(2,1)S(1)}, bf16[32,2048]{1,0:T(8,128)(2,1)S(1)}, u32[]{:S(2)}, u32[]{:S(2)}) collective-permute-start(bf16[32,2048]{1,0:T(8,128)(2,1)S(1)} %collective-permute-done.refs_1_), channel_id=1, source_target_pairs={{0,1},{1,0},{2,3},{3,2},{4,5},{5,4},{6,7},{7,6},{8,9},{9,8},{10,11... | collective-permute-start | bytes 393224 | tf_op jit(solution)/shard_map/ppermute | solution.py:327
  16.9 5.1 %copy-start.2 = (bf16[2048,256]{1,0:T(8,128)(2,1)S(1)}, bf16[2048,256]{1,0:T(8,128)(2,1)}, u32[]{:S(2)}) copy-start(bf16[2048,256]{1,0:T(8,128)(2,1)} %refs_8_.1) | copy-start | bytes 3145732
  16.9 5.1 %copy-start.5 = (bf16[2048,128]{1,0:T(8,128)(2,1)S(1)}, bf16[2048,128]{1,0:T(8,128)(2,1)}, u32[]{:S(2)}) copy-start(bf16[2048,128]{1,0:T(8,128)(2,1)} %refs_9_.1) | copy-start | bytes 1572868
  16.9 5.1 %copy-start.6 = (bf16[2048,128]{1,0:T(8,128)(2,1)S(1)}, bf16[2048,128]{1,0:T(8,128)(2,1)}, u32[]{:S(2)}) copy-start(bf16[2048,128]{1,0:T(8,128)(2,1)} %refs_10_.1) | copy-start | bytes 1572868
  16.9 5.1 %copy-start.7 = (bf16[2048,128]{1,0:T(8,128)(2,1)S(1)}, bf16[2048,128]{1,0:T(8,128)(2,1)}, u32[]{:S(2)}) copy-start(bf16[2048,128]{1,0:T(8,128)(2,1)} %refs_11_.1) | copy-start | bytes 1572868
  17.0 7.8 %copy-start.9 = (f32[16,1024]{1,0:T(8,128)S(1)}, f32[16,1024]{1,0:T(8,128)}, u32[]{:S(2)}) copy-start(f32[16,1024]{1,0:T(8,128)} %refs_2_.3) | copy-start | bytes 196612
  18.5 6.4 %collective-permute-start.8 = (bf16[128,256]{1,0:T(8,128)(2,1)S(1)}, bf16[128,256]{1,0:T(8,128)(2,1)S(1)}, u32[]{:S(2)}, u32[]{:S(2)}) collective-permute-start(bf16[128,256]{1,0:T(8,128)(2,1)S(1)} %shard_map.119.refs_12_.refs_3_), channel_id=1, source_target_pairs={{0,1},{1,0},{2,3},{3,2},{4,5},{5,4},{6,7},{7,6},{8,9},{9,8},{10,11... | collective-permute-start | bytes 196616 | tf_op jit(solution)/shard_map/ppermute | solution.py:327
  21.5 4.2 %collective-permute-start.12 = (bf16[128,256]{1,0:T(8,128)(2,1)S(1)}, bf16[128,256]{1,0:T(8,128)(2,1)S(1)}, u32[]{:S(2)}, u32[]{:S(2)}) collective-permute-start(bf16[128,256]{1,0:T(8,128)(2,1)S(1)} %collective-permute-done.11.refs_8_), channel_id=1, source_target_pairs={{0,1},{1,0},{2,3},{3,2},{4,5},{5,4},{6,7},{7,6},{8,9},{9,8},{10,11... | collective-permute-start | bytes 196616 | tf_op jit(solution)/shard_map/ppermute | solution.py:327
  21.5 4.2 %collective-permute-start.10 = (bf16[128,256]{1,0:T(8,128)(2,1)S(1)}, bf16[128,256]{1,0:T(8,128)(2,1)S(1)}, u32[]{:S(2)}, u32[]{:S(2)}) collective-permute-start(bf16[128,256]{1,0:T(8,128)(2,1)S(1)} %collective-permute-done.9.refs_6_), channel_id=1, source_target_pairs={{0,1},{1,0},{2,3},{3,2},{4,5},{5,4},{6,7},{7,6},{8,9},{9,8},{10,11... | collective-permute-start | bytes 196616 | tf_op jit(solution)/shard_map/ppermute | solution.py:327
  23.0 3.8 %collective-permute-start.7 = (bf16[144,256]{1,0:T(8,128)(2,1)S(1)}, bf16[144,256]{1,0:T(8,128)(2,1)S(1)}, u32[]{:S(2)}, u32[]{:S(2)}) collective-permute-start(bf16[144,256]{1,0:T(8,128)(2,1)S(1)} %get-tuple-element.23), channel_id=1, source_target_pairs={{0,8},{8,16},{16,24},{1,9},{9,17},{17,25},{2,10},{10,18},{18,26},{... | collective-permute-start | bytes 221192 | tf_op jit(solution)/shard_map/ppermute | solution.py:334
  25.7 1.1 %copy-start.11 = (bf16[3,1024]{1,0:T(4,128)(2,1)S(1)}, bf16[3,1024]{1,0:T(4,128)(2,1)}, u32[]{:S(2)}) copy-start(bf16[3,1024]{1,0:T(4,128)(2,1)} %taps_ref.1) | copy-start | bytes 18436
  26.8 1.3 %collective-permute-start.13 = (bf16[144,256]{1,0:T(8,128)(2,1)S(1)}, bf16[144,256]{1,0:T(8,128)(2,1)S(1)}, u32[]{:S(2)}, u32[]{:S(2)}) collective-permute-start(bf16[144,256]{1,0:T(8,128)(2,1)S(1)} %collective-permute-done.7.risen_ref.refs_7_), channel_id=1, source_target_pairs={{0,1},{1,0},{2,3},{3,2},{4,5},{5,4},{6,7},{7,6},{8,9},{9,8},{10,11... | collective-permute-start | bytes 221192 | tf_op jit(solution)/shard_map/ppermute | solution.py:327
  28.6 2.0 %collective-permute-start.14 = (bf16[128,2048]{1,0:T(8,128)(2,1)S(1)}, bf16[128,2048]{1,0:T(8,128)(2,1)S(1)}, u32[]{:S(2)}, u32[]{:S(2)}) collective-permute-start(bf16[128,2048]{1,0:T(8,128)(2,1)S(1)} %shard_map.127), channel_id=1, source_target_pairs={{0,1},{1,0},{2,3},{3,2},{4,5},{5,4},{6,7},{7,6},{8,9},{9,8},{10,11... | collective-permute-start | bytes 1572872 | tf_op jit(solution)/shard_map/ppermute | solution.py:327
  30.7 7.4 %collective-permute-start.15 = (bf16[32,2048]{1,0:T(8,128)(2,1)S(1)}, bf16[32,2048]{1,0:T(8,128)(2,1)S(1)}, u32[]{:S(2)}, u32[]{:S(2)}) collective-permute-start(bf16[32,2048]{1,0:T(8,128)(2,1)S(1)} %get-tuple-element.31), channel_id=1, source_target_pairs={{0,6},{2,4},{4,2},{6,0},{1,7},{3,5},{5,3},{7,1},{8,14},{10,12},{12... | collective-permute-start | bytes 393224 | tf_op jit(solution)/shard_map/ppermute | solution.py:330
  31.9 8.1 %collective-permute-start.16 = (bf16[32,2048]{1,0:T(8,128)(2,1)S(1)}, bf16[32,2048]{1,0:T(8,128)(2,1)S(1)}, u32[]{:S(2)}, u32[]{:S(2)}) collective-permute-start(bf16[32,2048]{1,0:T(8,128)(2,1)S(1)} %get-tuple-element.32), channel_id=1, source_target_pairs={{0,4},{2,6},{4,0},{6,2},{1,5},{3,7},{5,1},{7,3},{8,12},{10,14},{12... | collective-permute-start | bytes 393224 | tf_op jit(solution)/shard_map/ppermute | solution.py:330
  33.7 6.4 %collective-permute-start.17 = (bf16[32,2048]{1,0:T(8,128)(2,1)S(1)}, bf16[32,2048]{1,0:T(8,128)(2,1)S(1)}, u32[]{:S(2)}, u32[]{:S(2)}) collective-permute-start(bf16[32,2048]{1,0:T(8,128)(2,1)S(1)} %get-tuple-element.33), channel_id=1, source_target_pairs={{0,2},{2,0},{4,6},{6,4},{1,3},{3,1},{5,7},{7,5},{8,10},{10,8},{12,... | collective-permute-start | bytes 393224 | tf_op jit(solution)/shard_map/ppermute | solution.py:330

commit v5 on v4

--- a/solution.py
+++ b/solution.py
@@ -233,12 +233,13 @@
 
 def mixer_kernel(first, *refs):
     q_ref, conv_ref, gates_ref, column_ref, acc_ref, top_ref, den_ref = refs[:7]
-    near_ref, far_ref, weight_ref, out_ref, key_ref, value_ref, row_ref = refs[7:]
+    near_ref, far_ref, weight_ref = refs[7:10]
+    outs, (key_ref, value_ref, row_ref) = refs[10:-3], refs[-3:]
     block_rows = q_ref.shape[0]
     head_dim = key_ref.shape[1]
     channels = conv_ref.shape[1]
     heads = q_ref.shape[1] // head_dim
-    rows = out_ref.shape[0]
+    rows = sum(out_ref.shape[0] for out_ref in outs)
     origin = lax.axis_index("sp") - 1
     row_ref[:, :channels] = conv_ref[first : first + rows]
 
@@ -282,8 +283,11 @@
         for h, place in enumerate(places):
             put(h, (acc_ref[place : place + rows] * fades[h] + sums[h]) / dens[h])
 
-    out = jnp.dot(row_ref[...], weight_ref[...], preferred_element_type=f32)
-    out_ref[...] = out.astype(bf16)
+    out = jnp.dot(row_ref[...], weight_ref[...], preferred_element_type=f32).astype(bf16)
+    start = 0
+    for out_ref in outs:
+        out_ref[...] = out[start : start + out_ref.shape[0]]
+        start += out_ref.shape[0]
 
 
 def pair_sum_kernel(keep_ref, got_ref, *outs):
@@ -443,7 +447,7 @@
     def mixed_rows(first):
         return call(
             functools.partial(mixer_kernel, first),
-            shape_of(lane_rows, width),
+            tuple(shape_of(count * step, width) for count in (1, n_fs - 1)),
             [pltpu.VMEM((block_rows, head_dim), bf16)] * 2
             + [pltpu.VMEM((lane_rows, channels + heads * head_dim), bf16)],
             16,
@@ -458,19 +462,23 @@
             work=SMALL_WORK,
         )
 
-    send = mixed_rows(0)
-    got = swapped(send)
-    keep = mixed_rows(lane_rows)
-    parts = range(n_fs - 1, -1, -1)
-    pieces = call(
-        pair_sum_kernel,
-        tuple(shape_of(step, width, bf16 if k else f32) for k in parts),
-        [],
-        8,
-        keep,
-        got,
-    )
-    sums = [crossed(piece, k) if k else piece for k, piece in zip(parts, pieces)]
+    counts = (1, n_fs - 1)
+    sends = mixed_rows(0)
+    gots = [swapped(send) for send in sends]
+    keeps = mixed_rows(lane_rows)
+    parts = list(range(n_fs - 1, -1, -1))
+    sums = []
+    for count, keep, got in zip(counts, keeps, gots):
+        group, parts = parts[:count], parts[count:]
+        pieces = call(
+            pair_sum_kernel,
+            tuple(shape_of(step, width, bf16 if k else f32) for k in group),
+            [],
+            8,
+            keep,
+            got,
+        )
+        sums += [crossed(piece, k) if k else piece for k, piece in zip(group, pieces)]
     return call(final_kernel, shape_of(step, width), [], 4, *sums)
 
 

time: 41.6 us -> 41.6 us (level)
  the two profiles are of different devices: /device:TPU:0 before, /device:TPU:27 now
where the time goes in v5:
time: 41.6 us; the launch traced here: 41.3 us
  waiting for transfers between devices  17.6 us (42%)
  starting transfers between devices  16 us (38%)
  Pallas kernels  5.91 us (14%)
  local copies, waits for them, and re-layouts  1.66 us (4%)
    ppermute x6, waiting for transfers between devices, crossed(): return lax.ppermute(x, 'fs', [(i, i ^ k) for i in range(n_fs)])  11.3 us
    ppermute x10, starting transfers between devices, swapped(): return lax.ppermute(x, 'tp', [(0, 1), (1, 0)])  8.89 us
    pallas_call x13, Pallas kernels, call(): pl.pallas_call(kernel, out_shape=out_shape, scratch_shapes=scratch, compi...  5.91 us
    ppermute x6, starting transfers between devices, crossed(): return lax.ppermute(x, 'fs', [(i, i ^ k) for i in range(n_fs)])  5.49 us
    ppermute x3, waiting for transfers between devices, raised(): return lax.ppermute(x, 'sp', route)  4.93 us
    unnamed x24, local copies, waits for them, and re-layouts  1.66 us
    ppermute x3, starting transfers between devices, raised(): return lax.ppermute(x, 'sp', route)  1.57 us
    ppermute x10, waiting for transfers between devices, swapped(): return lax.ppermute(x, 'tp', [(0, 1), (1, 0)])  1.35 us
  transfers between devices with their start and end apart: 19, of which 8 were waited for; matrix products, arithmetic and copies ran while one was open for 0% of the time, Pallas kernels for 10%

profile of v5, /device:TPU:27, one launch (start us, length us, event | category | flops | bytes accessed | tf_op | source)
XLA Modules:
  0.0 41.3 jit_solution(2010245921802786530)
XLA Ops:
  0.0 0.9 %copy-done.8 = bf16[32,2048]{1,0:T(8,128)(2,1)S(1)} copy-done((bf16[32,2048]{1,0:T(8,128)(2,1)S(1)}, bf16[32,2048]{1,0:T(8,128)(2,1)}, u32[]{:S(2)}) %copy-start.8) | copy-done | bytes 131096
  0.9 0.7 %copy-done.10 = f32[2048]{0:T(1024)S(1)} copy-done((f32[2048]{0:T(1024)S(1)}, f32[2048]{0:T(1024)}, u32[]{:S(2)}) %copy-start.10) | copy-done | bytes 8216
  1.7 1.3 %collective-permute-start.2 = (bf16[32,2048]{1,0:T(8,128)(2,1)S(1)}, bf16[32,2048]{1,0:T(8,128)(2,1)S(1)}, u32[]{:S(2)}, u32[]{:S(2)}) collective-permute-start(bf16[32,2048]{1,0:T(8,128)(2,1)S(1)} %shard_map.118.refs_0_), channel_id=1, source_target_pairs={{0,6},{2,4},{4,2},{6,0},{1,7},{3,5},{5,3},{7,1},{8,14},{10,12},{12... | collective-permute-start | bytes 393224 | tf_op jit(solution)/shard_map/ppermute | solution.py:334
  3.0 0.2 collective-permute-start.1
  3.2 1.2 %collective-permute-start = (bf16[32,2048]{1,0:T(8,128)(2,1)S(1)}, bf16[32,2048]{1,0:T(8,128)(2,1)S(1)}, u32[]{:S(2)}, u32[]{:S(2)}) collective-permute-start(bf16[32,2048]{1,0:T(8,128)(2,1)S(1)} %shard_map.118.refs_0_), channel_id=1, source_target_pairs={{0,2},{2,0},{4,6},{6,4},{1,3},{3,1},{5,7},{7,5},{8,10},{10,8},{12,... | collective-permute-start | bytes 393224 | tf_op jit(solution)/shard_map/ppermute | solution.py:334
  4.5 1.5 %collective-permute-start.3 = (bf16[32,2048]{1,0:T(8,128)(2,1)S(1)}, bf16[32,2048]{1,0:T(8,128)(2,1)S(1)}, u32[]{:S(2)}, u32[]{:S(2)}) collective-permute-start(bf16[32,2048]{1,0:T(8,128)(2,1)S(1)} %shard_map.118.refs_0_), channel_id=1, source_target_pairs={{0,1},{1,0},{2,3},{3,2},{4,5},{5,4},{6,7},{7,6},{8,9},{9,8},{10,11... | collective-permute-start | bytes 393224 | tf_op jit(solution)/shard_map/ppermute | solution.py:331
  6.0 1.1 %collective-permute-done.2.refs_3_ = bf16[32,2048]{1,0:T(8,128)(2,1)S(1)} collective-permute-done((bf16[32,2048]{1,0:T(8,128)(2,1)S(1)}, bf16[32,2048]{1,0:T(8,128)(2,1)S(1)}, u32[]{:S(2)}, u32[]{:S(2)}) %collective-permute-start.2) | collective-permute-done | bytes 131104 | tf_op jit(solution)/shard_map/ppermute | solution.py:334
  7.1 3.8 %collective-permute-done.1.refs_2_ = bf16[32,2048]{1,0:T(8,128)(2,1)S(1)} collective-permute-done((bf16[32,2048]{1,0:T(8,128)(2,1)S(1)}, bf16[32,2048]{1,0:T(8,128)(2,1)S(1)}, u32[]{:S(2)}, u32[]{:S(2)}) %collective-permute-start.1) | collective-permute-done | bytes 131104 | tf_op jit(solution)/shard_map/ppermute | solution.py:334
  10.9 0.3 shard_map.119.refs_12_.refs_3_
  11.3 0.2 collective-permute-start.11
  11.6 1.1 %collective-permute-start.6 = (bf16[32,2048]{1,0:T(8,128)(2,1)S(1)}, bf16[32,2048]{1,0:T(8,128)(2,1)S(1)}, u32[]{:S(2)}, u32[]{:S(2)}) collective-permute-start(bf16[32,2048]{1,0:T(8,128)(2,1)S(1)} %collective-permute-done.2.refs_3_), channel_id=1, source_target_pairs={{0,1},{1,0},{2,3},{3,2},{4,5},{5,4},{6,7},{7,6},{8,9},{9,8},{10,11... | collective-permute-start | bytes 393224 | tf_op jit(solution)/shard_map/ppermute | solution.py:331
  12.7 0.5 %collective-permute-start.4 = (bf16[32,2048]{1,0:T(8,128)(2,1)S(1)}, bf16[32,2048]{1,0:T(8,128)(2,1)S(1)}, u32[]{:S(2)}, u32[]{:S(2)}) collective-permute-start(bf16[32,2048]{1,0:T(8,128)(2,1)S(1)} %collective-permute-done.refs_1_), channel_id=1, source_target_pairs={{0,1},{1,0},{2,3},{3,2},{4,5},{5,4},{6,7},{7,6},{8,9},{9,8},{10,11... | collective-permute-start | bytes 393224 | tf_op jit(solution)/shard_map/ppermute | solution.py:331
  13.5 2.8 %collective-permute-done.11.refs_8_ = bf16[128,256]{1,0:T(8,128)(2,1)S(1)} collective-permute-done((bf16[128,256]{1,0:T(8,128)(2,1)S(1)}, bf16[128,256]{1,0:T(8,128)(2,1)S(1)}, u32[]{:S(2)}, u32[]{:S(2)}) %collective-permute-start.11) | collective-permute-done | bytes 65568 | tf_op jit(solution)/shard_map/ppermute | solution.py:338
  16.3 2.2 %collective-permute-start.8 = (bf16[128,256]{1,0:T(8,128)(2,1)S(1)}, bf16[128,256]{1,0:T(8,128)(2,1)S(1)}, u32[]{:S(2)}, u32[]{:S(2)}) collective-permute-start(bf16[128,256]{1,0:T(8,128)(2,1)S(1)} %shard_map.119.refs_12_.refs_3_), channel_id=1, source_target_pairs={{0,1},{1,0},{2,3},{3,2},{4,5},{5,4},{6,7},{7,6},{8,9},{9,8},{10,11... | collective-permute-start | bytes 196616 | tf_op jit(solution)/shard_map/ppermute | solution.py:331
  18.5 1.3 %collective-permute-start.12 = (bf16[128,256]{1,0:T(8,128)(2,1)S(1)}, bf16[128,256]{1,0:T(8,128)(2,1)S(1)}, u32[]{:S(2)}, u32[]{:S(2)}) collective-permute-start(bf16[128,256]{1,0:T(8,128)(2,1)S(1)} %collective-permute-done.11.refs_8_), channel_id=1, source_target_pairs={{0,1},{1,0},{2,3},{3,2},{4,5},{5,4},{6,7},{7,6},{8,9},{9,8},{10,11... | collective-permute-start | bytes 196616 | tf_op jit(solution)/shard_map/ppermute | solution.py:331
  19.8 1.0 %shard_map.120 = (bf16[256,256]{1,0:T(8,128)(2,1)S(1)}, bf16[256,128]{1,0:T(8,128)(2,1)S(1)}, bf16[256,128]{1,0:T(8,128)(2,1)S(1)}, bf16[144,256]{1,0:T(8,128)(2,1)S(1)}) custom-call(bf16[32,2048]{1,0:T(8,128)(2,1)S(1)} %shard_map.118.refs_0_, bf16[32,2048]{1,0:T(8,128)(2,1)S(1)} %collective-permute-done.refs_1_, ...), custom_call_target="tpu_custom_call" | custom-call | flops 2000000000 | tf_op jit(solution)/shard_map/pallas_call | solution.py:346
  20.8 1.3 %collective-permute-start.7 = (bf16[144,256]{1,0:T(8,128)(2,1)S(1)}, bf16[144,256]{1,0:T(8,128)(2,1)S(1)}, u32[]{:S(2)}, u32[]{:S(2)}) collective-permute-start(bf16[144,256]{1,0:T(8,128)(2,1)S(1)} %get-tuple-element.26), channel_id=1, source_target_pairs={{0,8},{8,16},{16,24},{1,9},{9,17},{17,25},{2,10},{10,18},{18,26},{... | collective-permute-start | bytes 221192 | tf_op jit(solution)/shard_map/ppermute | solution.py:338
  22.2 0.8 %shard_map.123 = (f32[512,128]{1,0:T(8,128)S(1)}, f32[512,128]{1,0:T(8,128)S(1)}, f32[512,128]{1,0:T(8,128)S(1)}, f32[2,256,8]{2,1,0:T(8,128)S(1)}) custom-call(bf16[256,256]{1,0:T(8,128)(2,1)S(1)} %get-tuple-element.23.refs_0_, f32[16,1024]{1,0:T(8,128)S(1)} %copy-done.9, f32[256,256]{1,0:T(8,128)S(1)} %shard_map.122.refs_2_, ...), custom_call_target="tpu_custom_call" | custom-call | flops 2000000000 | tf_op jit(solution)/shard_map/pallas_call | solution.py:346
  23.0 0.8 %shard_map.124 = (f32[512,128]{1,0:T(8,128)S(1)}, f32[512,128]{1,0:T(8,128)S(1)}, f32[512,128]{1,0:T(8,128)S(1)}) custom-call(bf16[256,256]{1,0:T(8,128)(2,1)S(1)} %get-tuple-element.23.refs_0_, f32[16,1024]{1,0:T(8,128)S(1)} %copy-done.9, f32[2,256,8]{2,1,0:T(8,128)S(1)} %get-tuple-element.27.refs_2_.refs_3_, f32[512,128]{1,0:T(8,128)S(1)} %get-tuple-element.28.refs_3_, ...), custom_call_target="tpu_custom_call" | custom-call | flops 2000000000 | tf_op jit(solution)/shard_map/pallas_call | solution.py:346
  23.8 2.1 %collective-permute-done.7.risen_ref.refs_7_ = bf16[144,256]{1,0:T(8,128)(2,1)S(1)} collective-permute-done((bf16[144,256]{1,0:T(8,128)(2,1)S(1)}, bf16[144,256]{1,0:T(8,128)(2,1)S(1)}, u32[]{:S(2)}, u32[]{:S(2)}) %collective-permute-start.7) | collective-permute-done | bytes 73760 | tf_op jit(solution)/shard_map/ppermute | solution.py:338
  25.9 1.6 %collective-permute-start.13 = (bf16[144,256]{1,0:T(8,128)(2,1)S(1)}, bf16[144,256]{1,0:T(8,128)(2,1)S(1)}, u32[]{:S(2)}, u32[]{:S(2)}) collective-permute-start(bf16[144,256]{1,0:T(8,128)(2,1)S(1)} %collective-permute-done.7.risen_ref.refs_7_), channel_id=1, source_target_pairs={{0,1},{1,0},{2,3},{3,2},{4,5},{5,4},{6,7},{7,6},{8,9},{9,8},{10,11... | collective-permute-start | bytes 221192 | tf_op jit(solution)/shard_map/ppermute | solution.py:331
  27.7 0.8 %collective-permute-done.13.refs_8_ = bf16[144,256]{1,0:T(8,128)(2,1)S(1)} collective-permute-done((bf16[144,256]{1,0:T(8,128)(2,1)S(1)}, bf16[144,256]{1,0:T(8,128)(2,1)S(1)}, u32[]{:S(2)}, u32[]{:S(2)}) %collective-permute-start.13) | collective-permute-done | bytes 73760 | tf_op jit(solution)/shard_map/ppermute | solution.py:331
  28.5 0.9 %shard_map.127 = (bf16[32,2048]{1,0:T(8,128)(2,1)S(1)}, bf16[96,2048]{1,0:T(8,128)(2,1)S(1)}) custom-call(bf16[256,256]{1,0:T(8,128)(2,1)S(1)} %get-tuple-element.23.refs_0_, bf16[256,128]{1,0:T(8,128)(2,1)S(1)} %shard_map.121.refs_1_, f32[16,1024]{1,0:T(8,128)S(1)} %copy-done.9, f32[2,256,8]{2,1,0:T(8,128)S(1)} %get-tuple-element.27.refs_2_.refs_3_, ...), custom_call_target="tpu_custom_call" | custom-call | flops 2000000000 | tf_op jit(solution)/shard_map/pallas_call | solution.py:346
  29.4 0.4 %collective-permute-start.16 = (bf16[96,2048]{1,0:T(8,128)(2,1)S(1)}, bf16[96,2048]{1,0:T(8,128)(2,1)S(1)}, u32[]{:S(2)}, u32[]{:S(2)}) collective-permute-start(bf16[96,2048]{1,0:T(8,128)(2,1)S(1)} %get-tuple-element.37), channel_id=1, source_target_pairs={{0,1},{1,0},{2,3},{3,2},{4,5},{5,4},{6,7},{7,6},{8,9},{9,8},{10,11... | collective-permute-start | bytes 1179656 | tf_op jit(solution)/shard_map/ppermute | solution.py:331
  30.0 0.9 %shard_map.126 = (bf16[32,2048]{1,0:T(8,128)(2,1)S(1)}, bf16[96,2048]{1,0:T(8,128)(2,1)S(1)}) custom-call(bf16[256,256]{1,0:T(8,128)(2,1)S(1)} %get-tuple-element.23.refs_0_, bf16[256,128]{1,0:T(8,128)(2,1)S(1)} %shard_map.121.refs_1_, f32[16,1024]{1,0:T(8,128)S(1)} %copy-done.9, f32[2,256,8]{2,1,0:T(8,128)S(1)} %get-tuple-element.27.refs_2_.refs_3_, ...), custom_call_target="tpu_custom_call" | custom-call | flops 2000000000 | tf_op jit(solution)/shard_map/pallas_call | solution.py:346
  30.9 0.5 %collective-permute-done.14.got_ref = bf16[32,2048]{1,0:T(8,128)(2,1)S(1)} collective-permute-done((bf16[32,2048]{1,0:T(8,128)(2,1)S(1)}, bf16[32,2048]{1,0:T(8,128)(2,1)S(1)}, u32[]{:S(2)}, u32[]{:S(2)}) %collective-permute-start.14) | collective-permute-done | bytes 131104 | tf_op jit(solution)/shard_map/ppermute | solution.py:331
  31.4 1.3 %collective-permute-start.15 = (bf16[32,2048]{1,0:T(8,128)(2,1)S(1)}, bf16[32,2048]{1,0:T(8,128)(2,1)S(1)}, u32[]{:S(2)}, u32[]{:S(2)}) collective-permute-start(bf16[32,2048]{1,0:T(8,128)(2,1)S(1)} %shard_map.128), channel_id=1, source_target_pairs={{0,6},{2,4},{4,2},{6,0},{1,7},{3,5},{5,3},{7,1},{8,14},{10,12},{12... | collective-permute-start | bytes 393224 | tf_op jit(solution)/shard_map/ppermute | solution.py:334
  32.8 0.3 collective-permute-start.17
  33.1 1.2 %collective-permute-start.18 = (bf16[32,2048]{1,0:T(8,128)(2,1)S(1)}, bf16[32,2048]{1,0:T(8,128)(2,1)S(1)}, u32[]{:S(2)}, u32[]{:S(2)}) collective-permute-start(bf16[32,2048]{1,0:T(8,128)(2,1)S(1)} %get-tuple-element.39), channel_id=1, source_target_pairs={{0,2},{2,0},{4,6},{6,4},{1,3},{3,1},{5,7},{7,5},{8,10},{10,8},{12,... | collective-permute-start | bytes 393224 | tf_op jit(solution)/shard_map/ppermute | solution.py:334
  34.3 2.8 %collective-permute-done.15.refs_0_ = bf16[32,2048]{1,0:T(8,128)(2,1)S(1)} collective-permute-done((bf16[32,2048]{1,0:T(8,128)(2,1)S(1)}, bf16[32,2048]{1,0:T(8,128)(2,1)S(1)}, u32[]{:S(2)}, u32[]{:S(2)}) %collective-permute-start.15) | collective-permute-done | bytes 131104 | tf_op jit(solution)/shard_map/ppermute | solution.py:334
  37.1 3.5 %collective-permute-done.17.refs_1_ = bf16[32,2048]{1,0:T(8,128)(2,1)S(1)} collective-permute-done((bf16[32,2048]{1,0:T(8,128)(2,1)S(1)}, bf16[32,2048]{1,0:T(8,128)(2,1)S(1)}, u32[]{:S(2)}, u32[]{:S(2)}) %collective-permute-start.17) | collective-permute-done | bytes 131104 | tf_op jit(solution)/shard_map/ppermute | solution.py:334
  40.6 0.7 %shard_map.130 = bf16[32,2048]{1,0:T(8,128)(2,1)} custom-call(bf16[32,2048]{1,0:T(8,128)(2,1)S(1)} %collective-permute-done.15.refs_0_, bf16[32,2048]{1,0:T(8,128)(2,1)S(1)} %collective-permute-done.17.refs_1_, bf16[32,2048]{1,0:T(8,128)(2,1)S(1)} %collective-permute-done.18.refs_2_, f32[32,2048]{1,0:T(8,128)S(1)} %get-tuple-element.40.refs_3_), custom_call_target="tpu_custom_call" | custom-call | tf_op jit(solution)/shard_map/pallas_call | solution.py:346
  (43 shorter events, 0.7 us)
Async XLA Ops:
  0.0 0.9 %copy-start.8 = (bf16[32,2048]{1,0:T(8,128)(2,1)S(1)}, bf16[32,2048]{1,0:T(8,128)(2,1)}, u32[]{:S(2)}) copy-start(bf16[32,2048]{1,0:T(8,128)(2,1)} %tokens_ref.1) | copy-start | bytes 393220
  0.9 0.7 %copy-start.10 = (f32[2048]{0:T(1024)S(1)}, f32[2048]{0:T(1024)}, u32[]{:S(2)}) copy-start(f32[2048]{0:T(1024)} %param.13) | copy-start | bytes 24580
  1.6 9.3 %copy-start.3 = (bf16[2048,128]{1,0:T(8,128)(2,1)S(1)}, bf16[2048,128]{1,0:T(8,128)(2,1)}, u32[]{:S(2)}) copy-start(bf16[2048,128]{1,0:T(8,128)(2,1)} %refs_4_.1) | copy-start | bytes 1572868
  1.6 9.3 %copy-start.4 = (bf16[2048,128]{1,0:T(8,128)(2,1)S(1)}, bf16[2048,128]{1,0:T(8,128)(2,1)}, u32[]{:S(2)}) copy-start(bf16[2048,128]{1,0:T(8,128)(2,1)} %refs_5_.1) | copy-start | bytes 1572868
  1.7 5.3 %collective-permute-start.2 = (bf16[32,2048]{1,0:T(8,128)(2,1)S(1)}, bf16[32,2048]{1,0:T(8,128)(2,1)S(1)}, u32[]{:S(2)}, u32[]{:S(2)}) collective-permute-start(bf16[32,2048]{1,0:T(8,128)(2,1)S(1)} %shard_map.118.refs_0_), channel_id=1, source_target_pairs={{0,6},{2,4},{4,2},{6,0},{1,7},{3,5},{5,3},{7,1},{8,14},{10,12},{12... | collective-permute-start | bytes 393224 | tf_op jit(solution)/shard_map/ppermute | solution.py:334
  3.0 7.9 %collective-permute-start.1 = (bf16[32,2048]{1,0:T(8,128)(2,1)S(1)}, bf16[32,2048]{1,0:T(8,128)(2,1)S(1)}, u32[]{:S(2)}, u32[]{:S(2)}) collective-permute-start(bf16[32,2048]{1,0:T(8,128)(2,1)S(1)} %shard_map.118.refs_0_), channel_id=1, source_target_pairs={{0,4},{2,6},{4,0},{6,2},{1,5},{3,7},{5,1},{7,3},{8,12},{10,14},{12... | collective-permute-start | bytes 393224 | tf_op jit(solution)/shard_map/ppermute | solution.py:334
  3.2 7.7 %collective-permute-start = (bf16[32,2048]{1,0:T(8,128)(2,1)S(1)}, bf16[32,2048]{1,0:T(8,128)(2,1)S(1)}, u32[]{:S(2)}, u32[]{:S(2)}) collective-permute-start(bf16[32,2048]{1,0:T(8,128)(2,1)S(1)} %shard_map.118.refs_0_), channel_id=1, source_target_pairs={{0,2},{2,0},{4,6},{6,4},{1,3},{3,1},{5,7},{7,5},{8,10},{10,8},{12,... | collective-permute-start | bytes 393224 | tf_op jit(solution)/shard_map/ppermute | solution.py:334
  4.5 8.3 %collective-permute-start.3 = (bf16[32,2048]{1,0:T(8,128)(2,1)S(1)}, bf16[32,2048]{1,0:T(8,128)(2,1)S(1)}, u32[]{:S(2)}, u32[]{:S(2)}) collective-permute-start(bf16[32,2048]{1,0:T(8,128)(2,1)S(1)} %shard_map.118.refs_0_), channel_id=1, source_target_pairs={{0,1},{1,0},{2,3},{3,2},{4,5},{5,4},{6,7},{7,6},{8,9},{9,8},{10,11... | collective-permute-start | bytes 393224 | tf_op jit(solution)/shard_map/ppermute | solution.py:331
  11.3 2.0 %copy-start = (bf16[256,2048]{1,0:T(8,128)(2,1)S(1)}, bf16[256,2048]{1,0:T(8,128)(2,1)}, u32[]{:S(2)}) copy-start(bf16[256,2048]{1,0:T(8,128)(2,1)} %low_ref.1) | copy-start | bytes 3145732
  11.3 2.0 %copy-start.1 = (bf16[128,2048]{1,0:T(8,128)(2,1)S(1)}, bf16[128,2048]{1,0:T(8,128)(2,1)}, u32[]{:S(2)}) copy-start(bf16[128,2048]{1,0:T(8,128)(2,1)} %top_ref.1) | copy-start | bytes 1572868
  11.3 5.0 %collective-permute-start.11 = (bf16[128,256]{1,0:T(8,128)(2,1)S(1)}, bf16[128,256]{1,0:T(8,128)(2,1)S(1)}, u32[]{:S(2)}, u32[]{:S(2)}) collective-permute-start(bf16[128,256]{1,0:T(8,128)(2,1)S(1)} %shard_map.119.refs_12_.refs_3_), channel_id=1, source_target_pairs={{0,24},{8,0},{16,8},{24,16},{1,25},{9,1},{17,9},{25,17},{2,26},{10... | collective-permute-start | bytes 196616 | tf_op jit(solution)/shard_map/ppermute | solution.py:338
  11.5 6.9 %collective-permute-start.9 = (bf16[128,256]{1,0:T(8,128)(2,1)S(1)}, bf16[128,256]{1,0:T(8,128)(2,1)S(1)}, u32[]{:S(2)}, u32[]{:S(2)}) collective-permute-start(bf16[128,256]{1,0:T(8,128)(2,1)S(1)} %shard_map.119.refs_12_.refs_3_), channel_id=1, source_target_pairs={{0,16},{8,24},{16,0},{24,8},{1,17},{9,25},{17,1},{25,9},{2,18},{10... | collective-permute-start | bytes 196616 | tf_op jit(solution)/shard_map/ppermute | solution.py:338
  11.6 8.2 %collective-permute-start.6 = (bf16[32,2048]{1,0:T(8,128)(2,1)S(1)}, bf16[32,2048]{1,0:T(8,128)(2,1)S(1)}, u32[]{:S(2)}, u32[]{:S(2)}) collective-permute-start(bf16[32,2048]{1,0:T(8,128)(2,1)S(1)} %collective-permute-done.2.refs_3_), channel_id=1, source_target_pairs={{0,1},{1,0},{2,3},{3,2},{4,5},{5,4},{6,7},{7,6},{8,9},{9,8},{10,11... | collective-permute-start | bytes 393224 | tf_op jit(solution)/shard_map/ppermute | solution.py:331
  12.7 7.1 %collective-permute-start.5 = (bf16[32,2048]{1,0:T(8,128)(2,1)S(1)}, bf16[32,2048]{1,0:T(8,128)(2,1)S(1)}, u32[]{:S(2)}, u32[]{:S(2)}) collective-permute-start(bf16[32,2048]{1,0:T(8,128)(2,1)S(1)} %collective-permute-done.1.refs_2_), channel_id=1, source_target_pairs={{0,1},{1,0},{2,3},{3,2},{4,5},{5,4},{6,7},{7,6},{8,9},{9,8},{10,11... | collective-permute-start | bytes 393224 | tf_op jit(solution)/shard_map/ppermute | solution.py:331
  12.7 7.1 %collective-permute-start.4 = (bf16[32,2048]{1,0:T(8,128)(2,1)S(1)}, bf16[32,2048]{1,0:T(8,128)(2,1)S(1)}, u32[]{:S(2)}, u32[]{:S(2)}) collective-permute-start(bf16[32,2048]{1,0:T(8,128)(2,1)S(1)} %collective-permute-done.refs_1_), channel_id=1, source_target_pairs={{0,1},{1,0},{2,3},{3,2},{4,5},{5,4},{6,7},{7,6},{8,9},{9,8},{10,11... | collective-permute-start | bytes 393224 | tf_op jit(solution)/shard_map/ppermute | solution.py:331
  13.3 6.5 %copy-start.2 = (bf16[2048,256]{1,0:T(8,128)(2,1)S(1)}, bf16[2048,256]{1,0:T(8,128)(2,1)}, u32[]{:S(2)}) copy-start(bf16[2048,256]{1,0:T(8,128)(2,1)} %refs_8_.1) | copy-start | bytes 3145732
  13.3 6.5 %copy-start.5 = (bf16[2048,128]{1,0:T(8,128)(2,1)S(1)}, bf16[2048,128]{1,0:T(8,128)(2,1)}, u32[]{:S(2)}) copy-start(bf16[2048,128]{1,0:T(8,128)(2,1)} %refs_9_.1) | copy-start | bytes 1572868
  13.3 6.5 %copy-start.6 = (bf16[2048,128]{1,0:T(8,128)(2,1)S(1)}, bf16[2048,128]{1,0:T(8,128)(2,1)}, u32[]{:S(2)}) copy-start(bf16[2048,128]{1,0:T(8,128)(2,1)} %refs_10_.1) | copy-start | bytes 1572868
  13.3 6.5 %copy-start.7 = (bf16[2048,128]{1,0:T(8,128)(2,1)S(1)}, bf16[2048,128]{1,0:T(8,128)(2,1)}, u32[]{:S(2)}) copy-start(bf16[2048,128]{1,0:T(8,128)(2,1)} %refs_11_.1) | copy-start | bytes 1572868
  13.5 8.7 %copy-start.9 = (f32[16,1024]{1,0:T(8,128)S(1)}, f32[16,1024]{1,0:T(8,128)}, u32[]{:S(2)}) copy-start(f32[16,1024]{1,0:T(8,128)} %refs_2_.3) | copy-start | bytes 196612
  16.3 5.8 %collective-permute-start.8 = (bf16[128,256]{1,0:T(8,128)(2,1)S(1)}, bf16[128,256]{1,0:T(8,128)(2,1)S(1)}, u32[]{:S(2)}, u32[]{:S(2)}) collective-permute-start(bf16[128,256]{1,0:T(8,128)(2,1)S(1)} %shard_map.119.refs_12_.refs_3_), channel_id=1, source_target_pairs={{0,1},{1,0},{2,3},{3,2},{4,5},{5,4},{6,7},{7,6},{8,9},{9,8},{10,11... | collective-permute-start | bytes 196616 | tf_op jit(solution)/shard_map/ppermute | solution.py:331
  18.5 4.5 %collective-permute-start.12 = (bf16[128,256]{1,0:T(8,128)(2,1)S(1)}, bf16[128,256]{1,0:T(8,128)(2,1)S(1)}, u32[]{:S(2)}, u32[]{:S(2)}) collective-permute-start(bf16[128,256]{1,0:T(8,128)(2,1)S(1)} %collective-permute-done.11.refs_8_), channel_id=1, source_target_pairs={{0,1},{1,0},{2,3},{3,2},{4,5},{5,4},{6,7},{7,6},{8,9},{9,8},{10,11... | collective-permute-start | bytes 196616 | tf_op jit(solution)/shard_map/ppermute | solution.py:331
  19.8 3.2 %collective-permute-start.10 = (bf16[128,256]{1,0:T(8,128)(2,1)S(1)}, bf16[128,256]{1,0:T(8,128)(2,1)S(1)}, u32[]{:S(2)}, u32[]{:S(2)}) collective-permute-start(bf16[128,256]{1,0:T(8,128)(2,1)S(1)} %collective-permute-done.9.refs_6_), channel_id=1, source_target_pairs={{0,1},{1,0},{2,3},{3,2},{4,5},{5,4},{6,7},{7,6},{8,9},{9,8},{10,11... | collective-permute-start | bytes 196616 | tf_op jit(solution)/shard_map/ppermute | solution.py:331
  20.8 5.1 %collective-permute-start.7 = (bf16[144,256]{1,0:T(8,128)(2,1)S(1)}, bf16[144,256]{1,0:T(8,128)(2,1)S(1)}, u32[]{:S(2)}, u32[]{:S(2)}) collective-permute-start(bf16[144,256]{1,0:T(8,128)(2,1)S(1)} %get-tuple-element.26), channel_id=1, source_target_pairs={{0,8},{8,16},{16,24},{1,9},{9,17},{17,25},{2,10},{10,18},{18,26},{... | collective-permute-start | bytes 221192 | tf_op jit(solution)/shard_map/ppermute | solution.py:338
  23.0 4.6 %copy-start.11 = (bf16[3,1024]{1,0:T(4,128)(2,1)S(1)}, bf16[3,1024]{1,0:T(4,128)(2,1)}, u32[]{:S(2)}) copy-start(bf16[3,1024]{1,0:T(4,128)(2,1)} %taps_ref.1) | copy-start | bytes 18436
  25.9 2.6 %collective-permute-start.13 = (bf16[144,256]{1,0:T(8,128)(2,1)S(1)}, bf16[144,256]{1,0:T(8,128)(2,1)S(1)}, u32[]{:S(2)}, u32[]{:S(2)}) collective-permute-start(bf16[144,256]{1,0:T(8,128)(2,1)S(1)} %collective-permute-done.7.risen_ref.refs_7_), channel_id=1, source_target_pairs={{0,1},{1,0},{2,3},{3,2},{4,5},{5,4},{6,7},{7,6},{8,9},{9,8},{10,11... | collective-permute-start | bytes 221192 | tf_op jit(solution)/shard_map/ppermute | solution.py:331
  29.4 3.3 %collective-permute-start.16 = (bf16[96,2048]{1,0:T(8,128)(2,1)S(1)}, bf16[96,2048]{1,0:T(8,128)(2,1)S(1)}, u32[]{:S(2)}, u32[]{:S(2)}) collective-permute-start(bf16[96,2048]{1,0:T(8,128)(2,1)S(1)} %get-tuple-element.37), channel_id=1, source_target_pairs={{0,1},{1,0},{2,3},{3,2},{4,5},{5,4},{6,7},{7,6},{8,9},{9,8},{10,11... | collective-permute-start | bytes 1179656 | tf_op jit(solution)/shard_map/ppermute | solution.py:331
  29.8 1.6 %collective-permute-start.14 = (bf16[32,2048]{1,0:T(8,128)(2,1)S(1)}, bf16[32,2048]{1,0:T(8,128)(2,1)S(1)}, u32[]{:S(2)}, u32[]{:S(2)}) collective-permute-start(bf16[32,2048]{1,0:T(8,128)(2,1)S(1)} %get-tuple-element.35), channel_id=1, source_target_pairs={{0,1},{1,0},{2,3},{3,2},{4,5},{5,4},{6,7},{7,6},{8,9},{9,8},{10,11... | collective-permute-start | bytes 393224 | tf_op jit(solution)/shard_map/ppermute | solution.py:331
  31.4 5.7 %collective-permute-start.15 = (bf16[32,2048]{1,0:T(8,128)(2,1)S(1)}, bf16[32,2048]{1,0:T(8,128)(2,1)S(1)}, u32[]{:S(2)}, u32[]{:S(2)}) collective-permute-start(bf16[32,2048]{1,0:T(8,128)(2,1)S(1)} %shard_map.128), channel_id=1, source_target_pairs={{0,6},{2,4},{4,2},{6,0},{1,7},{3,5},{5,3},{7,1},{8,14},{10,12},{12... | collective-permute-start | bytes 393224 | tf_op jit(solution)/shard_map/ppermute | solution.py:334
  32.8 7.8 %collective-permute-start.17 = (bf16[32,2048]{1,0:T(8,128)(2,1)S(1)}, bf16[32,2048]{1,0:T(8,128)(2,1)S(1)}, u32[]{:S(2)}, u32[]{:S(2)}) collective-permute-start(bf16[32,2048]{1,0:T(8,128)(2,1)S(1)} %get-tuple-element.38), channel_id=1, source_target_pairs={{0,4},{2,6},{4,0},{6,2},{1,5},{3,7},{5,1},{7,3},{8,12},{10,14},{12... | collective-permute-start | bytes 393224 | tf_op jit(solution)/shard_map/ppermute | solution.py:334
  33.1 7.6 %collective-permute-start.18 = (bf16[32,2048]{1,0:T(8,128)(2,1)S(1)}, bf16[32,2048]{1,0:T(8,128)(2,1)S(1)}, u32[]{:S(2)}, u32[]{:S(2)}) collective-permute-start(bf16[32,2048]{1,0:T(8,128)(2,1)S(1)} %get-tuple-element.39), channel_id=1, source_target_pairs={{0,2},{2,0},{4,6},{6,4},{1,3},{3,1},{5,7},{7,5},{8,10},{10,8},{12,... | collective-permute-start | bytes 393224 | tf_op jit(solution)/shard_map/ppermute | solution.py:334

commit v6 on v5

--- a/solution.py
+++ b/solution.py
@@ -129,8 +129,12 @@
 
 
 def early_kernel(*refs):
-    q_ref, gates_ref, mask_ref, near_ref, far_ref = refs[:5]
-    outs, (column_ref, key_ref, value_ref, natural_ref) = refs[5:8], refs[8:]
+    q_ref, gates_ref, mask_ref, taps_ref, near_ref, far_ref = refs[:6]
+    outs, (column_ref, tap_ref, key_ref, value_ref, natural_ref) = refs[6:9], refs[9:]
+    group = lax.axis_index("fs") * lax.axis_size("tp") + lax.axis_index("tp")
+    channels = tap_ref.shape[1]
+    lanes = pl.ds(pl.multiple_of(group * channels, channels), channels)
+    tap_ref[...] = taps_ref[:, lanes].astype(f32)
     place_pairs(((near_ref, far_ref),), key_ref, value_ref)
     z = lax.axis_index("sp")
     block_rows = q_ref.shape[0]
@@ -186,12 +190,15 @@
     ]
 
 
-def project_kernel(n_fs, *refs):
+def gathered(own, other):
+    return jnp.concatenate([ref[...] for ref in (*other[::-1], *own[::-1])], axis=0)
+
+
+def gate_kernel(n_fs, *refs):
     own, other = refs[:n_fs], refs[n_fs : 2 * n_fs]
-    w_query, w_post, w_pre, w_conv, pair_ref = refs[2 * n_fs : 2 * n_fs + 5]
-    q_ref, post_ref, mixed_ref, rise_ref = refs[2 * n_fs + 5 :]
+    w_pre, w_conv, pair_ref, mixed_ref, rise_ref = refs[2 * n_fs :]
     step = own[0].shape[0]
-    rows = jnp.concatenate([ref[...] for ref in (*other[::-1], *own[::-1])], axis=0)
+    rows = gathered(own, other)
     weight = jnp.concatenate([w_pre[...], w_conv[...]], axis=1)
     gated = jnp.dot(rows, weight, preferred_element_type=f32).astype(bf16).astype(f32)
     channels = w_pre.shape[1]
@@ -202,6 +209,11 @@
     rise_ref[:lane_rows] = pair_ref[...]
     last = mixed_ref[mixed_ref.shape[0] - EDGE :]
     rise_ref[lane_rows:] = jnp.concatenate([last] * (rise_ref.shape[1] // channels), axis=1)
+
+
+def query_kernel(n_fs, *refs):
+    rows = gathered(refs[:n_fs], refs[n_fs : 2 * n_fs])
+    w_query, w_post, q_ref, post_ref = refs[2 * n_fs :]
     q_ref[...] = jnp.dot(rows, w_query[...], preferred_element_type=f32).astype(bf16)
     post_ref[...] = jnp.dot(rows, w_post[...], preferred_element_type=f32).astype(bf16)
 
@@ -213,13 +225,11 @@
 
 def conv_kernel(n_fs, post_ref, mixed_ref, risen_ref, taps_ref, out_ref, extended_ref, sum_ref):
     block_rows, channels = mixed_ref.shape
-    group = lax.axis_index("fs") * lax.axis_size("tp") + lax.axis_index("tp")
-    lanes = pl.ds(pl.multiple_of(group * channels, channels), channels)
     taps = taps_ref.shape[0]
     halo = risen_ref[risen_ref.shape[0] - EDGE :, :channels].astype(f32)
     extended_ref[0:EDGE] = jnp.where(lax.axis_index("sp") > 0, halo, 0.0)
     extended_ref[EDGE:] = mixed_ref[...].astype(f32)
-    tap_rows = taps_ref[:, lanes].astype(f32)
+    tap_rows = taps_ref[...]
     first = EDGE - (taps - 1)
     conv_sum = tap_rows[0:1] * extended_ref[first : first + block_rows]
     for i in range(1, taps):
@@ -379,36 +389,45 @@
     for shift in range(2, n_sp):
         piece = raised(pair, shift)
         halves += [piece, swapped(piece)]
-    queries, post, mixed, rise = call(
-        functools.partial(project_kernel, n_fs),
-        (
-            shape_of(block_rows, heads * head_dim),
-            shape_of(block_rows, channels),
-            shape_of(block_rows, channels),
-            shape_of(lane_rows + EDGE, 2 * head_dim),
-        ),
+    mixed, rise = call(
+        functools.partial(gate_kernel, n_fs),
+        (shape_of(block_rows, channels), shape_of(lane_rows + EDGE, 2 * head_dim)),
+        [],
+        16,
+        *own,
+        *other,
+        w_pre,
+        w_conv,
+        pair,
+        work=SMALL_WORK,
+    )
+    queries, post = call(
+        functools.partial(query_kernel, n_fs),
+        (shape_of(block_rows, heads * head_dim), shape_of(block_rows, channels)),
         [],
         16,
         *own,
         *other,
         w_query,
         w_post,
-        w_pre,
-        w_conv,
-        pair,
         work=SMALL_WORK,
     )
     near = raised(rise, 1)
     far = swapped(near)
     held_shapes = (shape_of(heads * block_rows, head_dim, f32),) * 3
-    *held, column = call(
+    *held, column, tap_rows = call(
         early_kernel,
-        (*held_shapes, jax.ShapeDtypeStruct((heads, block_rows, 8), f32)),
+        (
+            *held_shapes,
+            jax.ShapeDtypeStruct((heads, block_rows, 8), f32),
+            shape_of(taps.shape[0], channels, f32),
+        ),
         [pltpu.VMEM((block_rows, head_dim), bf16)] * 2 + [pltpu.VMEM((block_rows, 8), f32)],
         16,
         queries,
         gates,
         mask,
+        taps,
         *halves[:2],
         work=SMALL_WORK,
     )
@@ -432,7 +451,7 @@
         post,
         mixed,
         near,
-        taps,
+        tap_rows,
         work=SMALL_WORK,
     )
     w_out = call(

time: 41.6 us -> 41.1 us (0.988)
  the two profiles are of different devices: /device:TPU:27 before, /device:TPU:29 now
where the time goes in v6:
time: 41.1 us; the launch traced here: 40.9 us
  waiting for transfers between devices  17 us (41%)
  starting transfers between devices  16 us (39%)
  Pallas kernels  6.04 us (15%)
  local copies, waits for them, and re-layouts  1.66 us (4%)
    ppermute x6, waiting for transfers between devices, crossed(): return lax.ppermute(x, 'fs', [(i, i ^ k) for i in range(n_fs)])  11.3 us
    ppermute x10, starting transfers between devices, swapped(): return lax.ppermute(x, 'tp', [(0, 1), (1, 0)])  8.77 us
    pallas_call x14, Pallas kernels, call(): pl.pallas_call(kernel, out_shape=out_shape, scratch_shapes=scratch, compi...  6.04 us
    ppermute x6, starting transfers between devices, crossed(): return lax.ppermute(x, 'fs', [(i, i ^ k) for i in range(n_fs)])  5.49 us
    ppermute x3, waiting for transfers between devices, raised(): return lax.ppermute(x, 'sp', route)  4.31 us
    ppermute x3, starting transfers between devices, raised(): return lax.ppermute(x, 'sp', route)  1.71 us
    unnamed x24, local copies, waits for them, and re-layouts  1.66 us
    ppermute x10, waiting for transfers between devices, swapped(): return lax.ppermute(x, 'tp', [(0, 1), (1, 0)])  1.39 us
  transfers between devices with their start and end apart: 19, of which 8 were waited for; matrix products, arithmetic and copies ran while one was open for 0% of the time, Pallas kernels for 10%

profile of v6, /device:TPU:29, one launch (start us, length us, event | category | flops | bytes accessed | tf_op | source)
XLA Modules:
  0.0 40.9 jit_solution(13903115097019057030)
XLA Ops:
  0.0 0.9 %copy-done.8 = bf16[32,2048]{1,0:T(8,128)(2,1)S(1)} copy-done((bf16[32,2048]{1,0:T(8,128)(2,1)S(1)}, bf16[32,2048]{1,0:T(8,128)(2,1)}, u32[]{:S(2)}) %copy-start.8) | copy-done | bytes 131096
  0.9 0.7 %copy-done.10 = f32[2048]{0:T(1024)S(1)} copy-done((f32[2048]{0:T(1024)S(1)}, f32[2048]{0:T(1024)}, u32[]{:S(2)}) %copy-start.10) | copy-done | bytes 8216
  1.7 1.2 %collective-permute-start.2 = (bf16[32,2048]{1,0:T(8,128)(2,1)S(1)}, bf16[32,2048]{1,0:T(8,128)(2,1)S(1)}, u32[]{:S(2)}, u32[]{:S(2)}) collective-permute-start(bf16[32,2048]{1,0:T(8,128)(2,1)S(1)} %shard_map.118.refs_0_), channel_id=1, source_target_pairs={{0,6},{2,4},{4,2},{6,0},{1,7},{3,5},{5,3},{7,1},{8,14},{10,12},{12... | collective-permute-start | bytes 393224 | tf_op jit(solution)/shard_map/ppermute | solution.py:344
  3.0 1.2 %collective-permute-start.1 = (bf16[32,2048]{1,0:T(8,128)(2,1)S(1)}, bf16[32,2048]{1,0:T(8,128)(2,1)S(1)}, u32[]{:S(2)}, u32[]{:S(2)}) collective-permute-start(bf16[32,2048]{1,0:T(8,128)(2,1)S(1)} %shard_map.118.refs_0_), channel_id=1, source_target_pairs={{0,4},{2,6},{4,0},{6,2},{1,5},{3,7},{5,1},{7,3},{8,12},{10,14},{12... | collective-permute-start | bytes 393224 | tf_op jit(solution)/shard_map/ppermute | solution.py:344
  4.2 0.3 collective-permute-start
  4.5 1.5 %collective-permute-start.3 = (bf16[32,2048]{1,0:T(8,128)(2,1)S(1)}, bf16[32,2048]{1,0:T(8,128)(2,1)S(1)}, u32[]{:S(2)}, u32[]{:S(2)}) collective-permute-start(bf16[32,2048]{1,0:T(8,128)(2,1)S(1)} %shard_map.118.refs_0_), channel_id=1, source_target_pairs={{0,1},{1,0},{2,3},{3,2},{4,5},{5,4},{6,7},{7,6},{8,9},{9,8},{10,11... | collective-permute-start | bytes 393224 | tf_op jit(solution)/shard_map/ppermute | solution.py:341
  6.0 1.1 %collective-permute-done.2.refs_3_ = bf16[32,2048]{1,0:T(8,128)(2,1)S(1)} collective-permute-done((bf16[32,2048]{1,0:T(8,128)(2,1)S(1)}, bf16[32,2048]{1,0:T(8,128)(2,1)S(1)}, u32[]{:S(2)}, u32[]{:S(2)}) %collective-permute-start.2) | collective-permute-done | bytes 131104 | tf_op jit(solution)/shard_map/ppermute | solution.py:344
  7.1 3.8 %collective-permute-done.1.refs_2_ = bf16[32,2048]{1,0:T(8,128)(2,1)S(1)} collective-permute-done((bf16[32,2048]{1,0:T(8,128)(2,1)S(1)}, bf16[32,2048]{1,0:T(8,128)(2,1)S(1)}, u32[]{:S(2)}, u32[]{:S(2)}) %collective-permute-start.1) | collective-permute-done | bytes 131104 | tf_op jit(solution)/shard_map/ppermute | solution.py:344
  10.9 0.3 shard_map.120.refs_10_.refs_4_
  11.3 0.2 collective-permute-start.11
  11.6 1.0 %collective-permute-start.6 = (bf16[32,2048]{1,0:T(8,128)(2,1)S(1)}, bf16[32,2048]{1,0:T(8,128)(2,1)S(1)}, u32[]{:S(2)}, u32[]{:S(2)}) collective-permute-start(bf16[32,2048]{1,0:T(8,128)(2,1)S(1)} %collective-permute-done.2.refs_3_), channel_id=1, source_target_pairs={{0,1},{1,0},{2,3},{3,2},{4,5},{5,4},{6,7},{7,6},{8,9},{9,8},{10,11... | collective-permute-start | bytes 393224 | tf_op jit(solution)/shard_map/ppermute | solution.py:341
  12.6 0.5 %collective-permute-start.4 = (bf16[32,2048]{1,0:T(8,128)(2,1)S(1)}, bf16[32,2048]{1,0:T(8,128)(2,1)S(1)}, u32[]{:S(2)}, u32[]{:S(2)}) collective-permute-start(bf16[32,2048]{1,0:T(8,128)(2,1)S(1)} %collective-permute-done.refs_1_), channel_id=1, source_target_pairs={{0,1},{1,0},{2,3},{3,2},{4,5},{5,4},{6,7},{7,6},{8,9},{9,8},{10,11... | collective-permute-start | bytes 393224 | tf_op jit(solution)/shard_map/ppermute | solution.py:341
  13.3 2.9 %collective-permute-done.11.refs_8_ = bf16[128,256]{1,0:T(8,128)(2,1)S(1)} collective-permute-done((bf16[128,256]{1,0:T(8,128)(2,1)S(1)}, bf16[128,256]{1,0:T(8,128)(2,1)S(1)}, u32[]{:S(2)}, u32[]{:S(2)}) %collective-permute-start.11) | collective-permute-done | bytes 65568 | tf_op jit(solution)/shard_map/ppermute | solution.py:348
  16.3 2.2 %collective-permute-start.8 = (bf16[128,256]{1,0:T(8,128)(2,1)S(1)}, bf16[128,256]{1,0:T(8,128)(2,1)S(1)}, u32[]{:S(2)}, u32[]{:S(2)}) collective-permute-start(bf16[128,256]{1,0:T(8,128)(2,1)S(1)} %shard_map.120.refs_10_.refs_4_), channel_id=1, source_target_pairs={{0,1},{1,0},{2,3},{3,2},{4,5},{5,4},{6,7},{7,6},{8,9},{9,8},{10,11... | collective-permute-start | bytes 196616 | tf_op jit(solution)/shard_map/ppermute | solution.py:341
  18.5 1.3 %collective-permute-start.12 = (bf16[128,256]{1,0:T(8,128)(2,1)S(1)}, bf16[128,256]{1,0:T(8,128)(2,1)S(1)}, u32[]{:S(2)}, u32[]{:S(2)}) collective-permute-start(bf16[128,256]{1,0:T(8,128)(2,1)S(1)} %collective-permute-done.11.refs_8_), channel_id=1, source_target_pairs={{0,1},{1,0},{2,3},{3,2},{4,5},{5,4},{6,7},{7,6},{8,9},{9,8},{10,11... | collective-permute-start | bytes 196616 | tf_op jit(solution)/shard_map/ppermute | solution.py:341
  19.8 0.4 %shard_map.121 = (bf16[256,128]{1,0:T(8,128)(2,1)S(1)}, bf16[144,256]{1,0:T(8,128)(2,1)S(1)}) custom-call(bf16[32,2048]{1,0:T(8,128)(2,1)S(1)} %shard_map.118.refs_0_, bf16[32,2048]{1,0:T(8,128)(2,1)S(1)} %collective-permute-done.refs_1_, bf16[32,2048]{1,0:T(8,128)(2,1)S(1)} %collective-permute-done.1.refs_2_, ...), custom_call_target="tpu_custom_call" | custom-call | flops 2000000000 | tf_op jit(solution)/shard_map/pallas_call | solution.py:356
  20.3 1.4 %collective-permute-start.7 = (bf16[144,256]{1,0:T(8,128)(2,1)S(1)}, bf16[144,256]{1,0:T(8,128)(2,1)S(1)}, u32[]{:S(2)}, u32[]{:S(2)}) collective-permute-start(bf16[144,256]{1,0:T(8,128)(2,1)S(1)} %get-tuple-element.27), channel_id=1, source_target_pairs={{0,8},{8,16},{16,24},{1,9},{9,17},{17,25},{2,10},{10,18},{18,26},{... | collective-permute-start | bytes 221192 | tf_op jit(solution)/shard_map/ppermute | solution.py:348
  21.7 0.7 %shard_map.119 = (bf16[256,256]{1,0:T(8,128)(2,1)S(1)}, bf16[256,128]{1,0:T(8,128)(2,1)S(1)}) custom-call(bf16[32,2048]{1,0:T(8,128)(2,1)S(1)} %shard_map.118.refs_0_, bf16[32,2048]{1,0:T(8,128)(2,1)S(1)} %collective-permute-done.refs_1_, bf16[32,2048]{1,0:T(8,128)(2,1)S(1)} %collective-permute-done.1.refs_2_, ...), custom_call_target="tpu_custom_call" | custom-call | flops 2000000000 | tf_op jit(solution)/shard_map/pallas_call | solution.py:356
  22.5 0.8 %shard_map.123 = (f32[512,128]{1,0:T(8,128)S(1)}, f32[512,128]{1,0:T(8,128)S(1)}, f32[512,128]{1,0:T(8,128)S(1)}, f32[2,256,8]{2,1,0:T(8,128)S(1)}, f32[3,128]{1,0:T(4,128)S(1)}) custom-call(bf16[256,256]{1,0:T(8,128)(2,1)S(1)} %get-tuple-element.24.refs_0_, f32[16,1024]{1,0:T(8,128)S(1)} %copy-done.9, f32[256,256]{1,0:T(8,128)S(1)} %shard_map.122.refs_2_, ...), custom_call_target="tpu_custom_call" | custom-call | flops 2000000000 | tf_op jit(solution)/shard_map/pallas_call | solution.py:356
  23.3 0.9 %shard_map.125 = (f32[512,128]{1,0:T(8,128)S(1)}, f32[512,128]{1,0:T(8,128)S(1)}, f32[512,128]{1,0:T(8,128)S(1)}) custom-call(bf16[256,256]{1,0:T(8,128)(2,1)S(1)} %get-tuple-element.24.refs_0_, f32[16,1024]{1,0:T(8,128)S(1)} %copy-done.9, f32[2,256,8]{2,1,0:T(8,128)S(1)} %get-tuple-element.29.refs_2_.refs_3_, f32[512,128]{1,0:T(8,128)S(1)} %get-tuple-element.30.refs_3_, ...), custom_call_target="tpu_custom_call" | custom-call | flops 2000000000 | tf_op jit(solution)/shard_map/pallas_call | solution.py:356
  24.1 1.4 %collective-permute-done.7.risen_ref.refs_7_ = bf16[144,256]{1,0:T(8,128)(2,1)S(1)} collective-permute-done((bf16[144,256]{1,0:T(8,128)(2,1)S(1)}, bf16[144,256]{1,0:T(8,128)(2,1)S(1)}, u32[]{:S(2)}, u32[]{:S(2)}) %collective-permute-start.7) | collective-permute-done | bytes 73760 | tf_op jit(solution)/shard_map/ppermute | solution.py:348
  25.5 1.6 %collective-permute-start.13 = (bf16[144,256]{1,0:T(8,128)(2,1)S(1)}, bf16[144,256]{1,0:T(8,128)(2,1)S(1)}, u32[]{:S(2)}, u32[]{:S(2)}) collective-permute-start(bf16[144,256]{1,0:T(8,128)(2,1)S(1)} %collective-permute-done.7.risen_ref.refs_7_), channel_id=1, source_target_pairs={{0,1},{1,0},{2,3},{3,2},{4,5},{5,4},{6,7},{7,6},{8,9},{9,8},{10,11... | collective-permute-start | bytes 221192 | tf_op jit(solution)/shard_map/ppermute | solution.py:341
  27.2 0.9 %collective-permute-done.13.refs_8_ = bf16[144,256]{1,0:T(8,128)(2,1)S(1)} collective-permute-done((bf16[144,256]{1,0:T(8,128)(2,1)S(1)}, bf16[144,256]{1,0:T(8,128)(2,1)S(1)}, u32[]{:S(2)}, u32[]{:S(2)}) %collective-permute-start.13) | collective-permute-done | bytes 73760 | tf_op jit(solution)/shard_map/ppermute | solution.py:341
  28.1 0.9 %shard_map.128 = (bf16[32,2048]{1,0:T(8,128)(2,1)S(1)}, bf16[96,2048]{1,0:T(8,128)(2,1)S(1)}) custom-call(bf16[256,256]{1,0:T(8,128)(2,1)S(1)} %get-tuple-element.24.refs_0_, bf16[256,128]{1,0:T(8,128)(2,1)S(1)} %shard_map.124.refs_1_, f32[16,1024]{1,0:T(8,128)S(1)} %copy-done.9, f32[2,256,8]{2,1,0:T(8,128)S(1)} %get-tuple-element.29.refs_2_.refs_3_, ...), custom_call_target="tpu_custom_call" | custom-call | flops 2000000000 | tf_op jit(solution)/shard_map/pallas_call | solution.py:356
  29.0 0.4 collective-permute-start.16
  29.6 0.9 %shard_map.127 = (bf16[32,2048]{1,0:T(8,128)(2,1)S(1)}, bf16[96,2048]{1,0:T(8,128)(2,1)S(1)}) custom-call(bf16[256,256]{1,0:T(8,128)(2,1)S(1)} %get-tuple-element.24.refs_0_, bf16[256,128]{1,0:T(8,128)(2,1)S(1)} %shard_map.124.refs_1_, f32[16,1024]{1,0:T(8,128)S(1)} %copy-done.9, f32[2,256,8]{2,1,0:T(8,128)S(1)} %get-tuple-element.29.refs_2_.refs_3_, ...), custom_call_target="tpu_custom_call" | custom-call | flops 2000000000 | tf_op jit(solution)/shard_map/pallas_call | solution.py:356
  30.5 0.5 %collective-permute-done.14.got_ref = bf16[32,2048]{1,0:T(8,128)(2,1)S(1)} collective-permute-done((bf16[32,2048]{1,0:T(8,128)(2,1)S(1)}, bf16[32,2048]{1,0:T(8,128)(2,1)S(1)}, u32[]{:S(2)}, u32[]{:S(2)}) %collective-permute-start.14) | collective-permute-done | bytes 131104 | tf_op jit(solution)/shard_map/ppermute | solution.py:341
  31.0 1.2 %collective-permute-start.15 = (bf16[32,2048]{1,0:T(8,128)(2,1)S(1)}, bf16[32,2048]{1,0:T(8,128)(2,1)S(1)}, u32[]{:S(2)}, u32[]{:S(2)}) collective-permute-start(bf16[32,2048]{1,0:T(8,128)(2,1)S(1)} %shard_map.129), channel_id=1, source_target_pairs={{0,6},{2,4},{4,2},{6,0},{1,7},{3,5},{5,3},{7,1},{8,14},{10,12},{12... | collective-permute-start | bytes 393224 | tf_op jit(solution)/shard_map/ppermute | solution.py:344
  32.4 1.5 %collective-permute-start.18 = (bf16[32,2048]{1,0:T(8,128)(2,1)S(1)}, bf16[32,2048]{1,0:T(8,128)(2,1)S(1)}, u32[]{:S(2)}, u32[]{:S(2)}) collective-permute-start(bf16[32,2048]{1,0:T(8,128)(2,1)S(1)} %get-tuple-element.41), channel_id=1, source_target_pairs={{0,2},{2,0},{4,6},{6,4},{1,3},{3,1},{5,7},{7,5},{8,10},{10,8},{12,... | collective-permute-start | bytes 393224 | tf_op jit(solution)/shard_map/ppermute | solution.py:344
  33.9 2.8 %collective-permute-done.15.refs_0_ = bf16[32,2048]{1,0:T(8,128)(2,1)S(1)} collective-permute-done((bf16[32,2048]{1,0:T(8,128)(2,1)S(1)}, bf16[32,2048]{1,0:T(8,128)(2,1)S(1)}, u32[]{:S(2)}, u32[]{:S(2)}) %collective-permute-start.15) | collective-permute-done | bytes 131104 | tf_op jit(solution)/shard_map/ppermute | solution.py:344
  36.7 3.5 %collective-permute-done.17.refs_1_ = bf16[32,2048]{1,0:T(8,128)(2,1)S(1)} collective-permute-done((bf16[32,2048]{1,0:T(8,128)(2,1)S(1)}, bf16[32,2048]{1,0:T(8,128)(2,1)S(1)}, u32[]{:S(2)}, u32[]{:S(2)}) %collective-permute-start.17) | collective-permute-done | bytes 131104 | tf_op jit(solution)/shard_map/ppermute | solution.py:344
  40.2 0.7 %shard_map.131 = bf16[32,2048]{1,0:T(8,128)(2,1)} custom-call(bf16[32,2048]{1,0:T(8,128)(2,1)S(1)} %collective-permute-done.15.refs_0_, bf16[32,2048]{1,0:T(8,128)(2,1)S(1)} %collective-permute-done.17.refs_1_, bf16[32,2048]{1,0:T(8,128)(2,1)S(1)} %collective-permute-done.18.refs_2_, f32[32,2048]{1,0:T(8,128)S(1)} %get-tuple-element.42.refs_3_), custom_call_target="tpu_custom_call" | custom-call | tf_op jit(solution)/shard_map/pallas_call | solution.py:356
  (44 shorter events, 0.8 us)
Async XLA Ops:
  0.0 0.9 %copy-start.8 = (bf16[32,2048]{1,0:T(8,128)(2,1)S(1)}, bf16[32,2048]{1,0:T(8,128)(2,1)}, u32[]{:S(2)}) copy-start(bf16[32,2048]{1,0:T(8,128)(2,1)} %tokens_ref.1) | copy-start | bytes 393220
  0.9 0.7 %copy-start.10 = (f32[2048]{0:T(1024)S(1)}, f32[2048]{0:T(1024)}, u32[]{:S(2)}) copy-start(f32[2048]{0:T(1024)} %param.13) | copy-start | bytes 24580
  1.6 9.3 %copy-start.3 = (bf16[2048,128]{1,0:T(8,128)(2,1)S(1)}, bf16[2048,128]{1,0:T(8,128)(2,1)}, u32[]{:S(2)}) copy-start(bf16[2048,128]{1,0:T(8,128)(2,1)} %refs_4_.1) | copy-start | bytes 1572868
  1.6 9.3 %copy-start.4 = (bf16[2048,128]{1,0:T(8,128)(2,1)S(1)}, bf16[2048,128]{1,0:T(8,128)(2,1)}, u32[]{:S(2)}) copy-start(bf16[2048,128]{1,0:T(8,128)(2,1)} %refs_5_.1) | copy-start | bytes 1572868
  1.7 5.3 %collective-permute-start.2 = (bf16[32,2048]{1,0:T(8,128)(2,1)S(1)}, bf16[32,2048]{1,0:T(8,128)(2,1)S(1)}, u32[]{:S(2)}, u32[]{:S(2)}) collective-permute-start(bf16[32,2048]{1,0:T(8,128)(2,1)S(1)} %shard_map.118.refs_0_), channel_id=1, source_target_pairs={{0,6},{2,4},{4,2},{6,0},{1,7},{3,5},{5,3},{7,1},{8,14},{10,12},{12... | collective-permute-start | bytes 393224 | tf_op jit(solution)/shard_map/ppermute | solution.py:344
  3.0 8.0 %collective-permute-start.1 = (bf16[32,2048]{1,0:T(8,128)(2,1)S(1)}, bf16[32,2048]{1,0:T(8,128)(2,1)S(1)}, u32[]{:S(2)}, u32[]{:S(2)}) collective-permute-start(bf16[32,2048]{1,0:T(8,128)(2,1)S(1)} %shard_map.118.refs_0_), channel_id=1, source_target_pairs={{0,4},{2,6},{4,0},{6,2},{1,5},{3,7},{5,1},{7,3},{8,12},{10,14},{12... | collective-permute-start | bytes 393224 | tf_op jit(solution)/shard_map/ppermute | solution.py:344
  4.2 6.7 %collective-permute-start = (bf16[32,2048]{1,0:T(8,128)(2,1)S(1)}, bf16[32,2048]{1,0:T(8,128)(2,1)S(1)}, u32[]{:S(2)}, u32[]{:S(2)}) collective-permute-start(bf16[32,2048]{1,0:T(8,128)(2,1)S(1)} %shard_map.118.refs_0_), channel_id=1, source_target_pairs={{0,2},{2,0},{4,6},{6,4},{1,3},{3,1},{5,7},{7,5},{8,10},{10,8},{12,... | collective-permute-start | bytes 393224 | tf_op jit(solution)/shard_map/ppermute | solution.py:344
  4.5 8.2 %collective-permute-start.3 = (bf16[32,2048]{1,0:T(8,128)(2,1)S(1)}, bf16[32,2048]{1,0:T(8,128)(2,1)S(1)}, u32[]{:S(2)}, u32[]{:S(2)}) collective-permute-start(bf16[32,2048]{1,0:T(8,128)(2,1)S(1)} %shard_map.118.refs_0_), channel_id=1, source_target_pairs={{0,1},{1,0},{2,3},{3,2},{4,5},{5,4},{6,7},{7,6},{8,9},{9,8},{10,11... | collective-permute-start | bytes 393224 | tf_op jit(solution)/shard_map/ppermute | solution.py:341
  11.3 1.9 %copy-start = (bf16[256,2048]{1,0:T(8,128)(2,1)S(1)}, bf16[256,2048]{1,0:T(8,128)(2,1)}, u32[]{:S(2)}) copy-start(bf16[256,2048]{1,0:T(8,128)(2,1)} %low_ref.1) | copy-start | bytes 3145732
  11.3 1.9 %copy-start.1 = (bf16[128,2048]{1,0:T(8,128)(2,1)S(1)}, bf16[128,2048]{1,0:T(8,128)(2,1)}, u32[]{:S(2)}) copy-start(bf16[128,2048]{1,0:T(8,128)(2,1)} %top_ref.1) | copy-start | bytes 1572868
  11.3 5.0 %collective-permute-start.11 = (bf16[128,256]{1,0:T(8,128)(2,1)S(1)}, bf16[128,256]{1,0:T(8,128)(2,1)S(1)}, u32[]{:S(2)}, u32[]{:S(2)}) collective-permute-start(bf16[128,256]{1,0:T(8,128)(2,1)S(1)} %shard_map.120.refs_10_.refs_4_), channel_id=1, source_target_pairs={{0,24},{8,0},{16,8},{24,16},{1,25},{9,1},{17,9},{25,17},{2,26},{10... | collective-permute-start | bytes 196616 | tf_op jit(solution)/shard_map/ppermute | solution.py:348
  11.5 6.9 %collective-permute-start.9 = (bf16[128,256]{1,0:T(8,128)(2,1)S(1)}, bf16[128,256]{1,0:T(8,128)(2,1)S(1)}, u32[]{:S(2)}, u32[]{:S(2)}) collective-permute-start(bf16[128,256]{1,0:T(8,128)(2,1)S(1)} %shard_map.120.refs_10_.refs_4_), channel_id=1, source_target_pairs={{0,16},{8,24},{16,0},{24,8},{1,17},{9,25},{17,1},{25,9},{2,18},{10... | collective-permute-start | bytes 196616 | tf_op jit(solution)/shard_map/ppermute | solution.py:348
  11.6 8.2 %collective-permute-start.6 = (bf16[32,2048]{1,0:T(8,128)(2,1)S(1)}, bf16[32,2048]{1,0:T(8,128)(2,1)S(1)}, u32[]{:S(2)}, u32[]{:S(2)}) collective-permute-start(bf16[32,2048]{1,0:T(8,128)(2,1)S(1)} %collective-permute-done.2.refs_3_), channel_id=1, source_target_pairs={{0,1},{1,0},{2,3},{3,2},{4,5},{5,4},{6,7},{7,6},{8,9},{9,8},{10,11... | collective-permute-start | bytes 393224 | tf_op jit(solution)/shard_map/ppermute | solution.py:341
  12.6 7.1 %collective-permute-start.5 = (bf16[32,2048]{1,0:T(8,128)(2,1)S(1)}, bf16[32,2048]{1,0:T(8,128)(2,1)S(1)}, u32[]{:S(2)}, u32[]{:S(2)}) collective-permute-start(bf16[32,2048]{1,0:T(8,128)(2,1)S(1)} %collective-permute-done.1.refs_2_), channel_id=1, source_target_pairs={{0,1},{1,0},{2,3},{3,2},{4,5},{5,4},{6,7},{7,6},{8,9},{9,8},{10,11... | collective-permute-start | bytes 393224 | tf_op jit(solution)/shard_map/ppermute | solution.py:341
  12.6 7.1 %collective-permute-start.4 = (bf16[32,2048]{1,0:T(8,128)(2,1)S(1)}, bf16[32,2048]{1,0:T(8,128)(2,1)S(1)}, u32[]{:S(2)}, u32[]{:S(2)}) collective-permute-start(bf16[32,2048]{1,0:T(8,128)(2,1)S(1)} %collective-permute-done.refs_1_), channel_id=1, source_target_pairs={{0,1},{1,0},{2,3},{3,2},{4,5},{5,4},{6,7},{7,6},{8,9},{9,8},{10,11... | collective-permute-start | bytes 393224 | tf_op jit(solution)/shard_map/ppermute | solution.py:341
  13.2 6.6 %copy-start.5 = (bf16[2048,128]{1,0:T(8,128)(2,1)S(1)}, bf16[2048,128]{1,0:T(8,128)(2,1)}, u32[]{:S(2)}) copy-start(bf16[2048,128]{1,0:T(8,128)(2,1)} %refs_8_.3) | copy-start | bytes 1572868
  13.2 6.6 %copy-start.6 = (bf16[2048,128]{1,0:T(8,128)(2,1)S(1)}, bf16[2048,128]{1,0:T(8,128)(2,1)}, u32[]{:S(2)}) copy-start(bf16[2048,128]{1,0:T(8,128)(2,1)} %refs_9_.3) | copy-start | bytes 1572868
  13.3 8.4 %copy-start.2 = (bf16[2048,256]{1,0:T(8,128)(2,1)S(1)}, bf16[2048,256]{1,0:T(8,128)(2,1)}, u32[]{:S(2)}) copy-start(bf16[2048,256]{1,0:T(8,128)(2,1)} %refs_8_.2) | copy-start | bytes 3145732
  13.3 8.4 %copy-start.7 = (bf16[2048,128]{1,0:T(8,128)(2,1)S(1)}, bf16[2048,128]{1,0:T(8,128)(2,1)}, u32[]{:S(2)}) copy-start(bf16[2048,128]{1,0:T(8,128)(2,1)} %refs_9_.2) | copy-start | bytes 1572868
  16.3 6.2 %collective-permute-start.8 = (bf16[128,256]{1,0:T(8,128)(2,1)S(1)}, bf16[128,256]{1,0:T(8,128)(2,1)S(1)}, u32[]{:S(2)}, u32[]{:S(2)}) collective-permute-start(bf16[128,256]{1,0:T(8,128)(2,1)S(1)} %shard_map.120.refs_10_.refs_4_), channel_id=1, source_target_pairs={{0,1},{1,0},{2,3},{3,2},{4,5},{5,4},{6,7},{7,6},{8,9},{9,8},{10,11... | collective-permute-start | bytes 196616 | tf_op jit(solution)/shard_map/ppermute | solution.py:341
  18.5 4.8 %collective-permute-start.12 = (bf16[128,256]{1,0:T(8,128)(2,1)S(1)}, bf16[128,256]{1,0:T(8,128)(2,1)S(1)}, u32[]{:S(2)}, u32[]{:S(2)}) collective-permute-start(bf16[128,256]{1,0:T(8,128)(2,1)S(1)} %collective-permute-done.11.refs_8_), channel_id=1, source_target_pairs={{0,1},{1,0},{2,3},{3,2},{4,5},{5,4},{6,7},{7,6},{8,9},{9,8},{10,11... | collective-permute-start | bytes 196616 | tf_op jit(solution)/shard_map/ppermute | solution.py:341
  19.8 3.5 %collective-permute-start.10 = (bf16[128,256]{1,0:T(8,128)(2,1)S(1)}, bf16[128,256]{1,0:T(8,128)(2,1)S(1)}, u32[]{:S(2)}, u32[]{:S(2)}) collective-permute-start(bf16[128,256]{1,0:T(8,128)(2,1)S(1)} %collective-permute-done.9.refs_6_), channel_id=1, source_target_pairs={{0,1},{1,0},{2,3},{3,2},{4,5},{5,4},{6,7},{7,6},{8,9},{9,8},{10,11... | collective-permute-start | bytes 196616 | tf_op jit(solution)/shard_map/ppermute | solution.py:341
  20.3 2.2 %copy-start.9 = (f32[16,1024]{1,0:T(8,128)S(1)}, f32[16,1024]{1,0:T(8,128)}, u32[]{:S(2)}) copy-start(f32[16,1024]{1,0:T(8,128)} %refs_2_.3) | copy-start | bytes 196612
  20.3 2.2 %copy-start.11 = (bf16[3,1024]{1,0:T(4,128)(2,1)S(1)}, bf16[3,1024]{1,0:T(4,128)(2,1)}, u32[]{:S(2)}) copy-start(bf16[3,1024]{1,0:T(4,128)(2,1)} %refs_3_.1) | copy-start | bytes 18436
  20.3 5.2 %collective-permute-start.7 = (bf16[144,256]{1,0:T(8,128)(2,1)S(1)}, bf16[144,256]{1,0:T(8,128)(2,1)S(1)}, u32[]{:S(2)}, u32[]{:S(2)}) collective-permute-start(bf16[144,256]{1,0:T(8,128)(2,1)S(1)} %get-tuple-element.27), channel_id=1, source_target_pairs={{0,8},{8,16},{16,24},{1,9},{9,17},{17,25},{2,10},{10,18},{18,26},{... | collective-permute-start | bytes 221192 | tf_op jit(solution)/shard_map/ppermute | solution.py:348
  25.5 2.6 %collective-permute-start.13 = (bf16[144,256]{1,0:T(8,128)(2,1)S(1)}, bf16[144,256]{1,0:T(8,128)(2,1)S(1)}, u32[]{:S(2)}, u32[]{:S(2)}) collective-permute-start(bf16[144,256]{1,0:T(8,128)(2,1)S(1)} %collective-permute-done.7.risen_ref.refs_7_), channel_id=1, source_target_pairs={{0,1},{1,0},{2,3},{3,2},{4,5},{5,4},{6,7},{7,6},{8,9},{9,8},{10,11... | collective-permute-start | bytes 221192 | tf_op jit(solution)/shard_map/ppermute | solution.py:341
  29.0 3.2 %collective-permute-start.16 = (bf16[96,2048]{1,0:T(8,128)(2,1)S(1)}, bf16[96,2048]{1,0:T(8,128)(2,1)S(1)}, u32[]{:S(2)}, u32[]{:S(2)}) collective-permute-start(bf16[96,2048]{1,0:T(8,128)(2,1)S(1)} %get-tuple-element.39), channel_id=1, source_target_pairs={{0,1},{1,0},{2,3},{3,2},{4,5},{5,4},{6,7},{7,6},{8,9},{9,8},{10,11... | collective-permute-start | bytes 1179656 | tf_op jit(solution)/shard_map/ppermute | solution.py:341
  29.4 1.6 %collective-permute-start.14 = (bf16[32,2048]{1,0:T(8,128)(2,1)S(1)}, bf16[32,2048]{1,0:T(8,128)(2,1)S(1)}, u32[]{:S(2)}, u32[]{:S(2)}) collective-permute-start(bf16[32,2048]{1,0:T(8,128)(2,1)S(1)} %get-tuple-element.37), channel_id=1, source_target_pairs={{0,1},{1,0},{2,3},{3,2},{4,5},{5,4},{6,7},{7,6},{8,9},{9,8},{10,11... | collective-permute-start | bytes 393224 | tf_op jit(solution)/shard_map/ppermute | solution.py:341
  31.0 5.7 %collective-permute-start.15 = (bf16[32,2048]{1,0:T(8,128)(2,1)S(1)}, bf16[32,2048]{1,0:T(8,128)(2,1)S(1)}, u32[]{:S(2)}, u32[]{:S(2)}) collective-permute-start(bf16[32,2048]{1,0:T(8,128)(2,1)S(1)} %shard_map.129), channel_id=1, source_target_pairs={{0,6},{2,4},{4,2},{6,0},{1,7},{3,5},{5,3},{7,1},{8,14},{10,12},{12... | collective-permute-start | bytes 393224 | tf_op jit(solution)/shard_map/ppermute | solution.py:344
  32.3 7.9 %collective-permute-start.17 = (bf16[32,2048]{1,0:T(8,128)(2,1)S(1)}, bf16[32,2048]{1,0:T(8,128)(2,1)S(1)}, u32[]{:S(2)}, u32[]{:S(2)}) collective-permute-start(bf16[32,2048]{1,0:T(8,128)(2,1)S(1)} %get-tuple-element.40), channel_id=1, source_target_pairs={{0,4},{2,6},{4,0},{6,2},{1,5},{3,7},{5,1},{7,3},{8,12},{10,14},{12... | collective-permute-start | bytes 393224 | tf_op jit(solution)/shard_map/ppermute | solution.py:344
  32.4 7.8 %collective-permute-start.18 = (bf16[32,2048]{1,0:T(8,128)(2,1)S(1)}, bf16[32,2048]{1,0:T(8,128)(2,1)S(1)}, u32[]{:S(2)}, u32[]{:S(2)}) collective-permute-start(bf16[32,2048]{1,0:T(8,128)(2,1)S(1)} %get-tuple-element.41), channel_id=1, source_target_pairs={{0,2},{2,0},{4,6},{6,4},{1,3},{3,1},{5,7},{7,5},{8,10},{10,8},{12,... | collective-permute-start | bytes 393224 | tf_op jit(solution)/shard_map/ppermute | solution.py:344

commit v7 on v6

--- a/solution.py
+++ b/solution.py
@@ -15,7 +15,6 @@
 EDGE = 16
 RING = (False, False, True, True)
 NORM_WORK = 20000000000
-MASK_WORK = 2000000000
 SMALL_WORK = 2000000000
 
 
@@ -33,18 +32,20 @@
     out_ref[...] = jnp.where(query_place >= key_place, 0.0, masked_score)
 
 
-def norm_kernel(tokens_ref, gain_ref, out_ref):
-    rows = tokens_ref[...].astype(f32)
+def normalized(tokens, gain):
+    rows = tokens.astype(f32)
     scale = lax.rsqrt(jnp.mean(rows * rows, axis=1, keepdims=True) + epsilon)
-    out_ref[...] = (rows * scale * gain_ref[...]).astype(bf16)
+    return (rows * scale * gain).astype(bf16)
 
 
 def pair_kernel(n_fs, *refs):
-    chunks, (w_key, w_value, out_ref, rows_ref) = refs[:n_fs], refs[n_fs:]
+    chunks, (gain_ref, w_key, w_value, out_ref, normed_ref, rows_ref) = refs[:n_fs], refs[n_fs:]
     step = chunks[0].shape[0]
     f = lax.axis_index("fs")
     for k in range(n_fs):
-        rows_ref[pl.ds(pl.multiple_of((f ^ k) * step, step), step)] = chunks[k][...]
+        rows = normalized(chunks[k][...], gain_ref[...])
+        normed_ref[(n_fs - 1 - k) * step : (n_fs - k) * step] = rows
+        rows_ref[pl.ds(pl.multiple_of((f ^ k) * step, step), step)] = rows
     weight = jnp.concatenate([w_key[...], w_value[...]], axis=1)
     out_ref[...] = jnp.dot(rows_ref[...], weight, preferred_element_type=f32).astype(bf16)
 
@@ -190,15 +191,14 @@
     ]
 
 
-def gathered(own, other):
-    return jnp.concatenate([ref[...] for ref in (*other[::-1], *own[::-1])], axis=0)
-
-
 def gate_kernel(n_fs, *refs):
-    own, other = refs[:n_fs], refs[n_fs : 2 * n_fs]
-    w_pre, w_conv, pair_ref, mixed_ref, rise_ref = refs[2 * n_fs :]
-    step = own[0].shape[0]
-    rows = gathered(own, other)
+    other, (near_ref, gain_ref, w_pre, w_conv, pair_ref) = refs[:n_fs], refs[n_fs : n_fs + 5]
+    mixed_ref, rise_ref, rows_ref = refs[n_fs + 5 :]
+    step = other[0].shape[0]
+    for i, ref in enumerate(other[::-1]):
+        rows_ref[i * step : (i + 1) * step] = normalized(ref[...], gain_ref[...])
+    rows_ref[n_fs * step :] = near_ref[...]
+    rows = rows_ref[...]
     weight = jnp.concatenate([w_pre[...], w_conv[...]], axis=1)
     gated = jnp.dot(rows, weight, preferred_element_type=f32).astype(bf16).astype(f32)
     channels = w_pre.shape[1]
@@ -211,9 +211,8 @@
     rise_ref[lane_rows:] = jnp.concatenate([last] * (rise_ref.shape[1] // channels), axis=1)
 
 
-def query_kernel(n_fs, *refs):
-    rows = gathered(refs[:n_fs], refs[n_fs : 2 * n_fs])
-    w_query, w_post, q_ref, post_ref = refs[2 * n_fs :]
+def query_kernel(rows_ref, w_query, w_post, q_ref, post_ref):
+    rows = rows_ref[...]
     q_ref[...] = jnp.dot(rows, w_query[...], preferred_element_type=f32).astype(bf16)
     post_ref[...] = jnp.dot(rows, w_post[...], preferred_element_type=f32).astype(bf16)
 
@@ -361,26 +360,19 @@
             **extra,
         )(*operands)
 
-    mask = call(mask_kernel, shape_of(block_rows, block_rows, f32), [], 4, work=MASK_WORK)
-    normed = call(
-        norm_kernel,
-        shape_of(step, width),
-        [],
-        4,
-        tokens,
-        norm_gain.reshape(1, width),
-        work=NORM_WORK,
-    )
+    mask = call(mask_kernel, shape_of(block_rows, block_rows, f32), [], 4, work=NORM_WORK)
+    gain = norm_gain.reshape(1, width)
     w_post, w_pre, w_conv = w_conv_post, w_conv_pre, w_conv_value
     gates, taps = log_gate_cache, conv_taps
-    own = [normed] + [crossed(normed, k) for k in range(1, n_fs)]
+    own = [tokens] + [crossed(tokens, k) for k in range(1, n_fs)]
     other = [swapped(x) for x in own]
-    pair = call(
+    pair, near_rows = call(
         functools.partial(pair_kernel, n_fs),
-        shape_of(lane_rows, 2 * head_dim),
+        (shape_of(lane_rows, 2 * head_dim), shape_of(lane_rows, width)),
         [pltpu.VMEM((lane_rows, width), bf16)],
         8,
         *own,
+        gain,
         w_key,
         w_value,
         work=SMALL_WORK,
@@ -389,25 +381,29 @@
     for shift in range(2, n_sp):
         piece = raised(pair, shift)
         halves += [piece, swapped(piece)]
-    mixed, rise = call(
+    mixed, rise, rows = call(
         functools.partial(gate_kernel, n_fs),
-        (shape_of(block_rows, channels), shape_of(lane_rows + EDGE, 2 * head_dim)),
+        (
+            shape_of(block_rows, channels),
+            shape_of(lane_rows + EDGE, 2 * head_dim),
+            shape_of(block_rows, width),
+        ),
         [],
         16,
-        *own,
         *other,
+        near_rows,
+        gain,
         w_pre,
         w_conv,
         pair,
         work=SMALL_WORK,
     )
     queries, post = call(
-        functools.partial(query_kernel, n_fs),
+        query_kernel,
         (shape_of(block_rows, heads * head_dim), shape_of(block_rows, channels)),
         [],
         16,
-        *own,
-        *other,
+        rows,
         w_query,
         w_post,
         work=SMALL_WORK,

time: 41.1 us -> 43 us (1.046)
  the two profiles are of different devices: /device:TPU:29 before, /device:TPU:0 now
where the time goes in v7:
time: 43 us; the launch traced here: 42.3 us
  waiting for transfers between devices  18.6 us (43%)
  starting transfers between devices  14.9 us (35%)
  Pallas kernels  4.71 us (11%)
  local copies, waits for them, and re-layouts  3.82 us (9%)
    ppermute x6, waiting for transfers between devices, crossed(): return lax.ppermute(x, 'fs', [(i, i ^ k) for i in range(n_fs)])  11.9 us
    ppermute x6, starting transfers between devices, crossed(): return lax.ppermute(x, 'fs', [(i, i ^ k) for i in range(n_fs)])  8.11 us
    ppermute x3, starting transfers between devices, raised(): return lax.ppermute(x, 'sp', route)  5.18 us
    pallas_call x13, Pallas kernels, call(): pl.pallas_call(kernel, out_shape=out_shape, scratch_shapes=scratch, compi...  4.71 us
    ppermute x3, waiting for transfers between devices, raised(): return lax.ppermute(x, 'sp', route)  4.66 us
    unnamed x26, local copies, waits for them, and re-layouts  3.82 us
    ppermute x10, waiting for transfers between devices, swapped(): return lax.ppermute(x, 'tp', [(0, 1), (1, 0)])  2.13 us
    ppermute x10, starting transfers between devices, swapped(): return lax.ppermute(x, 'tp', [(0, 1), (1, 0)])  1.61 us
  transfers between devices with their start and end apart: 19, of which 10 were waited for; matrix products, arithmetic and copies ran while one was open for 0% of the time, Pallas kernels for 8%

profile of v7, /device:TPU:0, one launch (start us, length us, event | category | flops | bytes accessed | tf_op | source)
XLA Modules:
  0.0 42.3 jit_solution(18069057079437487162)
XLA Ops:
  0.0 3.0 %collective-permute-start.3 = (bf16[32,2048]{1,0:T(8,128)(2,1)}, bf16[32,2048]{1,0:T(8,128)(2,1)S(1)}, u32[]{:S(2)}, u32[]{:S(2)}) collective-permute-start(bf16[32,2048]{1,0:T(8,128)(2,1)} %refs_0_.1), channel_id=1, source_target_pairs={{0,4},{2,6},{4,0},{6,2},{1,5},{3,7},{5,1},{7,3},{8,12},{10,14},{12... | collective-permute-start | bytes 393224 | tf_op jit(solution)/shard_map/ppermute | solution.py:343
  3.0 1.5 %collective-permute-start.1 = (bf16[32,2048]{1,0:T(8,128)(2,1)}, bf16[32,2048]{1,0:T(8,128)(2,1)S(1)}, u32[]{:S(2)}, u32[]{:S(2)}) collective-permute-start(bf16[32,2048]{1,0:T(8,128)(2,1)} %refs_0_.1), channel_id=1, source_target_pairs={{0,2},{2,0},{4,6},{6,4},{1,3},{3,1},{5,7},{7,5},{8,10},{10,8},{12,... | collective-permute-start | bytes 393224 | tf_op jit(solution)/shard_map/ppermute | solution.py:343
  4.5 2.2 %collective-permute-done.3.refs_2_ = bf16[32,2048]{1,0:T(8,128)(2,1)S(1)} collective-permute-done((bf16[32,2048]{1,0:T(8,128)(2,1)}, bf16[32,2048]{1,0:T(8,128)(2,1)S(1)}, u32[]{:S(2)}, u32[]{:S(2)}) %collective-permute-start.3) | collective-permute-done | bytes 131104 | tf_op jit(solution)/shard_map/ppermute | solution.py:343
  6.7 2.9 %collective-permute-done.1.refs_1_ = bf16[32,2048]{1,0:T(8,128)(2,1)S(1)} collective-permute-done((bf16[32,2048]{1,0:T(8,128)(2,1)}, bf16[32,2048]{1,0:T(8,128)(2,1)S(1)}, u32[]{:S(2)}, u32[]{:S(2)}) %collective-permute-start.1) | collective-permute-done | bytes 131104 | tf_op jit(solution)/shard_map/ppermute | solution.py:343
  9.6 1.1 %collective-permute-done.5.refs_3_ = bf16[32,2048]{1,0:T(8,128)(2,1)S(1)} collective-permute-done((bf16[32,2048]{1,0:T(8,128)(2,1)}, bf16[32,2048]{1,0:T(8,128)(2,1)S(1)}, u32[]{:S(2)}, u32[]{:S(2)}) %collective-permute-start.5) | collective-permute-done | bytes 131104 | tf_op jit(solution)/shard_map/ppermute | solution.py:343
  10.7 1.0 %copy-done.3 = bf16[2048,128]{1,0:T(8,128)(2,1)S(1)} copy-done((bf16[2048,128]{1,0:T(8,128)(2,1)S(1)}, bf16[2048,128]{1,0:T(8,128)(2,1)}, u32[]{:S(2)}) %copy-start.3) | copy-done | bytes 524312
  11.7 1.0 %copy-done.4 = bf16[2048,128]{1,0:T(8,128)(2,1)S(1)} copy-done((bf16[2048,128]{1,0:T(8,128)(2,1)S(1)}, bf16[2048,128]{1,0:T(8,128)(2,1)}, u32[]{:S(2)}) %copy-start.4) | copy-done | bytes 524312
  12.8 0.9 %copy-done.8 = bf16[32,2048]{1,0:T(8,128)(2,1)S(1)} copy-done((bf16[32,2048]{1,0:T(8,128)(2,1)S(1)}, bf16[32,2048]{1,0:T(8,128)(2,1)}, u32[]{:S(2)}) %copy-start.8) | copy-done | bytes 131096
  13.7 0.7 %copy-done.10 = f32[2048]{0:T(1024)S(1)} copy-done((f32[2048]{0:T(1024)S(1)}, f32[2048]{0:T(1024)}, u32[]{:S(2)}) %copy-start.10) | copy-done | bytes 8216
  14.4 0.5 %shard_map.118 = (bf16[128,256]{1,0:T(8,128)(2,1)S(1)}, bf16[128,2048]{1,0:T(8,128)(2,1)S(1)}) custom-call(bf16[32,2048]{1,0:T(8,128)(2,1)S(1)} %copy-done.8, bf16[32,2048]{1,0:T(8,128)(2,1)S(1)} %collective-permute-done.1.refs_1_, bf16[32,2048]{1,0:T(8,128)(2,1)S(1)} %collective-permute-done.3.refs_2_, bf16[32,2048]{1,0:T(8,128)(2,1)S(1)} %collective-permute-done.5.refs_3_, ...), custom_call_target="tpu_custom_call" | custom-call | flops 2000000000 | tf_op jit(solution)/shard_map/pallas_call | solution.py:355
  15.0 3.9 %collective-permute-start.11 = (bf16[128,256]{1,0:T(8,128)(2,1)S(1)}, bf16[128,256]{1,0:T(8,128)(2,1)S(1)}, u32[]{:S(2)}, u32[]{:S(2)}) collective-permute-start(bf16[128,256]{1,0:T(8,128)(2,1)S(1)} %get-tuple-element.28.refs_8_.refs_4_), channel_id=1, source_target_pairs={{0,24},{8,0},{16,8},{24,16},{1,25},{9,1},{17,9},{25,17},{2,26},{10... | collective-permute-start | bytes 196616 | tf_op jit(solution)/shard_map/ppermute | solution.py:347
  18.8 0.5 %collective-permute-start.2 = (bf16[32,2048]{1,0:T(8,128)(2,1)S(1)}, bf16[32,2048]{1,0:T(8,128)(2,1)S(1)}, u32[]{:S(2)}, u32[]{:S(2)}) collective-permute-start(bf16[32,2048]{1,0:T(8,128)(2,1)S(1)} %collective-permute-done.1.refs_1_), channel_id=1, source_target_pairs={{0,1},{1,0},{2,3},{3,2},{4,5},{5,4},{6,7},{7,6},{8,9},{9,8},{10,11... | collective-permute-start | bytes 393224 | tf_op jit(solution)/shard_map/ppermute | solution.py:340
  19.5 1.2 %collective-permute-done.11.refs_8_ = bf16[128,256]{1,0:T(8,128)(2,1)S(1)} collective-permute-done((bf16[128,256]{1,0:T(8,128)(2,1)S(1)}, bf16[128,256]{1,0:T(8,128)(2,1)S(1)}, u32[]{:S(2)}, u32[]{:S(2)}) %collective-permute-start.11) | collective-permute-done | bytes 65568 | tf_op jit(solution)/shard_map/ppermute | solution.py:347
  20.7 3.3 %collective-permute-done.9.refs_6_ = bf16[128,256]{1,0:T(8,128)(2,1)S(1)} collective-permute-done((bf16[128,256]{1,0:T(8,128)(2,1)S(1)}, bf16[128,256]{1,0:T(8,128)(2,1)S(1)}, u32[]{:S(2)}, u32[]{:S(2)}) %collective-permute-start.9) | collective-permute-done | bytes 65568 | tf_op jit(solution)/shard_map/ppermute | solution.py:347
  24.0 0.5 %collective-permute-start.10 = (bf16[128,256]{1,0:T(8,128)(2,1)S(1)}, bf16[128,256]{1,0:T(8,128)(2,1)S(1)}, u32[]{:S(2)}, u32[]{:S(2)}) collective-permute-start(bf16[128,256]{1,0:T(8,128)(2,1)S(1)} %collective-permute-done.9.refs_6_), channel_id=1, source_target_pairs={{0,1},{1,0},{2,3},{3,2},{4,5},{5,4},{6,7},{7,6},{8,9},{9,8},{10,11... | collective-permute-start | bytes 196616 | tf_op jit(solution)/shard_map/ppermute | solution.py:340
  24.6 0.6 %shard_map.119 = (bf16[256,128]{1,0:T(8,128)(2,1)S(1)}, bf16[144,256]{1,0:T(8,128)(2,1)S(1)}, bf16[256,2048]{1,0:T(8,128)(2,1)S(1)}) custom-call(bf16[32,2048]{1,0:T(8,128)(2,1)S(1)} %collective-permute-done.refs_0_, bf16[32,2048]{1,0:T(8,128)(2,1)S(1)} %collective-permute-done.2.refs_1_, bf16[32,2048]{1,0:T(8,128)(2,1)S(1)} %collective-permute-done.4.refs_2_, ...), custom_call_target="tpu_custom_call" | custom-call | flops 2000000000 | tf_op jit(solution)/shard_map/pallas_call | solution.py:355
  25.2 1.3 %collective-permute-start.7 = (bf16[144,256]{1,0:T(8,128)(2,1)S(1)}, bf16[144,256]{1,0:T(8,128)(2,1)S(1)}, u32[]{:S(2)}, u32[]{:S(2)}) collective-permute-start(bf16[144,256]{1,0:T(8,128)(2,1)S(1)} %get-tuple-element.33), channel_id=1, source_target_pairs={{0,8},{8,16},{16,24},{1,9},{9,17},{17,25},{2,10},{10,18},{18,26},{... | collective-permute-start | bytes 221192 | tf_op jit(solution)/shard_map/ppermute | solution.py:347
  26.5 0.7 %shard_map.120 = (bf16[256,256]{1,0:T(8,128)(2,1)S(1)}, bf16[256,128]{1,0:T(8,128)(2,1)S(1)}) custom-call(bf16[256,2048]{1,0:T(8,128)(2,1)S(1)} %get-tuple-element.29.rows_ref, bf16[2048,256]{1,0:T(8,128)(2,1)S(1)} %copy-done.2, bf16[2048,128]{1,0:T(8,128)(2,1)S(1)} %copy-done.7), custom_call_target="tpu_custom_call" | custom-call | flops 2000000000 | tf_op jit(solution)/shard_map/pallas_call | solution.py:355
  27.4 0.8 %shard_map.122 = (f32[512,128]{1,0:T(8,128)S(1)}, f32[512,128]{1,0:T(8,128)S(1)}, f32[512,128]{1,0:T(8,128)S(1)}, f32[2,256,8]{2,1,0:T(8,128)S(1)}, f32[3,128]{1,0:T(4,128)S(1)}) custom-call(bf16[256,256]{1,0:T(8,128)(2,1)S(1)} %get-tuple-element.30.refs_0_, f32[16,1024]{1,0:T(8,128)S(1)} %copy-done.9, f32[256,256]{1,0:T(8,128)S(1)} %shard_map.121.refs_2_, ...), custom_call_target="tpu_custom_call" | custom-call | flops 2000000000 | tf_op jit(solution)/shard_map/pallas_call | solution.py:355
  28.2 0.2 collective-permute-done.7.risen_ref.refs_7_
  28.5 1.2 %collective-permute-done.13.refs_8_ = bf16[144,256]{1,0:T(8,128)(2,1)S(1)} collective-permute-done((bf16[144,256]{1,0:T(8,128)(2,1)S(1)}, bf16[144,256]{1,0:T(8,128)(2,1)S(1)}, u32[]{:S(2)}, u32[]{:S(2)}) %collective-permute-start.13) | collective-permute-done | bytes 73760 | tf_op jit(solution)/shard_map/ppermute | solution.py:340
  29.7 0.5 %shard_map.127 = (bf16[32,2048]{1,0:T(8,128)(2,1)S(1)}, bf16[96,2048]{1,0:T(8,128)(2,1)S(1)}) custom-call(bf16[256,256]{1,0:T(8,128)(2,1)S(1)} %get-tuple-element.30.refs_0_, bf16[256,128]{1,0:T(8,128)(2,1)S(1)} %shard_map.123.refs_1_, f32[16,1024]{1,0:T(8,128)S(1)} %copy-done.9, f32[2,256,8]{2,1,0:T(8,128)S(1)} %get-tuple-element.35.refs_2_.refs_3_, ...), custom_call_target="tpu_custom_call" | custom-call | flops 2000000000 | tf_op jit(solution)/shard_map/pallas_call | solution.py:355
  30.2 0.2 collective-permute-start.16
  30.4 0.4 collective-permute-start.14
  30.8 0.5 %shard_map.126 = (bf16[32,2048]{1,0:T(8,128)(2,1)S(1)}, bf16[96,2048]{1,0:T(8,128)(2,1)S(1)}) custom-call(bf16[256,256]{1,0:T(8,128)(2,1)S(1)} %get-tuple-element.30.refs_0_, bf16[256,128]{1,0:T(8,128)(2,1)S(1)} %shard_map.123.refs_1_, f32[16,1024]{1,0:T(8,128)S(1)} %copy-done.9, f32[2,256,8]{2,1,0:T(8,128)S(1)} %get-tuple-element.35.refs_2_.refs_3_, ...), custom_call_target="tpu_custom_call" | custom-call | flops 2000000000 | tf_op jit(solution)/shard_map/pallas_call | solution.py:355
  31.3 0.9 %collective-permute-done.14.got_ref = bf16[32,2048]{1,0:T(8,128)(2,1)S(1)} collective-permute-done((bf16[32,2048]{1,0:T(8,128)(2,1)S(1)}, bf16[32,2048]{1,0:T(8,128)(2,1)S(1)}, u32[]{:S(2)}, u32[]{:S(2)}) %collective-permute-start.14) | collective-permute-done | bytes 131104 | tf_op jit(solution)/shard_map/ppermute | solution.py:340
  32.2 2.5 %collective-permute-start.15 = (bf16[32,2048]{1,0:T(8,128)(2,1)S(1)}, bf16[32,2048]{1,0:T(8,128)(2,1)S(1)}, u32[]{:S(2)}, u32[]{:S(2)}) collective-permute-start(bf16[32,2048]{1,0:T(8,128)(2,1)S(1)} %shard_map.128), channel_id=1, source_target_pairs={{0,6},{2,4},{4,2},{6,0},{1,7},{3,5},{5,3},{7,1},{8,14},{10,12},{12... | collective-permute-start | bytes 393224 | tf_op jit(solution)/shard_map/ppermute | solution.py:343
  34.8 0.6 %collective-permute-start.17 = (bf16[32,2048]{1,0:T(8,128)(2,1)S(1)}, bf16[32,2048]{1,0:T(8,128)(2,1)S(1)}, u32[]{:S(2)}, u32[]{:S(2)}) collective-permute-start(bf16[32,2048]{1,0:T(8,128)(2,1)S(1)} %get-tuple-element.46), channel_id=1, source_target_pairs={{0,4},{2,6},{4,0},{6,2},{1,5},{3,7},{5,1},{7,3},{8,12},{10,14},{12... | collective-permute-start | bytes 393224 | tf_op jit(solution)/shard_map/ppermute | solution.py:343
  35.4 0.5 %collective-permute-start.18 = (bf16[32,2048]{1,0:T(8,128)(2,1)S(1)}, bf16[32,2048]{1,0:T(8,128)(2,1)S(1)}, u32[]{:S(2)}, u32[]{:S(2)}) collective-permute-start(bf16[32,2048]{1,0:T(8,128)(2,1)S(1)} %get-tuple-element.47), channel_id=1, source_target_pairs={{0,2},{2,0},{4,6},{6,4},{1,3},{3,1},{5,7},{7,5},{8,10},{10,8},{12,... | collective-permute-start | bytes 393224 | tf_op jit(solution)/shard_map/ppermute | solution.py:343
  36.0 3.0 %collective-permute-done.15.refs_0_ = bf16[32,2048]{1,0:T(8,128)(2,1)S(1)} collective-permute-done((bf16[32,2048]{1,0:T(8,128)(2,1)S(1)}, bf16[32,2048]{1,0:T(8,128)(2,1)S(1)}, u32[]{:S(2)}, u32[]{:S(2)}) %collective-permute-start.15) | collective-permute-done | bytes 131104 | tf_op jit(solution)/shard_map/ppermute | solution.py:343
  39.0 2.6 %collective-permute-done.17.refs_1_ = bf16[32,2048]{1,0:T(8,128)(2,1)S(1)} collective-permute-done((bf16[32,2048]{1,0:T(8,128)(2,1)S(1)}, bf16[32,2048]{1,0:T(8,128)(2,1)S(1)}, u32[]{:S(2)}, u32[]{:S(2)}) %collective-permute-start.17) | collective-permute-done | bytes 131104 | tf_op jit(solution)/shard_map/ppermute | solution.py:343
  41.6 0.7 %shard_map.130 = bf16[32,2048]{1,0:T(8,128)(2,1)} custom-call(bf16[32,2048]{1,0:T(8,128)(2,1)S(1)} %collective-permute-done.15.refs_0_, bf16[32,2048]{1,0:T(8,128)(2,1)S(1)} %collective-permute-done.17.refs_1_, bf16[32,2048]{1,0:T(8,128)(2,1)S(1)} %collective-permute-done.18.refs_2_, f32[32,2048]{1,0:T(8,128)S(1)} %get-tuple-element.48.refs_3_), custom_call_target="tpu_custom_call" | custom-call | tf_op jit(solution)/shard_map/pallas_call | solution.py:355
  (45 shorter events, 0.6 us)
Async XLA Ops:
  0.0 6.7 %collective-permute-start.3 = (bf16[32,2048]{1,0:T(8,128)(2,1)}, bf16[32,2048]{1,0:T(8,128)(2,1)S(1)}, u32[]{:S(2)}, u32[]{:S(2)}) collective-permute-start(bf16[32,2048]{1,0:T(8,128)(2,1)} %refs_0_.1), channel_id=1, source_target_pairs={{0,4},{2,6},{4,0},{6,2},{1,5},{3,7},{5,1},{7,3},{8,12},{10,14},{12... | collective-permute-start | bytes 393224 | tf_op jit(solution)/shard_map/ppermute | solution.py:343
  3.0 6.6 %collective-permute-start.1 = (bf16[32,2048]{1,0:T(8,128)(2,1)}, bf16[32,2048]{1,0:T(8,128)(2,1)S(1)}, u32[]{:S(2)}, u32[]{:S(2)}) collective-permute-start(bf16[32,2048]{1,0:T(8,128)(2,1)} %refs_0_.1), channel_id=1, source_target_pairs={{0,2},{2,0},{4,6},{6,4},{1,3},{3,1},{5,7},{7,5},{8,10},{10,8},{12,... | collective-permute-start | bytes 393224 | tf_op jit(solution)/shard_map/ppermute | solution.py:343
  4.5 6.2 %collective-permute-start.5 = (bf16[32,2048]{1,0:T(8,128)(2,1)}, bf16[32,2048]{1,0:T(8,128)(2,1)S(1)}, u32[]{:S(2)}, u32[]{:S(2)}) collective-permute-start(bf16[32,2048]{1,0:T(8,128)(2,1)} %refs_0_.1), channel_id=1, source_target_pairs={{0,6},{2,4},{4,2},{6,0},{1,7},{3,5},{5,3},{7,1},{8,14},{10,12},{12... | collective-permute-start | bytes 393224 | tf_op jit(solution)/shard_map/ppermute | solution.py:343
  4.5 14.9 %collective-permute-start = (bf16[32,2048]{1,0:T(8,128)(2,1)}, bf16[32,2048]{1,0:T(8,128)(2,1)S(1)}, u32[]{:S(2)}, u32[]{:S(2)}) collective-permute-start(bf16[32,2048]{1,0:T(8,128)(2,1)} %refs_0_.1), channel_id=1, source_target_pairs={{0,1},{1,0},{2,3},{3,2},{4,5},{5,4},{6,7},{7,6},{8,9},{9,8},{10,11... | collective-permute-start | bytes 393224 | tf_op jit(solution)/shard_map/ppermute | solution.py:340
  10.7 1.0 %copy-start.3 = (bf16[2048,128]{1,0:T(8,128)(2,1)S(1)}, bf16[2048,128]{1,0:T(8,128)(2,1)}, u32[]{:S(2)}) copy-start(bf16[2048,128]{1,0:T(8,128)(2,1)} %refs_5_.1) | copy-start | bytes 1572868
  11.7 1.0 %copy-start.4 = (bf16[2048,128]{1,0:T(8,128)(2,1)S(1)}, bf16[2048,128]{1,0:T(8,128)(2,1)}, u32[]{:S(2)}) copy-start(bf16[2048,128]{1,0:T(8,128)(2,1)} %refs_6_.2) | copy-start | bytes 1572868
  12.8 0.9 %copy-start.8 = (bf16[32,2048]{1,0:T(8,128)(2,1)S(1)}, bf16[32,2048]{1,0:T(8,128)(2,1)}, u32[]{:S(2)}) copy-start(bf16[32,2048]{1,0:T(8,128)(2,1)} %refs_0_.1) | copy-start | bytes 393220
  13.7 0.7 %copy-start.10 = (f32[2048]{0:T(1024)S(1)}, f32[2048]{0:T(1024)}, u32[]{:S(2)}) copy-start(f32[2048]{0:T(1024)} %param.13) | copy-start | bytes 24580
  14.9 4.5 %copy-start = (bf16[256,2048]{1,0:T(8,128)(2,1)S(1)}, bf16[256,2048]{1,0:T(8,128)(2,1)}, u32[]{:S(2)}) copy-start(bf16[256,2048]{1,0:T(8,128)(2,1)} %low_ref.1) | copy-start | bytes 3145732
  14.9 4.5 %copy-start.1 = (bf16[128,2048]{1,0:T(8,128)(2,1)S(1)}, bf16[128,2048]{1,0:T(8,128)(2,1)}, u32[]{:S(2)}) copy-start(bf16[128,2048]{1,0:T(8,128)(2,1)} %top_ref.1) | copy-start | bytes 1572868
  15.0 5.8 %collective-permute-start.11 = (bf16[128,256]{1,0:T(8,128)(2,1)S(1)}, bf16[128,256]{1,0:T(8,128)(2,1)S(1)}, u32[]{:S(2)}, u32[]{:S(2)}) collective-permute-start(bf16[128,256]{1,0:T(8,128)(2,1)S(1)} %get-tuple-element.28.refs_8_.refs_4_), channel_id=1, source_target_pairs={{0,24},{8,0},{16,8},{24,16},{1,25},{9,1},{17,9},{25,17},{2,26},{10... | collective-permute-start | bytes 196616 | tf_op jit(solution)/shard_map/ppermute | solution.py:347
  18.8 5.2 %collective-permute-start.9 = (bf16[128,256]{1,0:T(8,128)(2,1)S(1)}, bf16[128,256]{1,0:T(8,128)(2,1)S(1)}, u32[]{:S(2)}, u32[]{:S(2)}) collective-permute-start(bf16[128,256]{1,0:T(8,128)(2,1)S(1)} %get-tuple-element.28.refs_8_.refs_4_), channel_id=1, source_target_pairs={{0,16},{8,24},{16,0},{24,8},{1,17},{9,25},{17,1},{25,9},{2,18},{10... | collective-permute-start | bytes 196616 | tf_op jit(solution)/shard_map/ppermute | solution.py:347
  18.8 5.2 %collective-permute-start.4 = (bf16[32,2048]{1,0:T(8,128)(2,1)S(1)}, bf16[32,2048]{1,0:T(8,128)(2,1)S(1)}, u32[]{:S(2)}, u32[]{:S(2)}) collective-permute-start(bf16[32,2048]{1,0:T(8,128)(2,1)S(1)} %collective-permute-done.3.refs_2_), channel_id=1, source_target_pairs={{0,1},{1,0},{2,3},{3,2},{4,5},{5,4},{6,7},{7,6},{8,9},{9,8},{10,11... | collective-permute-start | bytes 393224 | tf_op jit(solution)/shard_map/ppermute | solution.py:340
  18.8 5.7 %collective-permute-start.2 = (bf16[32,2048]{1,0:T(8,128)(2,1)S(1)}, bf16[32,2048]{1,0:T(8,128)(2,1)S(1)}, u32[]{:S(2)}, u32[]{:S(2)}) collective-permute-start(bf16[32,2048]{1,0:T(8,128)(2,1)S(1)} %collective-permute-done.1.refs_1_), channel_id=1, source_target_pairs={{0,1},{1,0},{2,3},{3,2},{4,5},{5,4},{6,7},{7,6},{8,9},{9,8},{10,11... | collective-permute-start | bytes 393224 | tf_op jit(solution)/shard_map/ppermute | solution.py:340
  19.4 5.2 %collective-permute-start.6 = (bf16[32,2048]{1,0:T(8,128)(2,1)S(1)}, bf16[32,2048]{1,0:T(8,128)(2,1)S(1)}, u32[]{:S(2)}, u32[]{:S(2)}) collective-permute-start(bf16[32,2048]{1,0:T(8,128)(2,1)S(1)} %collective-permute-done.5.refs_3_), channel_id=1, source_target_pairs={{0,1},{1,0},{2,3},{3,2},{4,5},{5,4},{6,7},{7,6},{8,9},{9,8},{10,11... | collective-permute-start | bytes 393224 | tf_op jit(solution)/shard_map/ppermute | solution.py:340
  19.4 5.1 %copy-start.5 = (bf16[2048,128]{1,0:T(8,128)(2,1)S(1)}, bf16[2048,128]{1,0:T(8,128)(2,1)}, u32[]{:S(2)}) copy-start(bf16[2048,128]{1,0:T(8,128)(2,1)} %refs_6_.3) | copy-start | bytes 1572868
  19.4 5.1 %copy-start.6 = (bf16[2048,128]{1,0:T(8,128)(2,1)S(1)}, bf16[2048,128]{1,0:T(8,128)(2,1)}, u32[]{:S(2)}) copy-start(bf16[2048,128]{1,0:T(8,128)(2,1)} %refs_7_.1) | copy-start | bytes 1572868
  19.4 5.1 %copy-start.11 = (f32[2048]{0:T(1024)S(1)}, f32[2048]{0:T(1024)}, u32[]{:S(2)}) copy-start(f32[2048]{0:T(1024)} %param.13) | copy-start | bytes 24580
  20.7 6.5 %collective-permute-start.8 = (bf16[128,256]{1,0:T(8,128)(2,1)S(1)}, bf16[128,256]{1,0:T(8,128)(2,1)S(1)}, u32[]{:S(2)}, u32[]{:S(2)}) collective-permute-start(bf16[128,256]{1,0:T(8,128)(2,1)S(1)} %get-tuple-element.28.refs_8_.refs_4_), channel_id=1, source_target_pairs={{0,1},{1,0},{2,3},{3,2},{4,5},{5,4},{6,7},{7,6},{8,9},{9,8},{10,11... | collective-permute-start | bytes 196616 | tf_op jit(solution)/shard_map/ppermute | solution.py:340
  24.0 4.1 %collective-permute-start.12 = (bf16[128,256]{1,0:T(8,128)(2,1)S(1)}, bf16[128,256]{1,0:T(8,128)(2,1)S(1)}, u32[]{:S(2)}, u32[]{:S(2)}) collective-permute-start(bf16[128,256]{1,0:T(8,128)(2,1)S(1)} %collective-permute-done.11.refs_8_), channel_id=1, source_target_pairs={{0,1},{1,0},{2,3},{3,2},{4,5},{5,4},{6,7},{7,6},{8,9},{9,8},{10,11... | collective-permute-start | bytes 196616 | tf_op jit(solution)/shard_map/ppermute | solution.py:340
  24.0 4.1 %collective-permute-start.10 = (bf16[128,256]{1,0:T(8,128)(2,1)S(1)}, bf16[128,256]{1,0:T(8,128)(2,1)S(1)}, u32[]{:S(2)}, u32[]{:S(2)}) collective-permute-start(bf16[128,256]{1,0:T(8,128)(2,1)S(1)} %collective-permute-done.9.refs_6_), channel_id=1, source_target_pairs={{0,1},{1,0},{2,3},{3,2},{4,5},{5,4},{6,7},{7,6},{8,9},{9,8},{10,11... | collective-permute-start | bytes 196616 | tf_op jit(solution)/shard_map/ppermute | solution.py:340
  24.5 1.9 %copy-start.2 = (bf16[2048,256]{1,0:T(8,128)(2,1)S(1)}, bf16[2048,256]{1,0:T(8,128)(2,1)}, u32[]{:S(2)}) copy-start(bf16[2048,256]{1,0:T(8,128)(2,1)} %w_query.1) | copy-start | bytes 3145732
  24.6 1.9 %copy-start.7 = (bf16[2048,128]{1,0:T(8,128)(2,1)S(1)}, bf16[2048,128]{1,0:T(8,128)(2,1)}, u32[]{:S(2)}) copy-start(bf16[2048,128]{1,0:T(8,128)(2,1)} %w_post.1) | copy-start | bytes 1572868
  25.2 3.3 %collective-permute-start.7 = (bf16[144,256]{1,0:T(8,128)(2,1)S(1)}, bf16[144,256]{1,0:T(8,128)(2,1)S(1)}, u32[]{:S(2)}, u32[]{:S(2)}) collective-permute-start(bf16[144,256]{1,0:T(8,128)(2,1)S(1)} %get-tuple-element.33), channel_id=1, source_target_pairs={{0,8},{8,16},{16,24},{1,9},{9,17},{17,25},{2,10},{10,18},{18,26},{... | collective-permute-start | bytes 221192 | tf_op jit(solution)/shard_map/ppermute | solution.py:347
  26.5 0.8 %copy-start.9 = (f32[16,1024]{1,0:T(8,128)S(1)}, f32[16,1024]{1,0:T(8,128)}, u32[]{:S(2)}) copy-start(f32[16,1024]{1,0:T(8,128)} %refs_2_.3) | copy-start | bytes 196612
  26.5 0.8 %copy-start.12 = (bf16[3,1024]{1,0:T(4,128)(2,1)S(1)}, bf16[3,1024]{1,0:T(4,128)(2,1)}, u32[]{:S(2)}) copy-start(bf16[3,1024]{1,0:T(4,128)(2,1)} %refs_3_.1) | copy-start | bytes 18436
  28.5 1.3 %collective-permute-start.13 = (bf16[144,256]{1,0:T(8,128)(2,1)S(1)}, bf16[144,256]{1,0:T(8,128)(2,1)S(1)}, u32[]{:S(2)}, u32[]{:S(2)}) collective-permute-start(bf16[144,256]{1,0:T(8,128)(2,1)S(1)} %collective-permute-done.7.risen_ref.refs_7_), channel_id=1, source_target_pairs={{0,1},{1,0},{2,3},{3,2},{4,5},{5,4},{6,7},{7,6},{8,9},{9,8},{10,11... | collective-permute-start | bytes 221192 | tf_op jit(solution)/shard_map/ppermute | solution.py:340
  30.2 4.5 %collective-permute-start.16 = (bf16[96,2048]{1,0:T(8,128)(2,1)S(1)}, bf16[96,2048]{1,0:T(8,128)(2,1)S(1)}, u32[]{:S(2)}, u32[]{:S(2)}) collective-permute-start(bf16[96,2048]{1,0:T(8,128)(2,1)S(1)} %get-tuple-element.45), channel_id=1, source_target_pairs={{0,1},{1,0},{2,3},{3,2},{4,5},{5,4},{6,7},{7,6},{8,9},{9,8},{10,11... | collective-permute-start | bytes 1179656 | tf_op jit(solution)/shard_map/ppermute | solution.py:340
  30.4 1.8 %collective-permute-start.14 = (bf16[32,2048]{1,0:T(8,128)(2,1)S(1)}, bf16[32,2048]{1,0:T(8,128)(2,1)S(1)}, u32[]{:S(2)}, u32[]{:S(2)}) collective-permute-start(bf16[32,2048]{1,0:T(8,128)(2,1)S(1)} %get-tuple-element.43), channel_id=1, source_target_pairs={{0,1},{1,0},{2,3},{3,2},{4,5},{5,4},{6,7},{7,6},{8,9},{9,8},{10,11... | collective-permute-start | bytes 393224 | tf_op jit(solution)/shard_map/ppermute | solution.py:340
  32.2 6.7 %collective-permute-start.15 = (bf16[32,2048]{1,0:T(8,128)(2,1)S(1)}, bf16[32,2048]{1,0:T(8,128)(2,1)S(1)}, u32[]{:S(2)}, u32[]{:S(2)}) collective-permute-start(bf16[32,2048]{1,0:T(8,128)(2,1)S(1)} %shard_map.128), channel_id=1, source_target_pairs={{0,6},{2,4},{4,2},{6,0},{1,7},{3,5},{5,3},{7,1},{8,14},{10,12},{12... | collective-permute-start | bytes 393224 | tf_op jit(solution)/shard_map/ppermute | solution.py:343
  34.8 6.7 %collective-permute-start.17 = (bf16[32,2048]{1,0:T(8,128)(2,1)S(1)}, bf16[32,2048]{1,0:T(8,128)(2,1)S(1)}, u32[]{:S(2)}, u32[]{:S(2)}) collective-permute-start(bf16[32,2048]{1,0:T(8,128)(2,1)S(1)} %get-tuple-element.46), channel_id=1, source_target_pairs={{0,4},{2,6},{4,0},{6,2},{1,5},{3,7},{5,1},{7,3},{8,12},{10,14},{12... | collective-permute-start | bytes 393224 | tf_op jit(solution)/shard_map/ppermute | solution.py:343
  35.4 6.2 %collective-permute-start.18 = (bf16[32,2048]{1,0:T(8,128)(2,1)S(1)}, bf16[32,2048]{1,0:T(8,128)(2,1)S(1)}, u32[]{:S(2)}, u32[]{:S(2)}) collective-permute-start(bf16[32,2048]{1,0:T(8,128)(2,1)S(1)} %get-tuple-element.47), channel_id=1, source_target_pairs={{0,2},{2,0},{4,6},{6,4},{1,3},{3,1},{5,7},{7,5},{8,10},{10,8},{12,... | collective-permute-start | bytes 393224 | tf_op jit(solution)/shard_map/ppermute | solution.py:343
